TPU v7x, 128 devices: a whole 4x4x4 slice. The times are simulated.
128 devices in a mesh: sp: 64 (over z, y, x), tp: 2 (over core).
Axes of the slice: x: 4, y: 4, z: 4, core: 2. Of those that a mesh axis runs over, the one named last changes fastest.
Arguments:
- out_grad: bfloat16 [14336, 2048], P('sp'), may hold values from -16 to 16
- routes: int32 [14336, 2], P('sp'), may hold values from 0 to 63, all different within a row; in each aligned block of 224 rows (0 to 223, 224 to 447, ...) at most 18 rows name the same one
- route_weights: float32 [14336, 2], P('sp'), may hold values from 0.5 to 2
- routed_rows: bfloat16 [64, 64, 18, 2048], P('sp'), may hold values from -6 to 6
- gate_weight: bfloat16 [64, 2048, 1024], P('sp', None, 'tp'), may hold values from -0.125 to 0.125
- up_weight: bfloat16 [64, 2048, 1024], P('sp', None, 'tp'), may hold values from -0.125 to 0.125
- down_weight: bfloat16 [64, 1024, 2048], P('sp', 'tp'), may hold values from -0.1875 to 0.1875
- values: bfloat16 [14336, 1024], P('sp', 'tp'), may hold values from -0.625 to 0.625
- key_side: bfloat16 [14336, 512], P('sp', 'tp'), may hold values from -0.625 to 0.625
- query_side: bfloat16 [14336, 512], P('sp', 'tp'), may hold values from -0.625 to 0.625
- decay_log: float32 [16, 14336], P('tp', 'sp'), may hold values from -0.09 to 0, as said below
- gate_in: bfloat16 [14336, 1024], P('sp', 'tp'), may hold values from -6 to 6
- entry_states: float32 [64, 16, 64, 128], P('sp', 'tp'), may hold values from -6 to 6
- out_weight: bfloat16 [2048, 1024], P(None, 'tp'), may hold values from -0.1875 to 0.1875
Outputs:
- grad_hidden: bfloat16 [14336, 2048], P('sp')
- grad_gate_weight: bfloat16 [64, 2048, 1024], P('sp', None, 'tp')
- grad_up_weight: bfloat16 [64, 2048, 1024], P('sp', None, 'tp')
- grad_down_weight: bfloat16 [64, 1024, 2048], P('sp', 'tp')
- grad_out_weight: float32 [2048, 1024], P('sp', 'tp')
- grad_values: bfloat16 [14336, 1024], P('sp', 'tp')
- grad_key_side: bfloat16 [14336, 512], P('sp', 'tp')
- grad_query_side: bfloat16 [14336, 512], P('sp', 'tp')
- grad_decay: float32 [16, 14336], P('tp', 'sp')
- grad_gate_in: bfloat16 [14336, 1024], P('sp', 'tp')
Inputs may be any that keep to these rules, and one draw needn't show every extreme that they name: Each row names 2 different experts. Among the routes of one segment of 224 tokens no expert is named more than 18 times, and in some segments one expert is named exactly 18 times. `decay_log`: every entry is negative.
All inputs are finite; a program needn't handle non-finite values.
Results may differ from a plain program's by a relative error of at most 0.0072.
Values may be sent and summed in bfloat16 or wider, within the bound.
No kernel may reach another device: no remote copies, remote signals or barrier semaphores. Data moves between devices by JAX's collectives and lax.ppermute only.
A program may use at most 128 MiB of HBM per device.

v0:
```python
import functools

import jax
import jax.numpy as jnp
from jax import lax
from jax.experimental import pallas as pl
from jax.experimental.pallas import tpu as pltpu
from jax.sharding import Mesh
from jax.sharding import PartitionSpec as P

BF = jnp.bfloat16
F32 = jnp.float32
SP = ("sp_0", "sp_1", "sp_2")
PEERS = 64
CAP = 18
MAIN = 16
TAIL = CAP - MAIN
TOK = 224
HALF = 1024
COLS = HALF // 128
MSG = COLS * CAP
FH = 512
HEADS = 8
HD = 64
NS = 128
PER_GROUP = 4
GROUPS = 2

NT = (((1,), (1,)), ((), ()))
TN = (((0,), (0,)), ((), ()))
NN = (((1,), (0,)), ((), ()))


def cost(flops, nbytes):
    return pl.CostEstimate(flops=flops, bytes_accessed=nbytes, transcendentals=0)


def iota(shape, dim):
    return lax.broadcasted_iota(jnp.int32, shape, dim)


def dot(a, b, dims=NN):
    return lax.dot_general(a, b, dims, preferred_element_type=F32)


def split(a):
    hi = a.astype(BF)
    return hi, (a - hi.astype(F32)).astype(BF)


def dot2(a, b, dims=NN):
    hi, lo = split(a)
    return dot(hi, b, dims) + dot(lo, b, dims)


def dot2r(a, b, dims=NN):
    hi, lo = split(b)
    return dot(a, hi, dims) + dot(a, lo, dims)


def dot3(a, b, dims=NN):
    ah, al = split(a)
    bh, bl = split(b)
    return dot(ah, bh, dims) + (dot(ah, bl, dims) + dot(al, bh, dims))


def dotp(a, b, dims=NN):
    return lax.dot_general(
        a, b, dims, precision=lax.Precision.HIGHEST, preferred_element_type=F32
    )


def tail_rows(shape, row_dim):
    r = iota(shape, row_dim)
    return (r // TAIL) * 16 + (r % TAIL) * 8


def pack_tail(dt):
    place = iota((1024, 128), 0) - tail_rows((1024, 128), 1)
    out = None
    for c in range(COLS):
        mask = jnp.where(place == c, 1.0, 0.0).astype(BF)
        part = dot(mask, dt[:, c * 128 : (c + 1) * 128])
        out = part if out is None else out + part
    return out


def copy_out(from_ref, to_ref, sems, b):
    peers = slice(16 * b, 16 * b + 16)
    copy = pltpu.make_async_copy(from_ref.at[peers], to_ref.at[peers], sems.at[b])
    copy.start()
    return copy


def load(pairs, sems):
    copies = [
        pltpu.make_async_copy(far, near, sems.at[i]) for i, (far, near) in enumerate(pairs)
    ]
    for copy in copies:
        copy.start()
    for copy in copies:
        copy.wait()


def slots(routes):
    experts = iota((PEERS, TOK), 0)
    r0, r1 = routes[0:1, :], routes[1:2, :]
    h0, h1 = experts == r0, experts == r1
    counts = jnp.where(h0, 1.0, 0.0) + jnp.where(h1, 1.0, 0.0)
    before = jnp.where(iota((TOK, TOK), 0) < iota((TOK, TOK), 1), 1.0, 0.0).astype(BF)
    earlier = dot(counts.astype(BF), before)
    f0 = jnp.sum(jnp.where(h0, earlier, 0.0), axis=0, keepdims=True)
    f1 = jnp.sum(jnp.where(h1, earlier, 0.0), axis=0, keepdims=True)
    return r0, r1, f0, f1


def dispatch_kernel(
    tp_ref, far_routes, far_w, far_og, to_ref, routes_ref, w_ref, og_ref, out_ref, sems, in_sems
):
    own = half_of(tp_ref)
    load(((far_routes, routes_ref), (far_w, w_ref), (far_og.at[:, own], og_ref)), in_sems)
    r0, r1, f0, f1 = slots(routes_ref[...])
    w0, w1 = w_ref[0:1, :], w_ref[1:2, :]
    s0, s1 = f0.astype(jnp.int32), f1.astype(jnp.int32)
    m0 = jnp.where(s0 < MAIN, r0 * MAIN + s0, -1)
    m1 = jnp.where(s1 < MAIN, r1 * MAIN + s1, -1)
    t0 = jnp.where(s0 >= MAIN, r0 * TAIL + s0 - MAIN, -1)
    t1 = jnp.where(s1 >= MAIN, r1 * TAIL + s1 - MAIN, -1)
    og = og_ref[...]

    def rows_of(first, count, a0, a1):
        rows = iota((count, TOK), 0) + first
        q0, q1 = rows == a0, rows == a1
        pick = jnp.where(q0 | q1, 1.0, 0.0).astype(BF)
        scale = jnp.where(q0, w0, jnp.where(q1, w1, 0.0))
        scale = jnp.sum(scale, axis=1, keepdims=True)
        return (dot(pick, og) * scale).astype(BF)

    tail = pack_tail(rows_of(0, 128, t0, t1)).astype(BF)
    out_ref[:, 16 * COLS : MSG, :] = tail.reshape(PEERS, 16, 128)
    copies = []
    for b in range(4):
        block = rows_of(256 * b, 256, m0, m1)
        for c in range(COLS):
            out_ref[16 * b : 16 * b + 16, 16 * c : 16 * c + 16, :] = block[
                :, 128 * c : 128 * c + 128
            ].reshape(16, 16, 128)
        copies.append(copy_out(out_ref, to_ref, sems, b))
    for copy in copies:
        copy.wait()


def call(
    kernel,
    outs,
    args,
    flops,
    nbytes,
    scalar=None,
    scratch=(),
    name=None,
    limit=8,
    hbm_outs=(),
    hbm_ins=(),
):
    vmem = pl.BlockSpec(memory_space=pltpu.VMEM)
    far = pl.BlockSpec(memory_space=pltpu.HBM)
    in_specs = [far if i in hbm_ins else vmem for i in range(len(args))]
    if scalar is not None:
        in_specs = [pl.BlockSpec(memory_space=pltpu.SMEM)] + in_specs
        args = (scalar, *args)
    return pl.pallas_call(
        kernel,
        out_shape=outs,
        in_specs=in_specs,
        out_specs=[far if i in hbm_outs else vmem for i in range(len(outs))],
        scratch_shapes=list(scratch),
        compiler_params=pltpu.CompilerParams(vmem_limit_bytes=limit * 1024 * 1024),
        cost_estimate=cost(flops, nbytes),
        name=name,
    )(*args)


def sds(shape, dtype):
    return jax.ShapeDtypeStruct(shape, dtype)


def dispatch(tp, routes_t, weights_t, out_grad):
    dma = pltpu.SemaphoreType.DMA
    return call(
        dispatch_kernel,
        [sds((PEERS, MSG, 128), BF)],
        (routes_t, weights_t, out_grad),
        10**9,
        3 * 10**6,
        scalar=tp,
        scratch=[
            pltpu.VMEM((2, TOK), jnp.int32),
            pltpu.VMEM((2, TOK), F32),
            pltpu.VMEM((TOK, HALF), BF),
            pltpu.VMEM((PEERS, MSG, 128), BF),
            dma((4,)),
            dma((3,)),
        ],
        hbm_ins=(0, 1, 2),
        hbm_outs=(0,),
        limit=60,
        name="dispatch",
    )[0]


def half_of(tp_ref, other=False):
    half = 1 - tp_ref[0] if other else tp_ref[0]
    return pl.ds(pl.multiple_of(half * HALF, HALF), HALF)


def combine_kernel(tp_ref, meta_ref, ret_ref, og_ref, out_ref):
    own = og_ref[:, half_of(tp_ref)].astype(F32)
    meta = meta_ref[...].astype(jnp.int32)
    e0, s0, e1, s1 = (meta[:, k : k + 1] for k in range(4))
    m0 = jnp.where(s0 < MAIN, e0 * MAIN + s0, -1)
    m1 = jnp.where(s1 < MAIN, e1 * MAIN + s1, -1)
    t0 = jnp.where(s0 >= MAIN, e0 * 16 + (s0 - MAIN) * 8, -100)
    t1 = jnp.where(s1 >= MAIN, e1 * 16 + (s1 - MAIN) * 8, -100)
    lanes = iota((TOK, 1024), 1)
    pick = jnp.where((lanes == m0) | (lanes == m1), 1.0, 0.0).astype(BF)
    tail = ret_ref[:, 16 * COLS : MSG, :].reshape(1024, 128)
    d0, d1 = lanes - t0, lanes - t1
    for c in range(COLS):
        main = ret_ref[:, 16 * c : 16 * c + 16, :].reshape(1024, 128)
        tpick = jnp.where((d0 == c) | (d1 == c), 1.0, 0.0).astype(BF)
        moe = dot(pick, main) + dot(tpick, tail)
        cols = slice(128 * c, 128 * c + 128)
        out_ref[:, cols] = (own[:, cols] + moe).astype(BF)


def combine_rows(tp, meta, returned, out_grad):
    return call(
        combine_kernel,
        [sds((TOK, HALF), BF)],
        (meta, returned, out_grad),
        10**9,
        3 * 10**6,
        scalar=tp,
        name="combine",
    )[0]


def place_rows(msg_ref, arr_ref):
    for c in range(COLS):
        main = msg_ref[:, 16 * c : 16 * c + 16, :].reshape(1024, 128)
        arr_ref[0:1024, 128 * c : 128 * c + 128] = main
    tail = msg_ref[:, 16 * COLS : MSG, :].reshape(1024, 128)
    at = iota((128, 1024), 1) - tail_rows((128, 1024), 0)
    for c in range(COLS):
        mask = jnp.where(at == c, 1.0, 0.0).astype(BF)
        arr_ref[1024:1152, 128 * c : 128 * c + 128] = dot(mask, tail).astype(BF)


def first_half_kernel(tp_ref, mine_ref, down_ref, arr_ref, part_ref):
    place_rows(mine_ref, arr_ref)
    part_ref[...] = dot(arr_ref[...], down_ref[:, half_of(tp_ref)], NT)


def second_half_kernel(
    tp_ref, other_ref, down_ref, part_ref, a1_ref, a2_ref, arr_ref, gg_ref, ug_ref
):
    place_rows(other_ref, arr_ref)
    act_grad = part_ref[...] + dot(arr_ref[...], down_ref[:, half_of(tp_ref, True)], NT)
    gg_ref[...] = (act_grad * a1_ref[...]).astype(BF)
    ug_ref[...] = (act_grad * a2_ref[...]).astype(BF)


def hidden_grads(tp, mine, other, down, a1, a2):
    rows = PEERS * CAP
    own_cols, part = call(
        first_half_kernel,
        [sds((rows, HALF), BF), sds((rows, FH), F32)],
        (mine, down),
        2 * 10**9,
        10**7,
        scalar=tp,
        name="hidden_first",
    )
    other_cols, gg, ug = call(
        second_half_kernel,
        [sds((rows, HALF), BF), sds((rows, FH), BF), sds((rows, FH), BF)],
        (other, down, part, a1, a2),
        2 * 10**9,
        10**7,
        scalar=tp,
        name="hidden_second",
    )
    return (own_cols, other_cols), gg, ug


def down_kernel(tp_ref, act_ref, own_ref, other_ref, out_ref):
    for n in range(4):
        cols = slice(256 * n, 256 * n + 256)
        for other, ref in ((False, own_ref), (True, other_ref)):
            half = 1 - tp_ref[0] if other else tp_ref[0]
            to = pl.ds(pl.multiple_of(half * HALF + 256 * n, 256), 256)
            out_ref[:, to] = dot(act_ref[...], ref[:, cols], TN).astype(BF)


def down_grad(tp, act, arrived):
    return call(
        down_kernel,
        [sds((FH, 2 * HALF), BF)],
        (act, *arrived),
        2 * 10**9,
        10**7,
        scalar=tp,
        name="down_grad",
    )[0]


def span_kernel(other, half_ref, gg_ref, ug_ref, gw_ref, uw_ref, out_ref, tail_ref):
    base = (1 - half_ref[0] if other else half_ref[0]) * HALF
    for n in range(4):
        cols = pl.ds(pl.multiple_of(base + 256 * n, 256), 256)
        d = dot(gg_ref[...], gw_ref[cols, :], NT) + dot(ug_ref[...], uw_ref[cols, :], NT)
        d = d.astype(BF)
        for k in range(2):
            c = 2 * n + k
            part = d[:, 128 * k : 128 * k + 128]
            out_ref[:, 16 * c : 16 * c + 16, :] = part[:1024].reshape(PEERS, 16, 128)
            tail_ref[:, 128 * c : 128 * c + 128] = part[1024:]
    tail = pack_tail(tail_ref[...]).astype(BF)
    out_ref[:, 16 * COLS : MSG, :] = tail.reshape(PEERS, 16, 128)


def span_half(tp, other, gg, ug, gw, uw):
    return call(
        functools.partial(span_kernel, other),
        [sds((PEERS, MSG, 128), BF)],
        (gg, ug, gw, uw),
        4 * 10**9,
        10**7,
        scalar=tp,
        scratch=[pltpu.VMEM((128, HALF), BF)],
        name="span_half",
    )[0]


def decay_sums(decay):
    upto = jnp.where(iota((TOK, TOK), 0) <= iota((TOK, TOK), 1), 1.0, 0.0)
    down = jnp.where(iota((TOK, TOK), 0) >= iota((TOK, TOK), 1), 1.0, 0.0)
    return dotp(decay, upto), dotp(down, decay, NT)


def decay_weights(cum, cum_t, h):
    causal = iota((TOK, TOK), 0) >= iota((TOK, TOK), 1)
    spread = cum_t[:, h : h + 1] - cum[h : h + 1, :]
    return jnp.where(causal, jnp.exp(jnp.where(causal, spread, 0.0)), 0.0)


def head(h):
    return slice(HD * h, HD * h + HD)


def group(g):
    return slice(NS * g, NS * g + NS)


def forward_kernel(
    v_ref, k_ref, q_ref, decay_ref, gate_ref, e_ref, routes_ref, core_ref, mixed_ref, meta_ref
):
    r0, r1, f0, f1 = slots(routes_ref[...])
    zero = jnp.zeros((4, TOK), F32)
    table = jnp.concatenate([r0.astype(F32), f0, r1.astype(F32), f1, zero], axis=0).astype(BF)
    eye = jnp.where(iota((TOK, TOK), 0) == iota((TOK, TOK), 1), 1.0, 0.0).astype(BF)
    meta_ref[...] = dot(eye, table, NT)
    cum, cum_t = decay_sums(decay_ref[...])
    for g in range(GROUPS):
        q, k = q_ref[:, group(g)], k_ref[:, group(g)]
        scores = dot(q, k, NT)
        for h in range(PER_GROUP * g, PER_GROUP * g + PER_GROUP):
            m = scores * decay_weights(cum, cum_t, h)
            within = dot2(m, v_ref[:, head(h)])
            carried = dot2r(q, e_ref[h], NT)
            core = within + carried * jnp.exp(cum_t[:, h : h + 1])
            core_ref[:, head(h)] = core
            gate = gate_ref[:, head(h)].astype(F32)
            mixed_ref[:, head(h)] = (core * (gate * jax.nn.sigmoid(gate))).astype(BF)


def low_part(a, hi):
    return a - hi.astype(F32)


def cotangent_kernel(
    tp_ref, mine_ref, other_ref, ow_ref, core_ref, gate_ref, decay_ref, q_ref, mixed_ref,
    hidden_ref, dcore_ref, dgate_ref, to_ref, msg_ref, sems,
):
    first = tp_ref[0] == 0
    x, y = mine_ref[...], other_ref[...]
    lo, hi = jnp.where(first, x, y), jnp.where(first, y, x)
    hidden_ref[:, :HALF] = lo
    hidden_ref[:, HALF:] = hi
    cot = dot(lo, ow_ref[:HALF, :]) + dot(hi, ow_ref[HALF:, :])
    gate = gate_ref[...].astype(F32)
    sig = jax.nn.sigmoid(gate)
    dcore = cot * (gate * sig)
    dcore_ref[...] = dcore
    dgate_ref[...] = (cot * core_ref[...] * (sig * (1.0 + gate * (1.0 - sig)))).astype(BF)
    _, cum_t = decay_sums(decay_ref[...])
    growth = jnp.exp(cum_t)
    logs = jnp.sum(decay_ref[...], axis=1, keepdims=True)
    high, low = split(logs)
    mid, _ = split(low_part(logs, high))
    rest = low_part(logs, high) - mid.astype(F32)
    row = iota((8, 8, 128), 1)
    states = []
    for g in range(GROUPS):
        heads = range(PER_GROUP * g, PER_GROUP * g + PER_GROUP)
        grown = [dcore[:, head(h)] * growth[:, h : h + 1] for h in heads]
        states.append(dot2(jnp.concatenate(grown, axis=1), q_ref[:, group(g)], TN))
    for h in range(HEADS):
        at = HD * (h % PER_GROUP)
        state = states[h // PER_GROUP][at : at + HD]
        parts = [
            jnp.broadcast_to(p[h : h + 1, :], (8, 128)).reshape(1, 8, 128)
            for p in (high.astype(F32), mid.astype(F32), rest)
        ]
        extra = jnp.where(row == 0, parts[0], jnp.where(row == 1, parts[1], parts[2]))
        extra = jnp.where(row < 3, extra, 0.0)
        both = jnp.concatenate([state.reshape(8, 8, 128), extra], axis=1)
        msg_ref[8 * h : 8 * h + 8, 128:144, :] = both.astype(BF)
    copies = []
    for b in range(4):
        rows = hidden_ref[:, 512 * b : 512 * b + 512]
        share = dot(rows, mixed_ref[...], TN).astype(BF)
        for c in range(4):
            msg_ref[16 * b : 16 * b + 16, 32 * c : 32 * c + 32, :] = share[
                :, 128 * c : 128 * c + 128
            ].reshape(16, 32, 128)
        copies.append(copy_out(msg_ref, to_ref, sems, b))
    for copy in copies:
        copy.wait()


def backward_kernel(
    v_ref, k_ref, q_ref, decay_ref, e_ref, core_ref, dcore_ref, dv_ref, dk_ref, dq_ref, diff_ref
):
    cum, cum_t = decay_sums(decay_ref[...])
    for g in range(GROUPS):
        q, k = q_ref[:, group(g)], k_ref[:, group(g)]
        scores = dot(q, k, NT)
        ds = jnp.zeros((TOK, TOK), F32)
        dq = jnp.zeros((TOK, NS), F32)
        for h in range(PER_GROUP * g, PER_GROUP * g + PER_GROUP):
            w = decay_weights(cum, cum_t, h)
            dcore = dcore_ref[:, head(h)]
            dv = dot3(scores * w, dcore, TN)
            dv_ref[:, head(h)] = dv
            v = v_ref[:, head(h)].astype(F32)
            diff_ref[:, h : h + 1] = jnp.sum(
                dcore * core_ref[:, head(h)] - v * dv, axis=1, keepdims=True
            )
            ds = ds + dot2(dcore, v_ref[:, head(h)], NT) * w
            dq = dq + dot3(dcore * jnp.exp(cum_t[:, h : h + 1]), e_ref[h])
        dq_ref[:, group(g)] = (dq + dot2(ds, k)).astype(BF)
        dk_ref[:, group(g)] = dot2(ds, q, TN)


def ending_kernel(
    state_far, v_far, k_far, decay_far, e_far, dv_far, dk_far, diff_far,
    gv_ref, gk_ref, gd_ref, state_ref, v_ref, k_ref, decay_ref, e_ref, dv_ref, dk_ref, diff_ref, sems,
):
    load(
        (
            (state_far, state_ref),
            (decay_far, decay_ref),
            (v_far, v_ref),
            (k_far, k_ref),
            (e_far, e_ref),
            (dv_far, dv_ref),
            (dk_far, dk_ref),
            (diff_far, diff_ref),
        ),
        sems,
    )
    cum, cum_t = decay_sums(decay_ref[...])
    last = cum_t[TOK - 1 : TOK, :]
    tail = jnp.exp(last - cum_t)
    fresh = []
    kept = []
    diff = []
    for g in range(GROUPS):
        k = k_ref[:, group(g)]
        dk = dk_ref[:, group(g)]
        for h in range(PER_GROUP * g, PER_GROUP * g + PER_GROUP):
            state = state_ref[8 * h : 8 * h + 8].astype(F32).reshape(HD, NS)
            exact = state.astype(BF)
            v = v_ref[:, head(h)].astype(F32)
            t = tail[:, h : h + 1]
            dv2 = t * dot(k, exact, NT)
            dk = dk + dot2(v * t, exact)
            dv = dv_ref[:, head(h)] + dv2
            gv_ref[:, head(h)] = dv.astype(BF)
            moved = jnp.sum(v * dv2, axis=1, keepdims=True)
            diff.append(moved)
            fresh.append(jnp.sum(moved).reshape(1, 1))
            kept.append(jnp.sum(e_ref[h] * state).reshape(1, 1))
        gk_ref[:, group(g)] = dk.astype(BF)
    diff = diff_ref[...] - jnp.concatenate(diff, axis=1)
    at_end = jnp.concatenate(fresh, axis=1) + jnp.exp(last) * jnp.concatenate(kept, axis=1)
    diff = diff + jnp.where(iota((TOK, HEADS), 0) == TOK - 1, at_end, 0.0)
    later = jnp.where(iota((TOK, TOK), 0) >= iota((TOK, TOK), 1), 1.0, 0.0)
    gd_ref[...] = dotp(diff, later, TN)


def chain_kernel(in_ref, out_ref):
    wide = in_ref[:, 128:144, :].astype(F32)
    states = wide[:, 0:8, :].reshape(512, 128).astype(BF)
    logs = jnp.sum(wide[:, 8:16, :], axis=1)
    segment, entry = iota((512, PEERS), 0) // 8, iota((512, PEERS), 1)
    before = dotp(jnp.where(entry < segment, 1.0, 0.0), logs)
    through = dotp(jnp.where(entry <= segment, 1.0, 0.0), logs)
    i, j = iota((512, 512), 0), iota((512, 512), 1)
    later = (j // 8 > i // 8) & (j % 8 == i % 8)
    spread = jnp.transpose(before)[0:1, :] - through[:, 0:1]
    weights = jnp.where(later, jnp.exp(jnp.where(later, spread, 0.0)), 0.0)
    out_ref[...] = dot2(weights, states).reshape(PEERS, 8, 128).astype(BF)


def share_kernel(in_ref, out_ref):
    for c in range(4):
        total = in_ref[0, 32 * c : 32 * c + 32, :].astype(F32)
        for peer in range(1, PEERS):
            total = total + in_ref[peer, 32 * c : 32 * c + 32, :].astype(F32)
        out_ref[:, 128 * c : 128 * c + 128] = total


def per_device(
    out_grad,
    routes,
    route_weights,
    routed_rows,
    gate_weight,
    up_weight,
    down_weight,
    values,
    key_side,
    query_side,
    decay_log,
    gate_in,
    entry_states,
    out_weight,
):
    tp_index = lax.axis_index("tp").astype(jnp.int32)
    tp = tp_index.reshape(1)
    gate_w, up_w, down_w = gate_weight[0], up_weight[0], down_weight[0]
    entry = entry_states[0]

    def swap(x):
        return lax.ppermute(x, "tp", [(0, 1), (1, 0)])

    message = dispatch(tp, routes.T, route_weights.T, out_grad)
    moved = lax.all_to_all(message, SP, split_axis=0, concat_axis=0, tiled=True)

    rows = routed_rows[0]
    rows = jnp.concatenate(
        [rows[:, :MAIN].reshape(PEERS * MAIN, -1), rows[:, MAIN:].reshape(PEERS * TAIL, -1)], axis=0
    )
    gate_pre = jnp.dot(rows, gate_w, preferred_element_type=F32)
    up_pre = jnp.dot(rows, up_w, preferred_element_type=F32)
    sig = jax.nn.sigmoid(gate_pre)
    silu = gate_pre * sig
    act = (silu * up_pre).astype(BF)
    a1 = up_pre * sig * (1.0 + gate_pre * (1.0 - sig))
    _, later_values = lax.optimization_barrier((message, values))
    core, mixer_out, meta = call(
        forward_kernel,
        [sds((TOK, HEADS * HD), F32), sds((TOK, HEADS * HD), BF), sds((TOK, 8), F32)],
        (later_values, key_side, query_side, decay_log, gate_in, entry, routes.T),
        10**9,
        10**6,
        name="mixer_forward",
    )
    moved, rows, act, a1, silu, core, mixer_out, meta = lax.optimization_barrier(
        (moved, rows, act, a1, silu, core, mixer_out, meta)
    )

    arrived, gate_grad, up_grad = hidden_grads(tp, moved, swap(moved), down_w, a1, silu)
    for_peer = swap(span_half(tp, True, gate_grad, up_grad, gate_w, up_w))
    own_span = span_half(tp, False, gate_grad, up_grad, gate_w, up_w)
    back = (own_span.astype(F32) + for_peer.astype(F32)).astype(BF)
    returned = lax.all_to_all(back, SP, split_axis=0, concat_axis=0, tiled=True)

    _, gate_grad, up_grad, act = lax.optimization_barrier((back, gate_grad, up_grad, act))
    grad_down = down_grad(tp, act, arrived)
    grad_gate = dot(rows, gate_grad, TN).astype(BF)
    grad_up = dot(rows, up_grad, TN).astype(BF)
    returned, grad_down, grad_gate, grad_up = lax.optimization_barrier(
        (returned, grad_down, grad_gate, grad_up)
    )

    hidden_half = combine_rows(tp, meta, returned, out_grad)
    grad_hidden, dcore, dgate, tail_message = call(
        cotangent_kernel,
        [
            sds((TOK, 2 * HALF), BF),
            sds((TOK, FH), F32),
            sds((TOK, FH), BF),
            sds((PEERS, 144, NS), BF),
        ],
        (
            hidden_half,
            swap(hidden_half),
            out_weight,
            core,
            gate_in,
            decay_log,
            query_side,
            mixer_out,
        ),
        10**9,
        5 * 10**6,
        scalar=tp,
        scratch=[pltpu.VMEM((PEERS, 144, NS), BF), pltpu.SemaphoreType.DMA((4,))],
        hbm_outs=(3,),
        name="mixer_cotangent",
    )
    gathered = lax.all_to_all(tail_message, SP, split_axis=0, concat_axis=0, tiled=True)
    dv, dk, grad_query, diff = call(
        backward_kernel,
        [
            sds((TOK, HEADS * HD), F32),
            sds((TOK, GROUPS * NS), F32),
            sds((TOK, GROUPS * NS), BF),
            sds((TOK, HEADS), F32),
        ],
        (values, key_side, query_side, decay_log, entry, core, dcore),
        2 * 10**9,
        10**6,
        name="mixer_backward",
    )
    gathered, dv, dk, grad_query, diff = lax.optimization_barrier(
        (gathered, dv, dk, grad_query, diff)
    )
    states = call(
        chain_kernel,
        [sds((PEERS, 8, NS), BF)],
        (gathered,),
        10**8,
        10**6,
        name="state_chain",
    )[0]
    states = lax.all_to_all(states, SP, split_axis=0, concat_axis=0, tiled=True)
    grad_out_weight = call(
        share_kernel,
        [sds((32, FH), F32)],
        (gathered,),
        10**7,
        10**6,
        name="share_sum",
    )[0]
    grad_values, grad_key, grad_decay = call(
        ending_kernel,
        [
            sds((TOK, HEADS * HD), BF),
            sds((TOK, GROUPS * NS), BF),
            sds((HEADS, TOK), F32),
        ],
        (states, values, key_side, decay_log, entry, dv, dk, diff),
        10**9,
        10**6,
        scratch=[
            pltpu.VMEM((PEERS, 8, NS), BF),
            pltpu.VMEM((TOK, HEADS * HD), BF),
            pltpu.VMEM((TOK, GROUPS * NS), BF),
            pltpu.VMEM((HEADS, TOK), F32),
            pltpu.VMEM((HEADS, HD, NS), F32),
            pltpu.VMEM((TOK, HEADS * HD), F32),
            pltpu.VMEM((TOK, GROUPS * NS), F32),
            pltpu.VMEM((TOK, HEADS), F32),
            pltpu.SemaphoreType.DMA((8,)),
        ],
        hbm_ins=tuple(range(8)),
        limit=60,
        name="mixer_ending",
    )
    return (
        grad_hidden,
        grad_gate[None],
        grad_up[None],
        grad_down[None],
        grad_out_weight,
        grad_values,
        grad_key,
        grad_query,
        grad_decay,
        dgate,
    )


def solution(mesh):
    grid = Mesh(mesh.devices.reshape(4, 4, 4, mesh.shape["tp"]), ("sp_0", "sp_1", "sp_2", "tp"))
    placed = (
        P(SP, None),
        P(SP, None),
        P(SP, None),
        P(SP, None, None, None),
        P(SP, None, "tp"),
        P(SP, None, "tp"),
        P(SP, "tp", None),
        P(SP, "tp"),
        P(SP, "tp"),
        P(SP, "tp"),
        P("tp", SP),
        P(SP, "tp"),
        P(SP, "tp", None, None),
        P(None, "tp"),
    )
    return jax.shard_map(
        per_device,
        mesh=grid,
        in_specs=placed,
        out_specs=(
            P(SP, None),
            P(SP, None, "tp"),
            P(SP, None, "tp"),
            P(SP, "tp", None),
            P(SP, "tp"),
            P(SP, "tp"),
            P(SP, "tp"),
            P(SP, "tp"),
            P("tp", SP),
            P(SP, "tp"),
        ),
        check_vma=False,
    )
```

profile of v0, /device:TPU:0, one launch (start us, length us, event | category | flops | bytes accessed | tf_op | source)
XLA Modules:
  0.0 182.1 jit_solution(12121333824347266329)
XLA Ops:
  0.6 4.3 %dispatch.1 = bf16[64,144,128]{2,1,0:T(8,128)(2,1)} custom-call(s32[1]{0:T(128)} %bitcast.tp_ref.half_ref, s32[2,224]{1,0:T(2,128)} %bitcast.33, f32[2,224]{1,0:T(2,128)} %bitcast.43, bf16[224,2048]{1,0:T(8,128)(2,1)} %og_ref.1), custom_call_target="tpu_custom_call" | custom-call | flops 1000000000 | bytes 3000000 | tf_op jit(solution)/shard_map/dispatch/pallas_call | solution.py:172
  5.0 11.7 %all-to-all-start = ((bf16[64,144,128]{2,1,0:T(8,128)(2,1)}), bf16[64,144,128]{2,1,0:T(8,128)(2,1)S(1)}, u32[]{:S(2)}, u32[]{:S(2)}) async-start(bf16[64,144,128]{2,1,0:T(8,128)(2,1)} %dispatch.1), calls=%async_computation | async-start | bytes 4718592 | tf_op jit(solution)/shard_map/all_to_all | solution.py:561
  16.7 5.1 %copy.26 = bf16[1,64,18,2048]{3,2,1,0:T(8,128)(2,1)S(1)} copy(bf16[1,64,18,2048]{3,1,2,0:T(8,128)(2,1)} %param.17) | data formatting | bytes 9437184 | tf_op args[3]
  23.0 2.3 %slice.8 = bf16[64,16,2048]{2,1,0:T(8,128)(2,1)} slice(bf16[64,18,2048]{2,1,0:T(8,128)(2,1)S(1)} %bitcast.36), slice={[0:64], [0:16], [0:2048]} | slice | bytes 8388608 | tf_op jit(solution)/shard_map/slice | solution.py:565
  25.3 2.0 %reshape.31 = bf16[128,2048]{1,0:T(8,128)(2,1)} reshape(bf16[64,2,2048]{2,1,0:T(2,128)(2,1)} %slice.9) | data formatting | bytes 1048576 | tf_op jit(solution)/shard_map/reshape | solution.py:565
  27.4 1.9 %mixer_forward.1 = (f32[224,512]{1,0:T(8,128)S(1)}, bf16[224,512]{1,0:T(8,128)(2,1)S(1)}, f32[224,8]{1,0:T(8,128)S(1)}) custom-call(bf16[224,512]{1,0:T(8,128)(2,1)S(1)} %copy-done.35, bf16[224,256]{1,0:T(8,128)(2,1)S(1)} %copy-done.37, bf16[224,256]{1,0:T(8,128)(2,1)S(1)} %copy-done.17, f32[8,224]{1,0:T(8,128)S(1)} %copy-done.22, ...), custom_call_target="tpu_custom_call" | custom-call | flops 1000000000 | bytes 1000000 | tf_op jit(solution)/shard_map/mixer_forward/pallas_call | solution.py:172
  31.4 4.9 %fusion.1 = f32[1152,512]{1,0:T(8,128)S(1)} fusion(bf16[1,2048,512]{2,1,0:T(8,128)(2,1)S(1)} %copy-done.23, bf16[128,2048]{1,0:T(8,128)(2,1)S(1)} %copy-done.44, bf16[1024,2048]{1,0:T(8,128)(2,1)} %bitcast.37), kind=kOutput, calls=%fused_computation.9 | convolution fusion | flops 2425356288 | bytes 9175040 | tf_op jit(solution)/shard_map/dot_general | solution.py:568
  36.4 2.6 %pad_maximum_fusion = bf16[1152,2048]{1,0:T(8,128)(2,1)} fusion(bf16[128,2048]{1,0:T(8,128)(2,1)S(1)} %copy-done.44, bf16[1024,2048]{1,0:T(8,128)(2,1)S(1)} %bitcast.38), kind=kLoop, calls=%fused_computation.1 | loop fusion | flops 9437184 | bytes 9437184 | tf_op jit(solution)/shard_map/concatenate | solution.py:564
  38.9 5.5 %add_multiply_fusion = (f32[1152,512]{1,0:T(8,128)}, bf16[1152,512]{1,0:T(8,128)(2,1)S(1)}, f32[1152,512]{1,0:T(8,128)}) fusion(f32[1152,512]{1,0:T(8,128)S(1)} %fusion.1, bf16[1,2048,512]{2,1,0:T(8,128)(2,1)S(1)} %copy-done.25, bf16[128,2048]{1,0:T(8,128)(2,1)S(1)} %copy-done.44, bf16[1024,2048]{1,0:T(8,128)(2,1)S(1)} %bitcast.39), kind=kOutput, calls=%fused_computation.5 | convolution fusion | flops 2431844352 | bytes 15073280 | tf_op jit(solution)/shard_map/dot_general | solution.py:567
  44.4 5.1 %all-to-all-done.mine_ref = bf16[64,144,128]{2,1,0:T(8,128)(2,1)S(1)} async-done(((bf16[64,144,128]{2,1,0:T(8,128)(2,1)}), bf16[64,144,128]{2,1,0:T(8,128)(2,1)S(1)}, u32[]{:S(2)}, u32[]{:S(2)}) %all-to-all-start) | async-done | bytes 2359328 | tf_op jit(solution)/shard_map/all_to_all | solution.py:561
  51.3 2.0 %hidden_first.1 = (bf16[1152,1024]{1,0:T(8,128)(2,1)S(1)}, f32[1152,512]{1,0:T(8,128)S(1)}) custom-call(s32[1]{0:T(128)} %bitcast.tp_ref.half_ref, bf16[64,144,128]{2,1,0:T(8,128)(2,1)S(1)} %all-to-all-done.mine_ref, bf16[512,2048]{1,0:T(8,128)(2,1)S(1)} %bitcast.24), custom_call_target="tpu_custom_call" | custom-call | flops 2000000000 | bytes 10000000 | tf_op jit(solution)/shard_map/hidden_first/pallas_call | solution.py:172
  54.7 2.3 %hidden_second.1 = (bf16[1152,1024]{1,0:T(8,128)(2,1)S(1)}, bf16[1152,512]{1,0:T(8,128)(2,1)S(1)}, bf16[1152,512]{1,0:T(8,128)(2,1)S(1)}) custom-call(s32[1]{0:T(128)} %bitcast.tp_ref.half_ref, bf16[64,144,128]{2,1,0:T(8,128)(2,1)S(1)} %collective-permute-done.other_ref, bf16[512,2048]{1,0:T(8,128)(2,1)S(1)} %bitcast.25, ...), custom_call_target="tpu_custom_call" | custom-call | flops 2000000000 | bytes 10000000 | tf_op jit(solution)/shard_map/hidden_second/pallas_call | solution.py:172
  57.1 3.6 %span_half.3 = bf16[64,144,128]{2,1,0:T(8,128)(2,1)S(1)} custom-call(s32[1]{0:T(128)} %bitcast.tp_ref.half_ref, bf16[1152,512]{1,0:T(8,128)(2,1)S(1)} %get-tuple-element.66.gg_ref, bf16[1152,512]{1,0:T(8,128)(2,1)S(1)} %get-tuple-element.67.ug_ref, bf16[2048,512]{1,0:T(8,128)(2,1)S(1)} %bitcast.28, bf16[2048,512]{1,0:T(8,128)(2,1)S(1)} %bitcast.26), custom_call_target="tpu_custom_call" | custom-call | flops 4000000000 | bytes 10000000 | tf_op jit(solution)/shard_map/span_half/pallas_call | solution.py:172
  61.4 3.6 %span_half.2 = bf16[64,144,128]{2,1,0:T(8,128)(2,1)S(1)} custom-call(s32[1]{0:T(128)} %bitcast.tp_ref.half_ref, bf16[1152,512]{1,0:T(8,128)(2,1)S(1)} %get-tuple-element.66.gg_ref, bf16[1152,512]{1,0:T(8,128)(2,1)S(1)} %get-tuple-element.67.ug_ref, bf16[2048,512]{1,0:T(8,128)(2,1)S(1)} %bitcast.29, bf16[2048,512]{1,0:T(8,128)(2,1)S(1)} %bitcast.27), custom_call_target="tpu_custom_call" | custom-call | flops 4000000000 | bytes 10000000 | tf_op jit(solution)/shard_map/span_half/pallas_call | solution.py:172
  65.5 2.1 %add_convert_fusion = bf16[64,144,128]{2,1,0:T(8,128)(2,1)} fusion(bf16[64,144,128]{2,1,0:T(8,128)(2,1)S(1)} %collective-permute-done.1, bf16[64,144,128]{2,1,0:T(8,128)(2,1)S(1)} %span_half.2), kind=kLoop, calls=%fused_computation.2 | loop fusion | flops 4718592 | bytes 7077888 | tf_op jit(solution)/shard_map/convert_element_type | solution.py:589
  67.6 6.5 %all-to-all-start.1 = ((bf16[64,144,128]{2,1,0:T(8,128)(2,1)}), bf16[64,144,128]{2,1,0:T(8,128)(2,1)S(1)}, u32[]{:S(2)}, u32[]{:S(2)}) async-start(bf16[64,144,128]{2,1,0:T(8,128)(2,1)} %add_convert_fusion), calls=%async_computation.1 | async-start | bytes 4718592 | tf_op jit(solution)/shard_map/all_to_all | solution.py:590
  74.1 1.7 copy-done.2
  75.8 1.7 copy-done.4
  77.5 4.4 %down_grad.1 = bf16[512,2048]{1,0:T(8,128)(2,1)} custom-call(s32[1]{0:T(128)} %bitcast.tp_ref.half_ref, bf16[1152,512]{1,0:T(8,128)(2,1)S(1)} %get-tuple-element.62.act_ref, bf16[1152,1024]{1,0:T(8,128)(2,1)S(1)} %copy-done.2, bf16[1152,1024]{1,0:T(8,128)(2,1)S(1)} %copy-done.4), custom_call_target="tpu_custom_call" | custom-call | flops 2000000000 | bytes 10000000 | tf_op jit(solution)/shard_map/down_grad/pallas_call | solution.py:172
  81.8 6.6 %convolution_convert_fusion.1 = bf16[2048,512]{1,0:T(8,128)(2,1)} fusion(bf16[1152,2048]{1,0:T(8,128)(2,1)} %pad_maximum_fusion, bf16[1152,512]{1,0:T(8,128)(2,1)S(1)} %copy-done.30), kind=kOutput, calls=%fused_computation.4 | convolution fusion | flops 2416967680 | bytes 7995392 | tf_op jit(solution)/shard_map/dot_general | solution.py:43
  88.5 4.1 %convolution_convert_fusion = bf16[2048,512]{1,0:T(8,128)(2,1)} fusion(bf16[1152,2048]{1,0:T(8,128)(2,1)S(1)} %bitcast.41, bf16[1152,512]{1,0:T(8,128)(2,1)S(1)} %copy-done.28), kind=kOutput, calls=%fused_computation.3 | convolution fusion | flops 2416967680 | bytes 7995392 | tf_op jit(solution)/shard_map/dot_general | solution.py:43
  92.6 15.2 %all-to-all-done.1.ret_ref = bf16[64,144,128]{2,1,0:T(8,128)(2,1)S(1)} async-done(((bf16[64,144,128]{2,1,0:T(8,128)(2,1)}), bf16[64,144,128]{2,1,0:T(8,128)(2,1)S(1)}, u32[]{:S(2)}, u32[]{:S(2)}) %all-to-all-start.1) | async-done | bytes 2359328 | tf_op jit(solution)/shard_map/all_to_all | solution.py:590
  108.8 2.9 %combine.1.mine_ref = bf16[224,1024]{1,0:T(8,128)(2,1)S(1)} custom-call(s32[1]{0:T(128)} %bitcast.tp_ref.half_ref, f32[224,8]{1,0:T(8,128)S(1)} %copy-done.21, bf16[64,144,128]{2,1,0:T(8,128)(2,1)S(1)} %all-to-all-done.1.ret_ref, bf16[224,2048]{1,0:T(8,128)(2,1)S(1)} %copy-done.9), custom_call_target="tpu_custom_call" | custom-call | flops 1000000000 | bytes 3000000 | tf_op jit(solution)/shard_map/combine/pallas_call | solution.py:172
  111.7 1.8 collective-permute-done.2.other_ref
  113.6 4.4 %mixer_cotangent.1 = (bf16[224,2048]{1,0:T(8,128)(2,1)}, f32[224,512]{1,0:T(8,128)S(1)}, bf16[224,512]{1,0:T(8,128)(2,1)}, bf16[64,144,128]{2,1,0:T(8,128)(2,1)S(1)}) custom-call(s32[1]{0:T(128)} %bitcast.tp_ref.half_ref, bf16[224,1024]{1,0:T(8,128)(2,1)S(1)} %combine.1.mine_ref, bf16[224,1024]{1,0:T(8,128)(2,1)S(1)} %collective-permute-done.2.other_ref, ...), custom_call_target="tpu_custom_call" | custom-call | flops 1000000000 | bytes 5000000 | tf_op jit(solution)/shard_map/mixer_cotangent/pallas_call | solution.py:172
  120.2 5.6 %all-to-all-start.2 = ((bf16[64,144,128]{2,1,0:T(8,128)(2,1)}), bf16[64,144,128]{2,1,0:T(8,128)(2,1)S(1)}, u32[]{:S(2)}, u32[]{:S(2)}) async-start(bf16[64,144,128]{2,1,0:T(8,128)(2,1)} %copy-done), calls=%async_computation.2 | async-start | bytes 4718592 | tf_op jit(solution)/shard_map/all_to_all | solution.py:626
  127.8 4.5 %mixer_backward.1 = (f32[224,512]{1,0:T(8,128)S(1)}, f32[224,256]{1,0:T(8,128)S(1)}, bf16[224,256]{1,0:T(8,128)(2,1)}, f32[224,8]{1,0:T(8,128)S(1)}) custom-call(bf16[224,512]{1,0:T(8,128)(2,1)S(1)} %copy-done.36, bf16[224,256]{1,0:T(8,128)(2,1)S(1)} %copy-done.38, bf16[224,256]{1,0:T(8,128)(2,1)S(1)} %copy-done.19, f32[8,224]{1,0:T(8,128)S(1)} %copy-done.22, ...), custom_call_target="tpu_custom_call" | custom-call | flops 2000000000 | bytes 1000000 | tf_op jit(solution)/shard_map/mixer_backward/pallas_call | solution.py:172
  134.3 24.8 %all-to-all-done.2.in_ref = bf16[64,144,128]{2,1,0:T(8,128)(2,1)S(1)} async-done(((bf16[64,144,128]{2,1,0:T(8,128)(2,1)}), bf16[64,144,128]{2,1,0:T(8,128)(2,1)S(1)}, u32[]{:S(2)}, u32[]{:S(2)}) %all-to-all-start.2) | async-done | bytes 2359328 | tf_op jit(solution)/shard_map/all_to_all | solution.py:626
  159.1 1.9 %state_chain.1 = bf16[64,8,128]{2,1,0:T(8,128)(2,1)} custom-call(bf16[64,144,128]{2,1,0:T(8,128)(2,1)S(1)} %all-to-all-done.2.in_ref), custom_call_target="tpu_custom_call" | custom-call | flops 100000000 | bytes 1000000 | tf_op jit(solution)/shard_map/state_chain/pallas_call | solution.py:172
  161.0 5.9 %all-to-all-start.3 = ((bf16[64,8,128]{2,1,0:T(8,128)(2,1)}), bf16[64,8,128]{2,1,0:T(8,128)(2,1)S(1)}, u32[]{:S(2)}, u32[]{:S(2)}) async-start(bf16[64,8,128]{2,1,0:T(8,128)(2,1)} %state_chain.1), calls=%async_computation.3 | async-start | bytes 262144 | tf_op jit(solution)/shard_map/all_to_all | solution.py:651
  167.9 9.0 %all-to-all-done.3.state_far = bf16[64,8,128]{2,1,0:T(8,128)(2,1)S(1)} async-done(((bf16[64,8,128]{2,1,0:T(8,128)(2,1)}), bf16[64,8,128]{2,1,0:T(8,128)(2,1)S(1)}, u32[]{:S(2)}, u32[]{:S(2)}) %all-to-all-start.3) | async-done | bytes 131104 | tf_op jit(solution)/shard_map/all_to_all | solution.py:651
  177.5 4.3 %mixer_ending.1 = (bf16[224,512]{1,0:T(8,128)(2,1)}, bf16[224,256]{1,0:T(8,128)(2,1)}, f32[8,224]{1,0:T(8,128)}) custom-call(bf16[64,8,128]{2,1,0:T(8,128)(2,1)} %copy-done.45, bf16[224,512]{1,0:T(8,128)(2,1)} %v_far.1, bf16[224,256]{1,0:T(8,128)(2,1)} %k_far.1, f32[8,224]{1,0:T(8,128)} %decay_far.1, f32[8,64,128]{2,1,0:T(8,128)} %bitcast.30, ...), custom_call_target="tpu_custom_call" | custom-call | flops 1000000000 | bytes 1000000 | tf_op jit(solution)/shard_map/mixer_ending/pallas_call | solution.py:172
  (102 shorter events, 16.4 us)
Async XLA Ops:
  5.0 44.5 %all-to-all-start = ((bf16[64,144,128]{2,1,0:T(8,128)(2,1)}), bf16[64,144,128]{2,1,0:T(8,128)(2,1)S(1)}, u32[]{:S(2)}, u32[]{:S(2)}) async-start(bf16[64,144,128]{2,1,0:T(8,128)(2,1)} %dispatch.1), calls=%async_computation | async-start | bytes 4718592 | tf_op jit(solution)/shard_map/all_to_all | solution.py:561
  22.9 4.4 %copy-start.13 = (bf16[224,512]{1,0:T(8,128)(2,1)S(1)}, bf16[224,512]{1,0:T(8,128)(2,1)}, u32[]{:S(2)}) copy-start(bf16[224,512]{1,0:T(8,128)(2,1)} %gate_ref.3) | copy-start | bytes 688132
  23.0 4.4 %copy-start.17 = (bf16[224,256]{1,0:T(8,128)(2,1)S(1)}, bf16[224,256]{1,0:T(8,128)(2,1)}, u32[]{:S(2)}) copy-start(bf16[224,256]{1,0:T(8,128)(2,1)} %q_ref.5) | copy-start | bytes 344068
  23.0 4.4 %copy-start.22 = (f32[8,224]{1,0:T(8,128)S(1)}, f32[8,224]{1,0:T(8,128)}, u32[]{:S(2)}) copy-start(f32[8,224]{1,0:T(8,128)} %decay_far.1) | copy-start | bytes 21508
  23.0 4.4 %copy-start.33 = (f32[1,8,64,128]{3,2,1,0:T(8,128)S(1)}, f32[1,8,64,128]{3,2,1,0:T(8,128)}, u32[]{:S(2)}) copy-start(f32[1,8,64,128]{3,2,1,0:T(8,128)} %param.26) | copy-start | bytes 786436
  23.0 4.4 %copy-start.35 = (bf16[224,512]{1,0:T(8,128)(2,1)S(1)}, bf16[224,512]{1,0:T(8,128)(2,1)}, u32[]{:S(2)}) copy-start(bf16[224,512]{1,0:T(8,128)(2,1)} %v_far.1) | copy-start | bytes 688132
  23.0 4.4 %copy-start.37 = (bf16[224,256]{1,0:T(8,128)(2,1)S(1)}, bf16[224,256]{1,0:T(8,128)(2,1)}, u32[]{:S(2)}) copy-start(bf16[224,256]{1,0:T(8,128)(2,1)} %k_far.1) | copy-start | bytes 344068
  23.0 4.4 %copy-start.39 = (s32[224,2]{0,1:T(2,128)S(1)}, s32[224,2]{0,1:T(2,128)}, u32[]{:S(2)}) copy-start(s32[224,2]{0,1:T(2,128)} %param.15) | copy-start | bytes 5380
  27.3 4.1 %copy-start.44 = (bf16[128,2048]{1,0:T(8,128)(2,1)S(1)}, bf16[128,2048]{1,0:T(8,128)(2,1)}, u32[]{:S(2)}) copy-start(bf16[128,2048]{1,0:T(8,128)(2,1)} %reshape.31) | copy-start | bytes 1572868
  31.4 5.0 %copy-start.43 = (bf16[64,16,2048]{2,1,0:T(8,128)(2,1)S(1)}, bf16[64,16,2048]{2,1,0:T(8,128)(2,1)}, u32[]{:S(2)}) copy-start(bf16[64,16,2048]{2,1,0:T(8,128)(2,1)} %slice.8) | copy-start | bytes 12582916
  49.5 5.2 %collective-permute-start = (bf16[64,144,128]{2,1,0:T(8,128)(2,1)S(1)}, bf16[64,144,128]{2,1,0:T(8,128)(2,1)S(1)}, u32[]{:S(2)}, u32[]{:S(2)}) collective-permute-start(bf16[64,144,128]{2,1,0:T(8,128)(2,1)S(1)} %all-to-all-done.mine_ref), channel_id=1, source_target_pairs={{0,1},{1,0},{2,3},{3,2},{4,5},{5,4},{6,7},{7,6},{8,9},{9,8},{10,11... | collective-permute-start | bytes 7077896 | tf_op jit(solution)/shard_map/ppermute | solution.py:558
  57.1 4.3 %copy-start.27 = (bf16[1152,512]{1,0:T(8,128)(2,1)}, bf16[1152,512]{1,0:T(8,128)(2,1)S(1)}, u32[]{:S(2)}) copy-start(bf16[1152,512]{1,0:T(8,128)(2,1)S(1)} %get-tuple-element.67.ug_ref) | copy-start | bytes 3538948
  57.1 4.3 %copy-start.29 = (bf16[1152,512]{1,0:T(8,128)(2,1)}, bf16[1152,512]{1,0:T(8,128)(2,1)S(1)}, u32[]{:S(2)}) copy-start(bf16[1152,512]{1,0:T(8,128)(2,1)S(1)} %get-tuple-element.66.gg_ref) | copy-start | bytes 3538948
  60.8 4.7 %collective-permute-start.1 = (bf16[64,144,128]{2,1,0:T(8,128)(2,1)S(1)}, bf16[64,144,128]{2,1,0:T(8,128)(2,1)S(1)}, u32[]{:S(2)}, u32[]{:S(2)}) collective-permute-start(bf16[64,144,128]{2,1,0:T(8,128)(2,1)S(1)} %span_half.3), channel_id=1, source_target_pairs={{0,1},{1,0},{2,3},{3,2},{4,5},{5,4},{6,7},{7,6},{8,9},{9,8},{10,11... | collective-permute-start | bytes 7077896 | tf_op jit(solution)/shard_map/ppermute | solution.py:558
  67.6 40.3 %all-to-all-start.1 = ((bf16[64,144,128]{2,1,0:T(8,128)(2,1)}), bf16[64,144,128]{2,1,0:T(8,128)(2,1)S(1)}, u32[]{:S(2)}, u32[]{:S(2)}) async-start(bf16[64,144,128]{2,1,0:T(8,128)(2,1)} %add_convert_fusion), calls=%async_computation.1 | async-start | bytes 4718592 | tf_op jit(solution)/shard_map/all_to_all | solution.py:590
  77.5 4.4 %copy-start.30 = (bf16[1152,512]{1,0:T(8,128)(2,1)S(1)}, bf16[1152,512]{1,0:T(8,128)(2,1)}, u32[]{:S(2)}) copy-start(bf16[1152,512]{1,0:T(8,128)(2,1)} %copy-done.29) | copy-start | bytes 3538948
  77.5 11.0 %slice-start = ((s8[4718592]{0:T(1024)(128)(4,1)}), s8[4194304]{0:T(1024)(128)(4,1)S(1)}, s32[]{:S(2)}) async-start(s8[4718592]{0:T(1024)(128)(4,1)} %bitcast.40), calls=%async_computation.4 | async-start | bytes 8388608
  81.8 6.6 %copy-start.28 = (bf16[1152,512]{1,0:T(8,128)(2,1)S(1)}, bf16[1152,512]{1,0:T(8,128)(2,1)}, u32[]{:S(2)}) copy-start(bf16[1152,512]{1,0:T(8,128)(2,1)} %copy-done.27) | copy-start | bytes 3538948
  81.8 6.6 %slice-start.1 = ((s8[4718592]{0:T(1024)(128)(4,1)}), s8[524288]{0:T(1024)(128)(4,1)S(1)}, s32[]{:S(2)}) async-start(s8[4718592]{0:T(1024)(128)(4,1)} %bitcast.40), calls=%async_computation.5 | async-start | bytes 1048576
  88.5 19.3 %copy-start.9 = (bf16[224,2048]{1,0:T(8,128)(2,1)S(1)}, bf16[224,2048]{1,0:T(8,128)(2,1)}, u32[]{:S(2)}) copy-start(bf16[224,2048]{1,0:T(8,128)(2,1)} %og_ref.1) | copy-start | bytes 2752516
  92.6 20.9 %copy-start.14 = (bf16[224,512]{1,0:T(8,128)(2,1)S(1)}, bf16[224,512]{1,0:T(8,128)(2,1)}, u32[]{:S(2)}) copy-start(bf16[224,512]{1,0:T(8,128)(2,1)} %gate_ref.3) | copy-start | bytes 688132
  108.7 4.8 %copy-start.7 = (bf16[2048,512]{1,0:T(8,128)(2,1)S(1)}, bf16[2048,512]{1,0:T(8,128)(2,1)}, u32[]{:S(2)}) copy-start(bf16[2048,512]{1,0:T(8,128)(2,1)} %ow_ref.1) | copy-start | bytes 6291460
  108.7 4.8 %copy-start.11 = (f32[224,512]{1,0:T(8,128)S(1)}, f32[224,512]{1,0:T(8,128)}, u32[]{:S(2)}) copy-start(f32[224,512]{1,0:T(8,128)} %copy-done.10) | copy-start | bytes 1376260
  108.7 4.8 %copy-start.16 = (bf16[224,512]{1,0:T(8,128)(2,1)S(1)}, bf16[224,512]{1,0:T(8,128)(2,1)}, u32[]{:S(2)}) copy-start(bf16[224,512]{1,0:T(8,128)(2,1)} %copy-done.15) | copy-start | bytes 688132
  108.8 4.8 %copy-start.18 = (bf16[224,256]{1,0:T(8,128)(2,1)S(1)}, bf16[224,256]{1,0:T(8,128)(2,1)}, u32[]{:S(2)}) copy-start(bf16[224,256]{1,0:T(8,128)(2,1)} %q_ref.5) | copy-start | bytes 344068
  111.6 1.9 %collective-permute-start.2 = (bf16[224,1024]{1,0:T(8,128)(2,1)S(1)}, bf16[224,1024]{1,0:T(8,128)(2,1)S(1)}, u32[]{:S(2)}, u32[]{:S(2)}) collective-permute-start(bf16[224,1024]{1,0:T(8,128)(2,1)S(1)} %combine.1.mine_ref), channel_id=1, source_target_pairs={{0,1},{1,0},{2,3},{3,2},{4,5},{5,4},{6,7},{7,6},{8,9},{9,8},{10,11... | collective-permute-start | bytes 1376264 | tf_op jit(solution)/shard_map/ppermute | solution.py:558
  120.2 5.7 %copy-start.12 = (f32[224,512]{1,0:T(8,128)S(1)}, f32[224,512]{1,0:T(8,128)}, u32[]{:S(2)}) copy-start(f32[224,512]{1,0:T(8,128)} %copy-done.10) | copy-start | bytes 1376260
  120.2 5.7 %copy-start.19 = (bf16[224,256]{1,0:T(8,128)(2,1)S(1)}, bf16[224,256]{1,0:T(8,128)(2,1)}, u32[]{:S(2)}) copy-start(bf16[224,256]{1,0:T(8,128)(2,1)} %q_ref.5) | copy-start | bytes 344068
  120.2 5.7 %copy-start.32 = (f32[224,512]{1,0:T(8,128)S(1)}, f32[224,512]{1,0:T(8,128)}, u32[]{:S(2)}) copy-start(f32[224,512]{1,0:T(8,128)} %copy-done.31) | copy-start | bytes 1376260
  120.2 5.7 %copy-start.38 = (bf16[224,256]{1,0:T(8,128)(2,1)S(1)}, bf16[224,256]{1,0:T(8,128)(2,1)}, u32[]{:S(2)}) copy-start(bf16[224,256]{1,0:T(8,128)(2,1)} %k_far.1) | copy-start | bytes 344068
  120.2 38.9 %all-to-all-start.2 = ((bf16[64,144,128]{2,1,0:T(8,128)(2,1)}), bf16[64,144,128]{2,1,0:T(8,128)(2,1)S(1)}, u32[]{:S(2)}, u32[]{:S(2)}) async-start(bf16[64,144,128]{2,1,0:T(8,128)(2,1)} %copy-done), calls=%async_computation.2 | async-start | bytes 4718592 | tf_op jit(solution)/shard_map/all_to_all | solution.py:626
  161.0 15.8 %all-to-all-start.3 = ((bf16[64,8,128]{2,1,0:T(8,128)(2,1)}), bf16[64,8,128]{2,1,0:T(8,128)(2,1)S(1)}, u32[]{:S(2)}, u32[]{:S(2)}) async-start(bf16[64,8,128]{2,1,0:T(8,128)(2,1)} %state_chain.1), calls=%async_computation.3 | async-start | bytes 262144 | tf_op jit(solution)/shard_map/all_to_all | solution.py:651
  (23 other events, 38.1 us)
where the time goes:
time: 186 us; the launch traced here: 182 us
  waiting for transfers between devices  56.3 us (30%)
  Pallas kernels  41.1 us (22%)
  starting transfers between devices  30.6 us (16%)
  local copies, waits for them, and re-layouts  26.8 us (14%)
  matrix products  21.2 us (11%)
  other arithmetic  4.64 us (2%)
    pallas_call x13, Pallas kernels, call(): pl.pallas_call(kernel, out_shape=outs, in_specs=in_specs, out_specs=[far...  41.1 us
    all_to_all x1, waiting for transfers between devices, per_device(): lax.all_to_all(tail_message, SP, split_axis=0, concat_axis=0, tiled=True)  24.8 us
    unnamed x97, local copies, waits for them, and re-layouts  21.3 us
    all_to_all x1, waiting for transfers between devices, per_device(): returned = lax.all_to_all(back, SP, split_axis=0, concat_axis=0, tiled=True)  15.2 us
    all_to_all x1, starting transfers between devices, per_device(): moved = lax.all_to_all(message, SP, split_axis=0, concat_axis=0, tiled=True)  11.7 us
    dot_general x2, matrix products, dot(): return lax.dot_general(a, b, dims, preferred_element_type=F32)  10.7 us
    all_to_all x1, waiting for transfers between devices, per_device(): states = lax.all_to_all(states, SP, split_axis=0, concat_axis=0, tiled=True)  8.99 us
    all_to_all x1, starting transfers between devices, per_device(): returned = lax.all_to_all(back, SP, split_axis=0, concat_axis=0, tiled=True)  6.54 us
  transfers between devices with their start and end apart: 7, of which 6 were waited for; matrix products, arithmetic and copies ran while one was open for 19% of the time, Pallas kernels for 9%

commit v1 on v0

--- a/solution.py
+++ b/solution.py
@@ -162,6 +162,7 @@
     limit=8,
     hbm_outs=(),
     hbm_ins=(),
+    aliases=None,
 ):
     vmem = pl.BlockSpec(memory_space=pltpu.VMEM)
     far = pl.BlockSpec(memory_space=pltpu.HBM)
@@ -175,6 +176,7 @@
         in_specs=in_specs,
         out_specs=[far if i in hbm_outs else vmem for i in range(len(outs))],
         scratch_shapes=list(scratch),
+        input_output_aliases=aliases or {},
         compiler_params=pltpu.CompilerParams(vmem_limit_bytes=limit * 1024 * 1024),
         cost_estimate=cost(flops, nbytes),
         name=name,
@@ -215,7 +217,6 @@
 
 
 def combine_kernel(tp_ref, meta_ref, ret_ref, og_ref, out_ref):
-    own = og_ref[:, half_of(tp_ref)].astype(F32)
     meta = meta_ref[...].astype(jnp.int32)
     e0, s0, e1, s1 = (meta[:, k : k + 1] for k in range(4))
     m0 = jnp.where(s0 < MAIN, e0 * MAIN + s0, -1)
@@ -226,12 +227,14 @@
     pick = jnp.where((lanes == m0) | (lanes == m1), 1.0, 0.0).astype(BF)
     tail = ret_ref[:, 16 * COLS : MSG, :].reshape(1024, 128)
     d0, d1 = lanes - t0, lanes - t1
-    for c in range(COLS):
-        main = ret_ref[:, 16 * c : 16 * c + 16, :].reshape(1024, 128)
-        tpick = jnp.where((d0 == c) | (d1 == c), 1.0, 0.0).astype(BF)
-        moe = dot(pick, main) + dot(tpick, tail)
-        cols = slice(128 * c, 128 * c + 128)
-        out_ref[:, cols] = (own[:, cols] + moe).astype(BF)
+
+    for c in range(0, COLS, 2):
+        pair = [ret_ref[:, 16 * k : 16 * k + 16, :].reshape(1024, 128) for k in (c, c + 1)]
+        moe = dot(pick, jnp.concatenate(pair, axis=1))
+        masks = [jnp.where((d0 == k) | (d1 == k), 1.0, 0.0).astype(BF) for k in (c, c + 1)]
+        moe = moe + jnp.concatenate([dot(m, tail) for m in masks], axis=1)
+        own = og_ref[:, pl.ds(pl.multiple_of(tp_ref[0] * HALF + c * 128, 256), 256)]
+        out_ref[:, 128 * c : 128 * c + 256] = (own.astype(F32) + moe).astype(BF)
 
 
 def combine_rows(tp, meta, returned, out_grad):
@@ -257,6 +260,31 @@
         arr_ref[1024:1152, 128 * c : 128 * c + 128] = dot(mask, tail).astype(BF)
 
 
+def order_kernel(in_ref, out_ref):
+    i, j = iota((256, 256), 0), iota((256, 256), 1)
+    turn = jnp.where((i // 16 == j % 16) & (i % 16 == j // 16), 1.0, 0.0).astype(BF)
+    for b in range(4):
+        x = in_ref[0:MAIN, 16 * b : 16 * b + 16, :].reshape(256, -1)
+        out_ref[256 * b : 256 * b + 256, :] = dot(turn, x).astype(BF)
+    i, j = iota((128, 128), 0), iota((128, 128), 1)
+    turn = jnp.where((i // 2 == j % 64) & (i % 2 == j // 64), 1.0, 0.0).astype(BF)
+    x = in_ref[MAIN:CAP, :, :].reshape(128, -1)
+    out_ref[1024:1152, :] = dot(turn, x).astype(BF)
+
+
+def ordered_rows(rows):
+    width = rows.shape[-1]
+    return call(
+        order_kernel,
+        [sds((PEERS * CAP, width), BF)],
+        (jnp.transpose(rows, (1, 0, 2)),),
+        10**9,
+        10**7,
+        limit=16,
+        name="ordered_rows",
+    )[0]
+
+
 def first_half_kernel(tp_ref, mine_ref, down_ref, arr_ref, part_ref):
     place_rows(mine_ref, arr_ref)
     part_ref[...] = dot(arr_ref[...], down_ref[:, half_of(tp_ref)], NT)
@@ -295,12 +323,15 @@
 
 
 def down_kernel(tp_ref, act_ref, own_ref, other_ref, out_ref):
-    for n in range(4):
-        cols = slice(256 * n, 256 * n + 256)
+    def step(n, carry):
+        cols = pl.ds(pl.multiple_of(256 * n, 256), 256)
         for other, ref in ((False, own_ref), (True, other_ref)):
             half = 1 - tp_ref[0] if other else tp_ref[0]
             to = pl.ds(pl.multiple_of(half * HALF + 256 * n, 256), 256)
             out_ref[:, to] = dot(act_ref[...], ref[:, cols], TN).astype(BF)
+        return carry
+
+    lax.fori_loop(0, 4, step, 0)
 
 
 def down_grad(tp, act, arrived):
@@ -317,15 +348,24 @@
 
 def span_kernel(other, half_ref, gg_ref, ug_ref, gw_ref, uw_ref, out_ref, tail_ref):
     base = (1 - half_ref[0] if other else half_ref[0]) * HALF
-    for n in range(4):
+
+    def block(n):
         cols = pl.ds(pl.multiple_of(base + 256 * n, 256), 256)
         d = dot(gg_ref[...], gw_ref[cols, :], NT) + dot(ug_ref[...], uw_ref[cols, :], NT)
         d = d.astype(BF)
         for k in range(2):
             c = 2 * n + k
             part = d[:, 128 * k : 128 * k + 128]
-            out_ref[:, 16 * c : 16 * c + 16, :] = part[:1024].reshape(PEERS, 16, 128)
-            tail_ref[:, 128 * c : 128 * c + 128] = part[1024:]
+            rows = pl.ds(pl.multiple_of(16 * c, 16), 16)
+            out_ref[:, rows, :] = part[:1024].reshape(PEERS, 16, 128)
+            tail_ref[:, pl.ds(pl.multiple_of(128 * c, 128), 128)] = part[1024:]
+
+    def step(n, carry):
+        block(2 * n)
+        block(2 * n + 1)
+        return carry
+
+    lax.fori_loop(0, 2, step, 0)
     tail = pack_tail(tail_ref[...]).astype(BF)
     out_ref[:, 16 * COLS : MSG, :] = tail.reshape(PEERS, 16, 128)
 
@@ -390,8 +430,8 @@
 
 
 def cotangent_kernel(
-    tp_ref, mine_ref, other_ref, ow_ref, core_ref, gate_ref, decay_ref, q_ref, mixed_ref,
-    hidden_ref, dcore_ref, dgate_ref, to_ref, msg_ref, sems,
+    tp_ref, mine_ref, other_ref, ow_ref, core_ref, gate_ref, decay_ref, q_ref,
+    hidden_ref, dcore_ref, dgate_ref, msg_ref,
 ):
     first = tp_ref[0] == 0
     x, y = mine_ref[...], other_ref[...]
@@ -426,61 +466,80 @@
         extra = jnp.where(row == 0, parts[0], jnp.where(row == 1, parts[1], parts[2]))
         extra = jnp.where(row < 3, extra, 0.0)
         both = jnp.concatenate([state.reshape(8, 8, 128), extra], axis=1)
-        msg_ref[8 * h : 8 * h + 8, 128:144, :] = both.astype(BF)
-    copies = []
-    for b in range(4):
-        rows = hidden_ref[:, 512 * b : 512 * b + 512]
+        msg_ref[8 * h : 8 * h + 8] = both.astype(BF)
+
+
+def shares_kernel(hidden_ref, mixed_ref, msg_ref):
+    def step(b, carry):
+        rows = hidden_ref[:, pl.ds(pl.multiple_of(512 * b, 512), 512)]
         share = dot(rows, mixed_ref[...], TN).astype(BF)
+        peers = pl.ds(pl.multiple_of(16 * b, 16), 16)
         for c in range(4):
-            msg_ref[16 * b : 16 * b + 16, 32 * c : 32 * c + 32, :] = share[
-                :, 128 * c : 128 * c + 128
-            ].reshape(16, 32, 128)
-        copies.append(copy_out(msg_ref, to_ref, sems, b))
-    for copy in copies:
-        copy.wait()
+            msg_ref[peers, 32 * c : 32 * c + 32, :] = share[:, 128 * c : 128 * c + 128].reshape(
+                16, 32, 128
+            )
+        return carry
+
+    lax.fori_loop(0, 4, step, 0)
+    msg_ref[:, 128:136, :] = jnp.zeros((PEERS, 8, 128), BF)
 
 
 def backward_kernel(
-    v_ref, k_ref, q_ref, decay_ref, e_ref, core_ref, dcore_ref, dv_ref, dk_ref, dq_ref, diff_ref
+    v_far, k_far, q_far, decay_far, e_far, core_far, dcore_far,
+    dv_far, dk_far, dq_far, diff_far,
+    v_ref, k_ref, q_ref, decay_ref, e_ref, core_ref, dcore_ref,
+    dv_ref, dk_ref, dq_ref, diff_ref, sems,
 ):
+    load(
+        (
+            (decay_far, decay_ref),
+            (q_far, q_ref),
+            (k_far, k_ref),
+            (v_far, v_ref),
+            (e_far, e_ref),
+            (dcore_far, dcore_ref),
+            (core_far, core_ref),
+        ),
+        sems,
+    )
     cum, cum_t = decay_sums(decay_ref[...])
-    for g in range(GROUPS):
-        q, k = q_ref[:, group(g)], k_ref[:, group(g)]
+    causal = iota((TOK, TOK), 0) >= iota((TOK, TOK), 1)
+    lane = iota((TOK, HEADS), 1)
+
+    def step(g, diff):
+        span = pl.ds(pl.multiple_of(g * NS, NS), NS)
+        wide = pl.ds(pl.multiple_of(g * 256, 256), 256)
+        q, k = q_ref[:, span], k_ref[:, span]
+        v4, dcore4, core4 = v_ref[:, wide], dcore_ref[:, wide], core_ref[:, wide]
         scores = dot(q, k, NT)
         ds = jnp.zeros((TOK, TOK), F32)
         dq = jnp.zeros((TOK, NS), F32)
-        for h in range(PER_GROUP * g, PER_GROUP * g + PER_GROUP):
-            w = decay_weights(cum, cum_t, h)
-            dcore = dcore_ref[:, head(h)]
+        dvs = []
+        for i in range(PER_GROUP):
+            h = g * PER_GROUP + i
+            row = jnp.sum(jnp.where(iota((HEADS, TOK), 0) == h, cum, 0.0), axis=0, keepdims=True)
+            col = jnp.sum(jnp.where(lane == h, cum_t, 0.0), axis=1, keepdims=True)
+            w = jnp.where(causal, jnp.exp(jnp.where(causal, col - row, 0.0)), 0.0)
+            dcore = dcore4[:, head(i)]
             dv = dot3(scores * w, dcore, TN)
-            dv_ref[:, head(h)] = dv
-            v = v_ref[:, head(h)].astype(F32)
-            diff_ref[:, h : h + 1] = jnp.sum(
-                dcore * core_ref[:, head(h)] - v * dv, axis=1, keepdims=True
-            )
-            ds = ds + dot2(dcore, v_ref[:, head(h)], NT) * w
-            dq = dq + dot3(dcore * jnp.exp(cum_t[:, h : h + 1]), e_ref[h])
-        dq_ref[:, group(g)] = (dq + dot2(ds, k)).astype(BF)
-        dk_ref[:, group(g)] = dot2(ds, q, TN)
+            dvs.append(dv)
+            v = v4[:, head(i)]
+            change = dcore * core4[:, head(i)] - v.astype(F32) * dv
+            diff = diff + jnp.where(lane == h, jnp.sum(change, axis=1, keepdims=True), 0.0)
+            ds = ds + dot2(dcore, v, NT) * w
+            dq = dq + dot3(dcore * jnp.exp(col), e_ref[h])
+        dv_ref[:, wide] = jnp.concatenate(dvs, axis=1)
+        dq_ref[:, span] = (dq + dot2(ds, k)).astype(BF)
+        dk_ref[:, span] = dot2(ds, q, TN)
+        return diff
+
+    diff_ref[...] = lax.fori_loop(0, GROUPS, step, jnp.zeros((TOK, HEADS), F32))
+    load(((dv_ref, dv_far), (dk_ref, dk_far), (dq_ref, dq_far), (diff_ref, diff_far)), sems)
 
 
 def ending_kernel(
-    state_far, v_far, k_far, decay_far, e_far, dv_far, dk_far, diff_far,
-    gv_ref, gk_ref, gd_ref, state_ref, v_ref, k_ref, decay_ref, e_ref, dv_ref, dk_ref, diff_ref, sems,
+    in_ref, v_ref, k_ref, decay_ref, e_ref, dv_ref, dk_ref, diff_ref, gv_ref, gk_ref, gd_ref
 ):
-    load(
-        (
-            (state_far, state_ref),
-            (decay_far, decay_ref),
-            (v_far, v_ref),
-            (k_far, k_ref),
-            (e_far, e_ref),
-            (dv_far, dv_ref),
-            (dk_far, dk_ref),
-            (diff_far, diff_ref),
-        ),
-        sems,
-    )
     cum, cum_t = decay_sums(decay_ref[...])
     last = cum_t[TOK - 1 : TOK, :]
     tail = jnp.exp(last - cum_t)
@@ -491,7 +550,7 @@
         k = k_ref[:, group(g)]
         dk = dk_ref[:, group(g)]
         for h in range(PER_GROUP * g, PER_GROUP * g + PER_GROUP):
-            state = state_ref[8 * h : 8 * h + 8].astype(F32).reshape(HD, NS)
+            state = in_ref[8 * h : 8 * h + 8, 128:136, :].astype(F32).reshape(HD, NS)
             exact = state.astype(BF)
             v = v_ref[:, head(h)].astype(F32)
             t = tail[:, h : h + 1]
@@ -511,8 +570,9 @@
     gd_ref[...] = dotp(diff, later, TN)
 
 
-def chain_kernel(in_ref, out_ref):
-    wide = in_ref[:, 128:144, :].astype(F32)
+def chain_kernel(in_ref, shares_ref, out_ref):
+    del shares_ref
+    wide = in_ref[...].astype(F32)
     states = wide[:, 0:8, :].reshape(512, 128).astype(BF)
     logs = jnp.sum(wide[:, 8:16, :], axis=1)
     segment, entry = iota((512, PEERS), 0) // 8, iota((512, PEERS), 1)
@@ -522,7 +582,7 @@
     later = (j // 8 > i // 8) & (j % 8 == i % 8)
     spread = jnp.transpose(before)[0:1, :] - through[:, 0:1]
     weights = jnp.where(later, jnp.exp(jnp.where(later, spread, 0.0)), 0.0)
-    out_ref[...] = dot2(weights, states).reshape(PEERS, 8, 128).astype(BF)
+    out_ref[:, 128:136, :] = dot2(weights, states).reshape(PEERS, 8, 128).astype(BF)
 
 
 def share_kernel(in_ref, out_ref):
@@ -560,10 +620,8 @@
     message = dispatch(tp, routes.T, route_weights.T, out_grad)
     moved = lax.all_to_all(message, SP, split_axis=0, concat_axis=0, tiled=True)
 
-    rows = routed_rows[0]
-    rows = jnp.concatenate(
-        [rows[:, :MAIN].reshape(PEERS * MAIN, -1), rows[:, MAIN:].reshape(PEERS * TAIL, -1)], axis=0
-    )
+    _, rows = lax.optimization_barrier((message, routed_rows[0]))
+    rows = ordered_rows(rows)
     gate_pre = jnp.dot(rows, gate_w, preferred_element_type=F32)
     up_pre = jnp.dot(rows, up_w, preferred_element_type=F32)
     sig = jax.nn.sigmoid(gate_pre)
@@ -598,13 +656,13 @@
     )
 
     hidden_half = combine_rows(tp, meta, returned, out_grad)
-    grad_hidden, dcore, dgate, tail_message = call(
+    grad_hidden, dcore, dgate, own_state = call(
         cotangent_kernel,
         [
             sds((TOK, 2 * HALF), BF),
             sds((TOK, FH), F32),
             sds((TOK, FH), BF),
-            sds((PEERS, 144, NS), BF),
+            sds((PEERS, 16, NS), BF),
         ],
         (
             hidden_half,
@@ -614,16 +672,13 @@
             gate_in,
             decay_log,
             query_side,
-            mixer_out,
         ),
         10**9,
         5 * 10**6,
         scalar=tp,
-        scratch=[pltpu.VMEM((PEERS, 144, NS), BF), pltpu.SemaphoreType.DMA((4,))],
-        hbm_outs=(3,),
         name="mixer_cotangent",
     )
-    gathered = lax.all_to_all(tail_message, SP, split_axis=0, concat_axis=0, tiled=True)
+    gathered = lax.all_to_all(own_state, SP, split_axis=0, concat_axis=0, tiled=True)
     dv, dk, grad_query, diff = call(
         backward_kernel,
         [
@@ -635,24 +690,53 @@
         (values, key_side, query_side, decay_log, entry, core, dcore),
         2 * 10**9,
         10**6,
+        scratch=[
+            pltpu.VMEM((TOK, HEADS * HD), BF),
+            pltpu.VMEM((TOK, GROUPS * NS), BF),
+            pltpu.VMEM((TOK, GROUPS * NS), BF),
+            pltpu.VMEM((HEADS, TOK), F32),
+            pltpu.VMEM((HEADS, HD, NS), F32),
+            pltpu.VMEM((TOK, HEADS * HD), F32),
+            pltpu.VMEM((TOK, HEADS * HD), F32),
+            pltpu.VMEM((TOK, HEADS * HD), F32),
+            pltpu.VMEM((TOK, GROUPS * NS), F32),
+            pltpu.VMEM((TOK, GROUPS * NS), BF),
+            pltpu.VMEM((TOK, HEADS), F32),
+            pltpu.SemaphoreType.DMA((7,)),
+        ],
+        hbm_ins=tuple(range(7)),
+        hbm_outs=tuple(range(4)),
+        limit=60,
         name="mixer_backward",
     )
-    gathered, dv, dk, grad_query, diff = lax.optimization_barrier(
-        (gathered, dv, dk, grad_query, diff)
-    )
-    states = call(
+    shares_hidden, dv, dk, grad_query, diff = lax.optimization_barrier(
+        (grad_hidden, dv, dk, grad_query, diff)
+    )
+    shares = call(
+        shares_kernel,
+        [sds((PEERS, 136, NS), BF)],
+        (shares_hidden, mixer_out),
+        10**9,
+        10**6,
+        name="shares",
+    )[0]
+    gathered, shares, dv, dk, grad_query, diff = lax.optimization_barrier(
+        (gathered, shares, dv, dk, grad_query, diff)
+    )
+    message = call(
         chain_kernel,
-        [sds((PEERS, 8, NS), BF)],
-        (gathered,),
+        [sds((PEERS, 136, NS), BF)],
+        (gathered, shares),
         10**8,
         10**6,
+        aliases={1: 0},
         name="state_chain",
     )[0]
-    states = lax.all_to_all(states, SP, split_axis=0, concat_axis=0, tiled=True)
+    received = lax.all_to_all(message, SP, split_axis=0, concat_axis=0, tiled=True)
     grad_out_weight = call(
         share_kernel,
         [sds((32, FH), F32)],
-        (gathered,),
+        (received,),
         10**7,
         10**6,
         name="share_sum",
@@ -664,22 +748,9 @@
             sds((TOK, GROUPS * NS), BF),
             sds((HEADS, TOK), F32),
         ],
-        (states, values, key_side, decay_log, entry, dv, dk, diff),
+        (received, values, key_side, decay_log, entry, dv, dk, diff),
         10**9,
         10**6,
-        scratch=[
-            pltpu.VMEM((PEERS, 8, NS), BF),
-            pltpu.VMEM((TOK, HEADS * HD), BF),
-            pltpu.VMEM((TOK, GROUPS * NS), BF),
-            pltpu.VMEM((HEADS, TOK), F32),
-            pltpu.VMEM((HEADS, HD, NS), F32),
-            pltpu.VMEM((TOK, HEADS * HD), F32),
-            pltpu.VMEM((TOK, GROUPS * NS), F32),
-            pltpu.VMEM((TOK, HEADS), F32),
-            pltpu.SemaphoreType.DMA((8,)),
-        ],
-        hbm_ins=tuple(range(8)),
-        limit=60,
         name="mixer_ending",
     )
     return (

time: 186 us -> 177 us (0.952); the launches traced: 182 us -> 176 us
  blocking collectives: 0 us -> 38.7 us
  waiting for transfers between devices: 56.3 us -> 37.2 us
  local copies, waits for them, and re-layouts: 26.8 us -> 12.6 us
  starting transfers between devices: 30.6 us -> 24.1 us
  matrix products: 21.2 us -> 18.4 us
  other arithmetic: 4.64 us -> 2.2 us
    all_to_all x0 -> x1, blocking collectives: none -> 38.7 us  [per_device(): lax.all_to_all(message, SP, split_axis=0, concat_axis=0, tiled=True)]
    all_to_all x2 -> x1, waiting for transfers between devices: 33.8 us -> 3.26 us  [per_device(): lax.all_to_all(own_state, SP, split_axis=0, concat_axis=0, tiled=True)]
    all_to_all x1, waiting for transfers between devices: 5.06 us -> 17.2 us  [per_device(): moved = lax.all_to_all(message, SP, split_axis=0, concat_axis=0, tiled=True)]
    unnamed x97 -> x90, local copies, waits for them, and re-layouts: 21.3 us -> 12.6 us
    all_to_all x2 -> x1, starting transfers between devices: 11.5 us -> 5.51 us  [per_device(): lax.all_to_all(own_state, SP, split_axis=0, concat_axis=0, tiled=True)]
    slice x2 -> x0, local copies, waits for them, and re-layouts: 3.46 us -> none  [the longest x1 2.29 us: per_device(): rows[:, :MAIN].reshape(PEERS * MAIN, -1)]
    concatenate x1 -> x0, other arithmetic: 2.56 us -> none  [per_device(): jnp.concatenate([rows[:, :MAIN].reshape(PEERS * MAIN, -1), rows[:, MAIN:]...]
    dot_general x1, matrix products: 4.95 us -> 2.61 us  [per_device(): up_pre = jnp.dot(rows, up_w, preferred_element_type=F32)]
  transfers between devices with their start and end apart: 7 -> 6, of which waited for: 6 -> 5; matrix products, arithmetic and copies ran while one was open for 19% -> 10% of each run, Pallas kernels for 9% -> 12%
where the time goes in v1:
time: 177 us; the launch traced here: 176 us
  Pallas kernels  41.6 us (24%)
  blocking collectives  38.7 us (22%)
  waiting for transfers between devices  37.2 us (21%)
  starting transfers between devices  24.1 us (14%)
  matrix products  18.4 us (10%)
  local copies, waits for them, and re-layouts  12.6 us (7%)
  other arithmetic  2.2 us (1%)
    pallas_call x15, Pallas kernels, call(): pl.pallas_call(kernel, out_shape=outs, in_specs=in_specs, out_specs=[far...  41.6 us
    all_to_all x1, blocking collectives, per_device(): lax.all_to_all(message, SP, split_axis=0, concat_axis=0, tiled=True)  38.7 us
    all_to_all x1, waiting for transfers between devices, per_device(): moved = lax.all_to_all(message, SP, split_axis=0, concat_axis=0, tiled=True)  17.2 us
    all_to_all x1, waiting for transfers between devices, per_device(): returned = lax.all_to_all(back, SP, split_axis=0, concat_axis=0, tiled=True)  14.4 us
    unnamed x90, local copies, waits for them, and re-layouts  12.6 us
    all_to_all x1, starting transfers between devices, per_device(): moved = lax.all_to_all(message, SP, split_axis=0, concat_axis=0, tiled=True)  11.5 us
    dot_general x2, matrix products, dot(): return lax.dot_general(a, b, dims, preferred_element_type=F32)  10.8 us
    all_to_all x1, starting transfers between devices, per_device(): returned = lax.all_to_all(back, SP, split_axis=0, concat_axis=0, tiled=True)  6.35 us
  transfers between devices with their start and end apart: 6, of which 5 were waited for; matrix products, arithmetic and copies ran while one was open for 10% of the time, Pallas kernels for 12%

profile of v1, /device:TPU:0, one launch (start us, length us, event | category | flops | bytes accessed | tf_op | source)
XLA Modules:
  0.0 175.9 jit_solution(5705050049974108384)
XLA Ops:
  0.6 4.3 %dispatch.1 = bf16[64,144,128]{2,1,0:T(8,128)(2,1)} custom-call(s32[1]{0:T(128)} %bitcast.tp_ref.half_ref, s32[2,224]{1,0:T(2,128)} %bitcast.36, f32[2,224]{1,0:T(2,128)} %bitcast.39, bf16[224,2048]{1,0:T(8,128)(2,1)} %og_ref.1), custom_call_target="tpu_custom_call" | custom-call | flops 1000000000 | bytes 3000000 | tf_op jit(solution)/shard_map/dispatch/pallas_call | solution.py:173
  5.0 11.5 %all-to-all-start = ((bf16[64,144,128]{2,1,0:T(8,128)(2,1)}), bf16[64,144,128]{2,1,0:T(8,128)(2,1)S(1)}, u32[]{:S(2)}, u32[]{:S(2)}) async-start(bf16[64,144,128]{2,1,0:T(8,128)(2,1)} %dispatch.1), calls=%async_computation | async-start | bytes 4718592 | tf_op jit(solution)/shard_map/all_to_all | solution.py:621
  16.5 2.3 %copy-done = bf16[1,64,18,2048]{3,1,2,0:T(8,128)(2,1)S(1)} copy-done((bf16[1,64,18,2048]{3,1,2,0:T(8,128)(2,1)S(1)}, bf16[1,64,18,2048]{3,1,2,0:T(8,128)(2,1)}, u32[]{:S(2)}) %copy-start) | copy-done | bytes 4718616
  18.9 1.4 ordered_rows.1
  20.4 1.9 %mixer_forward.1 = (f32[224,512]{1,0:T(8,128)S(1)}, bf16[224,512]{1,0:T(8,128)(2,1)S(1)}, f32[224,8]{1,0:T(8,128)S(1)}) custom-call(bf16[224,512]{1,0:T(8,128)(2,1)S(1)} %copy-done.33, bf16[224,256]{1,0:T(8,128)(2,1)S(1)} %copy-done.35, bf16[224,256]{1,0:T(8,128)(2,1)S(1)} %copy-done.15, f32[8,224]{1,0:T(8,128)S(1)} %copy-done.19, ...), custom_call_target="tpu_custom_call" | custom-call | flops 1000000000 | bytes 1000000 | tf_op jit(solution)/shard_map/mixer_forward/pallas_call | solution.py:173
  24.4 2.6 %fusion.1 = f32[1152,512]{1,0:T(8,128)S(1)} fusion(bf16[1152,2048]{1,0:T(8,128)(2,1)S(1)} %ordered_rows.1, bf16[1,2048,512]{2,1,0:T(8,128)(2,1)S(1)} %copy-done.21), kind=kOutput, calls=%fused_computation.7 | convolution fusion | flops 2415919104 | bytes 9175040 | tf_op jit(solution)/shard_map/dot_general | solution.py:626
  27.1 5.1 %add_multiply_fusion = (f32[1152,512]{1,0:T(8,128)}, bf16[1152,512]{1,0:T(8,128)(2,1)S(1)}, f32[1152,512]{1,0:T(8,128)}) fusion(f32[1152,512]{1,0:T(8,128)S(1)} %fusion.1, bf16[1152,2048]{1,0:T(8,128)(2,1)S(1)} %ordered_rows.1, bf16[1,2048,512]{2,1,0:T(8,128)(2,1)S(1)} %copy-done.23), kind=kOutput, calls=%fused_computation.3 | convolution fusion | flops 2422407168 | bytes 15073280 | tf_op jit(solution)/shard_map/dot_general | solution.py:625
  32.1 17.2 %all-to-all-done.mine_ref = bf16[64,144,128]{2,1,0:T(8,128)(2,1)S(1)} async-done(((bf16[64,144,128]{2,1,0:T(8,128)(2,1)}), bf16[64,144,128]{2,1,0:T(8,128)(2,1)S(1)}, u32[]{:S(2)}, u32[]{:S(2)}) %all-to-all-start) | async-done | bytes 2359328 | tf_op jit(solution)/shard_map/all_to_all | solution.py:621
  49.3 1.6 copy-done.9
  50.9 2.0 %hidden_first.1 = (bf16[1152,1024]{1,0:T(8,128)(2,1)S(1)}, f32[1152,512]{1,0:T(8,128)S(1)}) custom-call(s32[1]{0:T(128)} %bitcast.tp_ref.half_ref, bf16[64,144,128]{2,1,0:T(8,128)(2,1)S(1)} %all-to-all-done.mine_ref, bf16[512,2048]{1,0:T(8,128)(2,1)S(1)} %bitcast.27), custom_call_target="tpu_custom_call" | custom-call | flops 2000000000 | bytes 10000000 | tf_op jit(solution)/shard_map/hidden_first/pallas_call | solution.py:173
  52.9 1.4 copy-done.2
  54.4 2.3 %hidden_second.1 = (bf16[1152,1024]{1,0:T(8,128)(2,1)S(1)}, bf16[1152,512]{1,0:T(8,128)(2,1)S(1)}, bf16[1152,512]{1,0:T(8,128)(2,1)S(1)}) custom-call(s32[1]{0:T(128)} %bitcast.tp_ref.half_ref, bf16[64,144,128]{2,1,0:T(8,128)(2,1)S(1)} %collective-permute-done.other_ref, bf16[512,2048]{1,0:T(8,128)(2,1)S(1)} %bitcast.28, ...), custom_call_target="tpu_custom_call" | custom-call | flops 2000000000 | bytes 10000000 | tf_op jit(solution)/shard_map/hidden_second/pallas_call | solution.py:173
  56.8 3.7 %span_half.3 = bf16[64,144,128]{2,1,0:T(8,128)(2,1)S(1)} custom-call(s32[1]{0:T(128)} %bitcast.tp_ref.half_ref, bf16[1152,512]{1,0:T(8,128)(2,1)S(1)} %get-tuple-element.74.gg_ref, bf16[1152,512]{1,0:T(8,128)(2,1)S(1)} %get-tuple-element.75.ug_ref, bf16[2048,512]{1,0:T(8,128)(2,1)S(1)} %bitcast.31, bf16[2048,512]{1,0:T(8,128)(2,1)S(1)} %bitcast.29), custom_call_target="tpu_custom_call" | custom-call | flops 4000000000 | bytes 10000000 | tf_op jit(solution)/shard_map/span_half/pallas_call | solution.py:173
  61.0 3.7 %span_half.2 = bf16[64,144,128]{2,1,0:T(8,128)(2,1)S(1)} custom-call(s32[1]{0:T(128)} %bitcast.tp_ref.half_ref, bf16[1152,512]{1,0:T(8,128)(2,1)S(1)} %get-tuple-element.74.gg_ref, bf16[1152,512]{1,0:T(8,128)(2,1)S(1)} %get-tuple-element.75.ug_ref, bf16[2048,512]{1,0:T(8,128)(2,1)S(1)} %bitcast.32, bf16[2048,512]{1,0:T(8,128)(2,1)S(1)} %bitcast.30), custom_call_target="tpu_custom_call" | custom-call | flops 4000000000 | bytes 10000000 | tf_op jit(solution)/shard_map/span_half/pallas_call | solution.py:173
  65.2 2.2 %add_convert_fusion = bf16[64,144,128]{2,1,0:T(8,128)(2,1)} fusion(bf16[64,144,128]{2,1,0:T(8,128)(2,1)S(1)} %collective-permute-done.1, bf16[64,144,128]{2,1,0:T(8,128)(2,1)S(1)} %span_half.2), kind=kLoop, calls=%fused_computation | loop fusion | flops 4718592 | bytes 7077888 | tf_op jit(solution)/shard_map/convert_element_type | solution.py:647
  67.4 6.4 %all-to-all-start.1 = ((bf16[64,144,128]{2,1,0:T(8,128)(2,1)}), bf16[64,144,128]{2,1,0:T(8,128)(2,1)S(1)}, u32[]{:S(2)}, u32[]{:S(2)}) async-start(bf16[64,144,128]{2,1,0:T(8,128)(2,1)} %add_convert_fusion), calls=%async_computation.1 | async-start | bytes 4718592 | tf_op jit(solution)/shard_map/all_to_all | solution.py:648
  73.8 1.7 copy-done.3
  75.4 1.7 copy-done.5
  77.1 4.9 %down_grad.1 = bf16[512,2048]{1,0:T(8,128)(2,1)} custom-call(s32[1]{0:T(128)} %bitcast.tp_ref.half_ref, bf16[1152,512]{1,0:T(8,128)(2,1)S(1)} %get-tuple-element.70.act_ref, bf16[1152,1024]{1,0:T(8,128)(2,1)S(1)} %copy-done.3, bf16[1152,1024]{1,0:T(8,128)(2,1)S(1)} %copy-done.5), custom_call_target="tpu_custom_call" | custom-call | flops 2000000000 | bytes 10000000 | tf_op jit(solution)/shard_map/down_grad/pallas_call | solution.py:173
  82.0 6.6 %convolution_convert_fusion.1 = bf16[2048,512]{1,0:T(8,128)(2,1)} fusion(bf16[1152,2048]{1,0:T(8,128)(2,1)} %copy-done.1, bf16[1152,512]{1,0:T(8,128)(2,1)S(1)} %copy-done.28), kind=kOutput, calls=%fused_computation.2 | convolution fusion | flops 2416967680 | bytes 7995392 | tf_op jit(solution)/shard_map/dot_general | solution.py:43
  88.7 4.1 %convolution_convert_fusion = bf16[2048,512]{1,0:T(8,128)(2,1)} fusion(bf16[1152,2048]{1,0:T(8,128)(2,1)S(1)} %bitcast.26, bf16[1152,512]{1,0:T(8,128)(2,1)S(1)} %copy-done.26), kind=kOutput, calls=%fused_computation.1 | convolution fusion | flops 2416967680 | bytes 7995392 | tf_op jit(solution)/shard_map/dot_general | solution.py:43
  92.8 14.4 %all-to-all-done.1.ret_ref = bf16[64,144,128]{2,1,0:T(8,128)(2,1)S(1)} async-done(((bf16[64,144,128]{2,1,0:T(8,128)(2,1)}), bf16[64,144,128]{2,1,0:T(8,128)(2,1)S(1)}, u32[]{:S(2)}, u32[]{:S(2)}) %all-to-all-start.1) | async-done | bytes 2359328 | tf_op jit(solution)/shard_map/all_to_all | solution.py:648
  108.2 2.3 %combine.1.mine_ref = bf16[224,1024]{1,0:T(8,128)(2,1)S(1)} custom-call(s32[1]{0:T(128)} %bitcast.tp_ref.half_ref, f32[224,8]{1,0:T(8,128)S(1)} %copy-done.18, bf16[64,144,128]{2,1,0:T(8,128)(2,1)S(1)} %all-to-all-done.1.ret_ref, bf16[224,2048]{1,0:T(8,128)(2,1)S(1)} %copy-done.10), custom_call_target="tpu_custom_call" | custom-call | flops 1000000000 | bytes 3000000 | tf_op jit(solution)/shard_map/combine/pallas_call | solution.py:173
  110.6 1.8 %collective-permute-done.2.other_ref = bf16[224,1024]{1,0:T(8,128)(2,1)S(1)} collective-permute-done((bf16[224,1024]{1,0:T(8,128)(2,1)S(1)}, bf16[224,1024]{1,0:T(8,128)(2,1)S(1)}, u32[]{:S(2)}, u32[]{:S(2)}) %collective-permute-start.2) | collective-permute-done | bytes 458784 | tf_op jit(solution)/shard_map/ppermute | solution.py:618
  112.4 2.5 %mixer_cotangent.1 = (bf16[224,2048]{1,0:T(8,128)(2,1)}, f32[224,512]{1,0:T(8,128)S(1)}, bf16[224,512]{1,0:T(8,128)(2,1)}, bf16[64,16,128]{2,1,0:T(8,128)(2,1)}) custom-call(s32[1]{0:T(128)} %bitcast.tp_ref.half_ref, bf16[224,1024]{1,0:T(8,128)(2,1)S(1)} %combine.1.mine_ref, bf16[224,1024]{1,0:T(8,128)(2,1)S(1)} %collective-permute-done.2.other_ref, ...), custom_call_target="tpu_custom_call" | custom-call | flops 1000000000 | bytes 5000000 | tf_op jit(solution)/shard_map/mixer_cotangent/pallas_call | solution.py:173
  115.6 5.5 %all-to-all-start.2 = ((bf16[64,16,128]{2,1,0:T(8,128)(2,1)}), bf16[64,16,128]{2,1,0:T(8,128)(2,1)S(1)}, u32[]{:S(2)}, u32[]{:S(2)}) async-start(bf16[64,16,128]{2,1,0:T(8,128)(2,1)} %get-tuple-element.82), calls=%async_computation.2 | async-start | bytes 524288 | tf_op jit(solution)/shard_map/all_to_all | solution.py:681
  121.2 6.2 %mixer_backward.1 = (f32[224,512]{1,0:T(8,128)}, f32[224,256]{1,0:T(8,128)}, bf16[224,256]{1,0:T(8,128)(2,1)}, f32[224,8]{1,0:T(8,128)}) custom-call(bf16[224,512]{1,0:T(8,128)(2,1)} %v_ref.2, bf16[224,256]{1,0:T(8,128)(2,1)} %k_ref.3, bf16[224,256]{1,0:T(8,128)(2,1)} %q_far.1, f32[8,224]{1,0:T(8,128)} %decay_ref.5, f32[8,64,128]{2,1,0:T(8,128)} %bitcast.33, ...), custom_call_target="tpu_custom_call" | custom-call | flops 2000000000 | bytes 1000000 | tf_op jit(solution)/shard_map/mixer_backward/pallas_call | solution.py:173
  127.4 1.4 shares.1.shares_ref
  128.8 3.3 %all-to-all-done.2.in_ref = bf16[64,16,128]{2,1,0:T(8,128)(2,1)S(1)} async-done(((bf16[64,16,128]{2,1,0:T(8,128)(2,1)}), bf16[64,16,128]{2,1,0:T(8,128)(2,1)S(1)}, u32[]{:S(2)}, u32[]{:S(2)}) %all-to-all-start.2) | async-done | bytes 262176 | tf_op jit(solution)/shard_map/all_to_all | solution.py:681
  132.0 1.3 state_chain.1
  133.4 38.7 %all_to_all.20.in_ref = bf16[64,136,128]{2,1,0:T(8,128)(2,1)S(1)} all-to-all(bf16[64,136,128]{2,1,0:T(8,128)(2,1)S(1)} %state_chain.1), channel_id=1, replica_groups=mesh['sp_0'=4,'sp_1'=4,'sp_2'=4,'tp'=2] {'sp_0','sp_1','sp_2'}, dimensions={0} | all-to-all | bytes 4456448 | tf_op jit(solution)/shard_map/all_to_all | solution.py:735
  173.1 2.8 %mixer_ending.1 = (bf16[224,512]{1,0:T(8,128)(2,1)}, bf16[224,256]{1,0:T(8,128)(2,1)}, f32[8,224]{1,0:T(8,128)}) custom-call(bf16[64,136,128]{2,1,0:T(8,128)(2,1)S(1)} %all_to_all.20.in_ref, bf16[224,512]{1,0:T(8,128)(2,1)S(1)} %copy-done.34, bf16[224,256]{1,0:T(8,128)(2,1)S(1)} %copy-done.36, f32[8,224]{1,0:T(8,128)S(1)} %copy-done.20, ...), custom_call_target="tpu_custom_call" | custom-call | flops 1000000000 | bytes 1000000 | tf_op jit(solution)/shard_map/mixer_ending/pallas_call | solution.py:173
  (92 shorter events, 6.1 us)
Async XLA Ops:
  5.0 44.3 %all-to-all-start = ((bf16[64,144,128]{2,1,0:T(8,128)(2,1)}), bf16[64,144,128]{2,1,0:T(8,128)(2,1)S(1)}, u32[]{:S(2)}, u32[]{:S(2)}) async-start(bf16[64,144,128]{2,1,0:T(8,128)(2,1)} %dispatch.1), calls=%async_computation | async-start | bytes 4718592 | tf_op jit(solution)/shard_map/all_to_all | solution.py:621
  20.3 6.7 %copy-start.1 = (bf16[1152,2048]{1,0:T(8,128)(2,1)}, bf16[1152,2048]{1,0:T(8,128)(2,1)S(1)}, u32[]{:S(2)}) copy-start(bf16[1152,2048]{1,0:T(8,128)(2,1)S(1)} %ordered_rows.1) | copy-start | bytes 14155780
  20.3 4.1 %copy-start.21 = (bf16[1,2048,512]{2,1,0:T(8,128)(2,1)S(1)}, bf16[1,2048,512]{2,1,0:T(8,128)(2,1)}, u32[]{:S(2)}) copy-start(bf16[1,2048,512]{2,1,0:T(8,128)(2,1)} %param.19) | copy-start | bytes 6291460
  24.4 2.6 %copy-start.23 = (bf16[1,2048,512]{2,1,0:T(8,128)(2,1)S(1)}, bf16[1,2048,512]{2,1,0:T(8,128)(2,1)}, u32[]{:S(2)}) copy-start(bf16[1,2048,512]{2,1,0:T(8,128)(2,1)} %param.18) | copy-start | bytes 6291460
  49.3 5.0 %collective-permute-start = (bf16[64,144,128]{2,1,0:T(8,128)(2,1)S(1)}, bf16[64,144,128]{2,1,0:T(8,128)(2,1)S(1)}, u32[]{:S(2)}, u32[]{:S(2)}) collective-permute-start(bf16[64,144,128]{2,1,0:T(8,128)(2,1)S(1)} %all-to-all-done.mine_ref), channel_id=1, source_target_pairs={{0,1},{1,0},{2,3},{3,2},{4,5},{5,4},{6,7},{7,6},{8,9},{9,8},{10,11... | collective-permute-start | bytes 7077896 | tf_op jit(solution)/shard_map/ppermute | solution.py:618
  50.9 3.4 %copy-start.6 = (f32[1152,512]{1,0:T(8,128)S(1)}, f32[1152,512]{1,0:T(8,128)}, u32[]{:S(2)}) copy-start(f32[1152,512]{1,0:T(8,128)} %get-tuple-element.65.a1_ref) | copy-start | bytes 7077892
  50.9 3.4 %copy-start.7 = (f32[1152,512]{1,0:T(8,128)S(1)}, f32[1152,512]{1,0:T(8,128)}, u32[]{:S(2)}) copy-start(f32[1152,512]{1,0:T(8,128)} %get-tuple-element.66.a2_ref) | copy-start | bytes 7077892
  56.7 3.7 %copy-start.4 = (bf16[1152,1024]{1,0:T(8,128)(2,1)}, bf16[1152,1024]{1,0:T(8,128)(2,1)S(1)}, u32[]{:S(2)}) copy-start(bf16[1152,1024]{1,0:T(8,128)(2,1)S(1)} %get-tuple-element.72.other_ref) | copy-start | bytes 7077892
  56.7 4.3 %copy-start.25 = (bf16[1152,512]{1,0:T(8,128)(2,1)}, bf16[1152,512]{1,0:T(8,128)(2,1)S(1)}, u32[]{:S(2)}) copy-start(bf16[1152,512]{1,0:T(8,128)(2,1)S(1)} %get-tuple-element.75.ug_ref) | copy-start | bytes 3538948
  56.7 4.3 %copy-start.27 = (bf16[1152,512]{1,0:T(8,128)(2,1)}, bf16[1152,512]{1,0:T(8,128)(2,1)S(1)}, u32[]{:S(2)}) copy-start(bf16[1152,512]{1,0:T(8,128)(2,1)S(1)} %get-tuple-element.74.gg_ref) | copy-start | bytes 3538948
  60.5 4.7 %collective-permute-start.1 = (bf16[64,144,128]{2,1,0:T(8,128)(2,1)S(1)}, bf16[64,144,128]{2,1,0:T(8,128)(2,1)S(1)}, u32[]{:S(2)}, u32[]{:S(2)}) collective-permute-start(bf16[64,144,128]{2,1,0:T(8,128)(2,1)S(1)} %span_half.3), channel_id=1, source_target_pairs={{0,1},{1,0},{2,3},{3,2},{4,5},{5,4},{6,7},{7,6},{8,9},{9,8},{10,11... | collective-permute-start | bytes 7077896 | tf_op jit(solution)/shard_map/ppermute | solution.py:618
  67.4 39.8 %all-to-all-start.1 = ((bf16[64,144,128]{2,1,0:T(8,128)(2,1)}), bf16[64,144,128]{2,1,0:T(8,128)(2,1)S(1)}, u32[]{:S(2)}, u32[]{:S(2)}) async-start(bf16[64,144,128]{2,1,0:T(8,128)(2,1)} %add_convert_fusion), calls=%async_computation.1 | async-start | bytes 4718592 | tf_op jit(solution)/shard_map/all_to_all | solution.py:648
  77.1 4.9 %copy-start.28 = (bf16[1152,512]{1,0:T(8,128)(2,1)S(1)}, bf16[1152,512]{1,0:T(8,128)(2,1)}, u32[]{:S(2)}) copy-start(bf16[1152,512]{1,0:T(8,128)(2,1)} %copy-done.27) | copy-start | bytes 3538948
  77.1 11.6 %slice-start = ((s8[4718592]{0:T(1024)(128)(4,1)}), s8[4194304]{0:T(1024)(128)(4,1)S(1)}, s32[]{:S(2)}) async-start(s8[4718592]{0:T(1024)(128)(4,1)} %bitcast.25), calls=%async_computation.4 | async-start | bytes 8388608
  82.0 6.7 %slice-start.1 = ((s8[4718592]{0:T(1024)(128)(4,1)}), s8[524288]{0:T(1024)(128)(4,1)S(1)}, s32[]{:S(2)}) async-start(s8[4718592]{0:T(1024)(128)(4,1)} %bitcast.25), calls=%async_computation.5 | async-start | bytes 1048576
  82.0 6.7 %copy-start.26 = (bf16[1152,512]{1,0:T(8,128)(2,1)S(1)}, bf16[1152,512]{1,0:T(8,128)(2,1)}, u32[]{:S(2)}) copy-start(bf16[1152,512]{1,0:T(8,128)(2,1)} %copy-done.25) | copy-start | bytes 3538948
  88.7 18.6 %copy-start.10 = (bf16[224,2048]{1,0:T(8,128)(2,1)S(1)}, bf16[224,2048]{1,0:T(8,128)(2,1)}, u32[]{:S(2)}) copy-start(bf16[224,2048]{1,0:T(8,128)(2,1)} %og_ref.1) | copy-start | bytes 2752516
  92.8 19.6 %copy-start.14 = (bf16[224,512]{1,0:T(8,128)(2,1)S(1)}, bf16[224,512]{1,0:T(8,128)(2,1)}, u32[]{:S(2)}) copy-start(bf16[224,512]{1,0:T(8,128)(2,1)} %gate_ref.3) | copy-start | bytes 688132
  108.1 4.2 %copy-start.8 = (bf16[2048,512]{1,0:T(8,128)(2,1)S(1)}, bf16[2048,512]{1,0:T(8,128)(2,1)}, u32[]{:S(2)}) copy-start(bf16[2048,512]{1,0:T(8,128)(2,1)} %ow_ref.1) | copy-start | bytes 6291460
  108.1 4.2 %copy-start.12 = (f32[224,512]{1,0:T(8,128)S(1)}, f32[224,512]{1,0:T(8,128)}, u32[]{:S(2)}) copy-start(f32[224,512]{1,0:T(8,128)} %copy-done.11) | copy-start | bytes 1376260
  108.2 4.2 %copy-start.16 = (bf16[224,256]{1,0:T(8,128)(2,1)S(1)}, bf16[224,256]{1,0:T(8,128)(2,1)}, u32[]{:S(2)}) copy-start(bf16[224,256]{1,0:T(8,128)(2,1)} %q_far.1) | copy-start | bytes 344068
  110.5 1.9 %collective-permute-start.2 = (bf16[224,1024]{1,0:T(8,128)(2,1)S(1)}, bf16[224,1024]{1,0:T(8,128)(2,1)S(1)}, u32[]{:S(2)}, u32[]{:S(2)}) collective-permute-start(bf16[224,1024]{1,0:T(8,128)(2,1)S(1)} %combine.1.mine_ref), channel_id=1, source_target_pairs={{0,1},{1,0},{2,3},{3,2},{4,5},{5,4},{6,7},{7,6},{8,9},{9,8},{10,11... | collective-permute-start | bytes 1376264 | tf_op jit(solution)/shard_map/ppermute | solution.py:618
  115.6 16.4 %all-to-all-start.2 = ((bf16[64,16,128]{2,1,0:T(8,128)(2,1)}), bf16[64,16,128]{2,1,0:T(8,128)(2,1)S(1)}, u32[]{:S(2)}, u32[]{:S(2)}) async-start(bf16[64,16,128]{2,1,0:T(8,128)(2,1)} %get-tuple-element.82), calls=%async_computation.2 | async-start | bytes 524288 | tf_op jit(solution)/shard_map/all_to_all | solution.py:681
  121.1 6.2 %copy-start.29 = (bf16[224,2048]{1,0:T(8,128)(2,1)S(1)}, bf16[224,2048]{1,0:T(8,128)(2,1)}, u32[]{:S(2)}) copy-start(bf16[224,2048]{1,0:T(8,128)(2,1)} %get-tuple-element.88.hidden_ref) | copy-start | bytes 2752516
  121.2 6.2 %copy-start.42 = (bf16[224,512]{1,0:T(8,128)(2,1)S(1)}, bf16[224,512]{1,0:T(8,128)(2,1)}, u32[]{:S(2)}) copy-start(bf16[224,512]{1,0:T(8,128)(2,1)} %copy-done.41) | copy-start | bytes 688132
  133.3 39.7 %copy-start.20 = (f32[8,224]{1,0:T(8,128)S(1)}, f32[8,224]{1,0:T(8,128)}, u32[]{:S(2)}) copy-start(f32[8,224]{1,0:T(8,128)} %decay_ref.5) | copy-start | bytes 21508
  133.3 39.7 %copy-start.32 = (f32[1,8,64,128]{3,2,1,0:T(8,128)S(1)}, f32[1,8,64,128]{3,2,1,0:T(8,128)}, u32[]{:S(2)}) copy-start(f32[1,8,64,128]{3,2,1,0:T(8,128)} %param.26) | copy-start | bytes 786436
  133.3 39.7 %copy-start.34 = (bf16[224,512]{1,0:T(8,128)(2,1)S(1)}, bf16[224,512]{1,0:T(8,128)(2,1)}, u32[]{:S(2)}) copy-start(bf16[224,512]{1,0:T(8,128)(2,1)} %v_ref.2) | copy-start | bytes 688132
  133.3 39.7 %copy-start.36 = (bf16[224,256]{1,0:T(8,128)(2,1)S(1)}, bf16[224,256]{1,0:T(8,128)(2,1)}, u32[]{:S(2)}) copy-start(bf16[224,256]{1,0:T(8,128)(2,1)} %k_ref.3) | copy-start | bytes 344068
  133.4 39.7 %copy-start.38 = (f32[224,512]{1,0:T(8,128)S(1)}, f32[224,512]{1,0:T(8,128)}, u32[]{:S(2)}) copy-start(f32[224,512]{1,0:T(8,128)} %get-tuple-element.96.dv_ref) | copy-start | bytes 1376260
  133.4 39.7 %copy-start.39 = (f32[224,256]{1,0:T(8,128)S(1)}, f32[224,256]{1,0:T(8,128)}, u32[]{:S(2)}) copy-start(f32[224,256]{1,0:T(8,128)} %get-tuple-element.97.dk_ref) | copy-start | bytes 688132
  133.4 39.7 %copy-start.40 = (f32[224,8]{1,0:T(8,128)S(1)}, f32[224,8]{1,0:T(8,128)}, u32[]{:S(2)}) copy-start(f32[224,8]{1,0:T(8,128)} %get-tuple-element.98.diff_ref) | copy-start | bytes 21508
  (19 other events, 27.8 us)

commit v2 on v1

--- a/solution.py
+++ b/solution.py
@@ -85,9 +85,8 @@
     return out
 
 
-def copy_out(from_ref, to_ref, sems, b):
-    peers = slice(16 * b, 16 * b + 16)
-    copy = pltpu.make_async_copy(from_ref.at[peers], to_ref.at[peers], sems.at[b])
+def begin(far, near, sem):
+    copy = pltpu.make_async_copy(far, near, sem)
     copy.start()
     return copy
 
@@ -118,14 +117,19 @@
     tp_ref, far_routes, far_w, far_og, to_ref, routes_ref, w_ref, og_ref, out_ref, sems, in_sems
 ):
     own = half_of(tp_ref)
-    load(((far_routes, routes_ref), (far_w, w_ref), (far_og.at[:, own], og_ref)), in_sems)
+    load_routes = begin(far_routes, routes_ref, in_sems.at[0])
+    load_w = begin(far_w, w_ref, in_sems.at[1])
+    load_og = begin(far_og.at[:, own], og_ref, in_sems.at[2])
+    load_routes.wait()
     r0, r1, f0, f1 = slots(routes_ref[...])
+    load_w.wait()
     w0, w1 = w_ref[0:1, :], w_ref[1:2, :]
     s0, s1 = f0.astype(jnp.int32), f1.astype(jnp.int32)
     m0 = jnp.where(s0 < MAIN, r0 * MAIN + s0, -1)
     m1 = jnp.where(s1 < MAIN, r1 * MAIN + s1, -1)
     t0 = jnp.where(s0 >= MAIN, r0 * TAIL + s0 - MAIN, -1)
     t1 = jnp.where(s1 >= MAIN, r1 * TAIL + s1 - MAIN, -1)
+    load_og.wait()
     og = og_ref[...]
 
     def rows_of(first, count, a0, a1):
@@ -136,16 +140,20 @@
         scale = jnp.sum(scale, axis=1, keepdims=True)
         return (dot(pick, og) * scale).astype(BF)
 
-    tail = pack_tail(rows_of(0, 128, t0, t1)).astype(BF)
-    out_ref[:, 16 * COLS : MSG, :] = tail.reshape(PEERS, 16, 128)
     copies = []
     for b in range(4):
         block = rows_of(256 * b, 256, m0, m1)
+        peers = slice(16 * b, 16 * b + 16)
         for c in range(COLS):
-            out_ref[16 * b : 16 * b + 16, 16 * c : 16 * c + 16, :] = block[
-                :, 128 * c : 128 * c + 128
-            ].reshape(16, 16, 128)
-        copies.append(copy_out(out_ref, to_ref, sems, b))
+            out_ref[peers, 16 * c : 16 * c + 16, :] = block[:, 128 * c : 128 * c + 128].reshape(
+                16, 16, 128
+            )
+        main = slice(0, 16 * COLS)
+        copies.append(begin(out_ref.at[peers, main], to_ref.at[peers, main], sems.at[b]))
+    tail = pack_tail(rows_of(0, 128, t0, t1)).astype(BF)
+    out_ref[:, 16 * COLS : MSG, :] = tail.reshape(PEERS, 16, 128)
+    rest = slice(16 * COLS, MSG)
+    copies.append(begin(out_ref.at[:, rest], to_ref.at[:, rest], sems.at[4]))
     for copy in copies:
         copy.wait()
 
@@ -201,7 +209,7 @@
             pltpu.VMEM((2, TOK), F32),
             pltpu.VMEM((TOK, HALF), BF),
             pltpu.VMEM((PEERS, MSG, 128), BF),
-            dma((4,)),
+            dma((5,)),
             dma((3,)),
         ],
         hbm_ins=(0, 1, 2),
@@ -404,7 +412,7 @@
 
 
 def forward_kernel(
-    v_ref, k_ref, q_ref, decay_ref, gate_ref, e_ref, routes_ref, core_ref, mixed_ref, meta_ref
+    v_ref, k_ref, q_ref, decay_ref, gate_ref, e_ref, routes_ref, core_ref, mixed_ref, meta_ref, fade_ref
 ):
     r0, r1, f0, f1 = slots(routes_ref[...])
     zero = jnp.zeros((4, TOK), F32)
@@ -412,6 +420,8 @@
     eye = jnp.where(iota((TOK, TOK), 0) == iota((TOK, TOK), 1), 1.0, 0.0).astype(BF)
     meta_ref[...] = dot(eye, table, NT)
     cum, cum_t = decay_sums(decay_ref[...])
+    fade_ref[:, 0:HEADS] = jnp.exp(cum_t)
+    fade_ref[:, HEADS : 2 * HEADS] = jnp.exp(cum_t[TOK - 1 : TOK, :] - cum_t)
     for g in range(GROUPS):
         q, k = q_ref[:, group(g)], k_ref[:, group(g)]
         scores = dot(q, k, NT)
@@ -430,7 +440,7 @@
 
 
 def cotangent_kernel(
-    tp_ref, mine_ref, other_ref, ow_ref, core_ref, gate_ref, decay_ref, q_ref,
+    tp_ref, mine_ref, other_ref, ow_ref, core_ref, gate_ref, decay_ref, q_ref, fade_ref,
     hidden_ref, dcore_ref, dgate_ref, msg_ref,
 ):
     first = tp_ref[0] == 0
@@ -444,8 +454,7 @@
     dcore = cot * (gate * sig)
     dcore_ref[...] = dcore
     dgate_ref[...] = (cot * core_ref[...] * (sig * (1.0 + gate * (1.0 - sig)))).astype(BF)
-    _, cum_t = decay_sums(decay_ref[...])
-    growth = jnp.exp(cum_t)
+    growth = fade_ref[:, 0:HEADS]
     logs = jnp.sum(decay_ref[...], axis=1, keepdims=True)
     high, low = split(logs)
     mid, _ = split(low_part(logs, high))
@@ -538,33 +547,31 @@
 
 
 def ending_kernel(
-    in_ref, v_ref, k_ref, decay_ref, e_ref, dv_ref, dk_ref, diff_ref, gv_ref, gk_ref, gd_ref
+    in_ref, v_ref, k_ref, fade_ref, e_ref, dv_ref, dk_ref, diff_ref, gv_ref, gk_ref, gd_ref
 ):
-    cum, cum_t = decay_sums(decay_ref[...])
-    last = cum_t[TOK - 1 : TOK, :]
-    tail = jnp.exp(last - cum_t)
-    fresh = []
-    kept = []
-    diff = []
+    fade = fade_ref[...]
+    tail = fade[:, HEADS : 2 * HEADS]
+    last = fade[TOK - 1 : TOK, 0:HEADS]
+    fresh, kept, diff = [], [], []
     for g in range(GROUPS):
-        k = k_ref[:, group(g)]
-        dk = dk_ref[:, group(g)]
-        for h in range(PER_GROUP * g, PER_GROUP * g + PER_GROUP):
-            state = in_ref[8 * h : 8 * h + 8, 128:136, :].astype(F32).reshape(HD, NS)
-            exact = state.astype(BF)
-            v = v_ref[:, head(h)].astype(F32)
-            t = tail[:, h : h + 1]
-            dv2 = t * dot(k, exact, NT)
-            dk = dk + dot2(v * t, exact)
-            dv = dv_ref[:, head(h)] + dv2
-            gv_ref[:, head(h)] = dv.astype(BF)
-            moved = jnp.sum(v * dv2, axis=1, keepdims=True)
+        wide = slice(256 * g, 256 * g + 256)
+        heads = range(PER_GROUP * g, PER_GROUP * g + PER_GROUP)
+        state = in_ref[32 * g : 32 * g + 32, 128:136, :].astype(F32).reshape(PER_GROUP * HD, NS)
+        exact = state.astype(BF)
+        v = v_ref[:, wide].astype(F32)
+        spread = [jnp.broadcast_to(tail[:, h : h + 1], (TOK, HD)) for h in heads]
+        spread = jnp.concatenate(spread, axis=1)
+        dv2 = spread * dot(k_ref[:, group(g)], exact, NT)
+        gv_ref[:, wide] = (dv_ref[:, wide] + dv2).astype(BF)
+        gk_ref[:, group(g)] = (dk_ref[:, group(g)] + dot2(v * spread, exact)).astype(BF)
+        change = v * dv2
+        for i, h in enumerate(heads):
+            moved = jnp.sum(change[:, head(i)], axis=1, keepdims=True)
             diff.append(moved)
             fresh.append(jnp.sum(moved).reshape(1, 1))
-            kept.append(jnp.sum(e_ref[h] * state).reshape(1, 1))
-        gk_ref[:, group(g)] = dk.astype(BF)
+            kept.append(jnp.sum(e_ref[h] * state[head(i)]).reshape(1, 1))
     diff = diff_ref[...] - jnp.concatenate(diff, axis=1)
-    at_end = jnp.concatenate(fresh, axis=1) + jnp.exp(last) * jnp.concatenate(kept, axis=1)
+    at_end = jnp.concatenate(fresh, axis=1) + last * jnp.concatenate(kept, axis=1)
     diff = diff + jnp.where(iota((TOK, HEADS), 0) == TOK - 1, at_end, 0.0)
     later = jnp.where(iota((TOK, TOK), 0) >= iota((TOK, TOK), 1), 1.0, 0.0)
     gd_ref[...] = dotp(diff, later, TN)
@@ -629,16 +636,16 @@
     act = (silu * up_pre).astype(BF)
     a1 = up_pre * sig * (1.0 + gate_pre * (1.0 - sig))
     _, later_values = lax.optimization_barrier((message, values))
-    core, mixer_out, meta = call(
+    core, mixer_out, meta, fade = call(
         forward_kernel,
-        [sds((TOK, HEADS * HD), F32), sds((TOK, HEADS * HD), BF), sds((TOK, 8), F32)],
+        [sds((TOK, HEADS * HD), F32), sds((TOK, HEADS * HD), BF), sds((TOK, 8), F32), sds((TOK, 16), F32)],
         (later_values, key_side, query_side, decay_log, gate_in, entry, routes.T),
         10**9,
         10**6,
         name="mixer_forward",
     )
-    moved, rows, act, a1, silu, core, mixer_out, meta = lax.optimization_barrier(
-        (moved, rows, act, a1, silu, core, mixer_out, meta)
+    moved, rows, act, a1, silu, core, mixer_out, meta, fade = lax.optimization_barrier(
+        (moved, rows, act, a1, silu, core, mixer_out, meta, fade)
     )
 
     arrived, gate_grad, up_grad = hidden_grads(tp, moved, swap(moved), down_w, a1, silu)
@@ -672,6 +679,7 @@
             gate_in,
             decay_log,
             query_side,
+            fade,
         ),
         10**9,
         5 * 10**6,
@@ -748,7 +756,7 @@
             sds((TOK, GROUPS * NS), BF),
             sds((HEADS, TOK), F32),
         ],
-        (received, values, key_side, decay_log, entry, dv, dk, diff),
+        (received, values, key_side, fade, entry, dv, dk, diff),
         10**9,
         10**6,
         name="mixer_ending",

time: 177 us -> 176 us (level)
  Pallas kernels: 41.6 us -> 39.8 us
  waiting for transfers between devices: 37.2 us -> 35.4 us
  local copies, waits for them, and re-layouts: 12.6 us -> 14.4 us
    pallas_call x15, Pallas kernels: 41.6 us -> 39.8 us  [call(): pl.pallas_call(kernel, out_shape=outs, in_specs=in_specs, out_specs=[far...]
    unnamed x90 -> x92, local copies, waits for them, and re-layouts: 12.6 us -> 14.4 us
  transfers between devices with their start and end apart: 6 -> 6, of which waited for: 5 -> 5; matrix products, arithmetic and copies ran while one was open for 10% -> 11% of each run, Pallas kernels for 12% -> 12%
where the time goes in v2:
time: 176 us; the launch traced here: 175 us
  Pallas kernels  39.8 us (23%)
  blocking collectives  39.6 us (22%)
  waiting for transfers between devices  35.4 us (20%)
  starting transfers between devices  24.1 us (14%)
  matrix products  18.4 us (10%)
  local copies, waits for them, and re-layouts  14.4 us (8%)
  other arithmetic  2.19 us (1%)
    pallas_call x15, Pallas kernels, call(): pl.pallas_call(kernel, out_shape=outs, in_specs=in_specs, out_specs=[far...  39.8 us
    all_to_all x1, blocking collectives, per_device(): lax.all_to_all(message, SP, split_axis=0, concat_axis=0, tiled=True)  39.6 us
    all_to_all x1, waiting for transfers between devices, per_device(): moved = lax.all_to_all(message, SP, split_axis=0, concat_axis=0, tiled=True)  16.5 us
    all_to_all x1, waiting for transfers between devices, per_device(): returned = lax.all_to_all(back, SP, split_axis=0, concat_axis=0, tiled=True)  14.4 us
    unnamed x92, local copies, waits for them, and re-layouts  14.4 us
    all_to_all x1, starting transfers between devices, per_device(): moved = lax.all_to_all(message, SP, split_axis=0, concat_axis=0, tiled=True)  11.5 us
    dot_general x2, matrix products, dot(): return lax.dot_general(a, b, dims, preferred_element_type=F32)  10.8 us
    all_to_all x1, starting transfers between devices, per_device(): returned = lax.all_to_all(back, SP, split_axis=0, concat_axis=0, tiled=True)  6.35 us
  transfers between devices with their start and end apart: 6, of which 5 were waited for; matrix products, arithmetic and copies ran while one was open for 11% of the time, Pallas kernels for 12%

profile of v2, /device:TPU:0, one launch (start us, length us, event | category | flops | bytes accessed | tf_op | source)
XLA Modules:
  0.0 174.9 jit_solution(4924064684238044174)
XLA Ops:
  0.6 3.4 %dispatch.1 = bf16[64,144,128]{2,1,0:T(8,128)(2,1)} custom-call(s32[1]{0:T(128)} %bitcast.tp_ref.half_ref, s32[2,224]{1,0:T(2,128)} %bitcast.36, f32[2,224]{1,0:T(2,128)} %bitcast.39, bf16[224,2048]{1,0:T(8,128)(2,1)} %og_ref.1), custom_call_target="tpu_custom_call" | custom-call | flops 1000000000 | bytes 3000000 | tf_op jit(solution)/shard_map/dispatch/pallas_call | solution.py:181
  4.1 11.5 %all-to-all-start = ((bf16[64,144,128]{2,1,0:T(8,128)(2,1)}), bf16[64,144,128]{2,1,0:T(8,128)(2,1)S(1)}, u32[]{:S(2)}, u32[]{:S(2)}) async-start(bf16[64,144,128]{2,1,0:T(8,128)(2,1)} %dispatch.1), calls=%async_computation | async-start | bytes 4718592 | tf_op jit(solution)/shard_map/all_to_all | solution.py:628
  15.7 2.3 %copy-done = bf16[1,64,18,2048]{3,1,2,0:T(8,128)(2,1)S(1)} copy-done((bf16[1,64,18,2048]{3,1,2,0:T(8,128)(2,1)S(1)}, bf16[1,64,18,2048]{3,1,2,0:T(8,128)(2,1)}, u32[]{:S(2)}) %copy-start) | copy-done | bytes 4718616
  18.0 1.4 ordered_rows.1
  19.5 1.9 %mixer_forward.1 = (f32[224,512]{1,0:T(8,128)S(1)}, bf16[224,512]{1,0:T(8,128)(2,1)S(1)}, f32[224,8]{1,0:T(8,128)S(1)}, f32[224,16]{1,0:T(8,128)S(1)}) custom-call(bf16[224,512]{1,0:T(8,128)(2,1)S(1)} %copy-done.20, bf16[224,256]{1,0:T(8,128)(2,1)S(1)} %copy-done.25, bf16[224,256]{1,0:T(8,128)(2,1)S(1)} %copy-done.23, f32[8,224]{1,0:T(8,128)S(1)} %copy-done.30, ...), custom_call_target="tpu_custom_call" | custom-call | flops 1000000000 | bytes 1000000 | tf_op jit(solution)/shard_map/mixer_forward/pallas_call | solution.py:181
  24.2 2.6 %fusion.1 = f32[1152,512]{1,0:T(8,128)S(1)} fusion(bf16[1152,2048]{1,0:T(8,128)(2,1)S(1)} %ordered_rows.1, bf16[1,2048,512]{2,1,0:T(8,128)(2,1)S(1)} %copy-done.31), kind=kOutput, calls=%fused_computation.7 | convolution fusion | flops 2415919104 | bytes 9175040 | tf_op jit(solution)/shard_map/dot_general | solution.py:633
  26.9 5.1 %add_multiply_fusion = (f32[1152,512]{1,0:T(8,128)}, bf16[1152,512]{1,0:T(8,128)(2,1)S(1)}, f32[1152,512]{1,0:T(8,128)}) fusion(f32[1152,512]{1,0:T(8,128)S(1)} %fusion.1, bf16[1152,2048]{1,0:T(8,128)(2,1)S(1)} %ordered_rows.1, bf16[1,2048,512]{2,1,0:T(8,128)(2,1)S(1)} %copy-done.33), kind=kOutput, calls=%fused_computation.3 | convolution fusion | flops 2422407168 | bytes 15073280 | tf_op jit(solution)/shard_map/dot_general | solution.py:632
  31.9 16.5 %all-to-all-done.mine_ref = bf16[64,144,128]{2,1,0:T(8,128)(2,1)S(1)} async-done(((bf16[64,144,128]{2,1,0:T(8,128)(2,1)}), bf16[64,144,128]{2,1,0:T(8,128)(2,1)S(1)}, u32[]{:S(2)}, u32[]{:S(2)}) %all-to-all-start) | async-done | bytes 2359328 | tf_op jit(solution)/shard_map/all_to_all | solution.py:628
  48.5 1.6 copy-done.9
  50.0 2.0 %hidden_first.1 = (bf16[1152,1024]{1,0:T(8,128)(2,1)S(1)}, f32[1152,512]{1,0:T(8,128)S(1)}) custom-call(s32[1]{0:T(128)} %bitcast.tp_ref.half_ref, bf16[64,144,128]{2,1,0:T(8,128)(2,1)S(1)} %all-to-all-done.mine_ref, bf16[512,2048]{1,0:T(8,128)(2,1)S(1)} %bitcast.27), custom_call_target="tpu_custom_call" | custom-call | flops 2000000000 | bytes 10000000 | tf_op jit(solution)/shard_map/hidden_first/pallas_call | solution.py:181
  52.0 1.4 copy-done.2
  53.5 2.3 %hidden_second.1 = (bf16[1152,1024]{1,0:T(8,128)(2,1)S(1)}, bf16[1152,512]{1,0:T(8,128)(2,1)S(1)}, bf16[1152,512]{1,0:T(8,128)(2,1)S(1)}) custom-call(s32[1]{0:T(128)} %bitcast.tp_ref.half_ref, bf16[64,144,128]{2,1,0:T(8,128)(2,1)S(1)} %collective-permute-done.other_ref, bf16[512,2048]{1,0:T(8,128)(2,1)S(1)} %bitcast.28, ...), custom_call_target="tpu_custom_call" | custom-call | flops 2000000000 | bytes 10000000 | tf_op jit(solution)/shard_map/hidden_second/pallas_call | solution.py:181
  55.9 3.7 %span_half.3 = bf16[64,144,128]{2,1,0:T(8,128)(2,1)S(1)} custom-call(s32[1]{0:T(128)} %bitcast.tp_ref.half_ref, bf16[1152,512]{1,0:T(8,128)(2,1)S(1)} %get-tuple-element.77.gg_ref, bf16[1152,512]{1,0:T(8,128)(2,1)S(1)} %get-tuple-element.78.ug_ref, bf16[2048,512]{1,0:T(8,128)(2,1)S(1)} %bitcast.34, bf16[2048,512]{1,0:T(8,128)(2,1)S(1)} %bitcast.32), custom_call_target="tpu_custom_call" | custom-call | flops 4000000000 | bytes 10000000 | tf_op jit(solution)/shard_map/span_half/pallas_call | solution.py:181
  60.2 3.7 %span_half.2 = bf16[64,144,128]{2,1,0:T(8,128)(2,1)S(1)} custom-call(s32[1]{0:T(128)} %bitcast.tp_ref.half_ref, bf16[1152,512]{1,0:T(8,128)(2,1)S(1)} %get-tuple-element.77.gg_ref, bf16[1152,512]{1,0:T(8,128)(2,1)S(1)} %get-tuple-element.78.ug_ref, bf16[2048,512]{1,0:T(8,128)(2,1)S(1)} %bitcast.35, bf16[2048,512]{1,0:T(8,128)(2,1)S(1)} %bitcast.33), custom_call_target="tpu_custom_call" | custom-call | flops 4000000000 | bytes 10000000 | tf_op jit(solution)/shard_map/span_half/pallas_call | solution.py:181
  64.3 2.2 %add_convert_fusion = bf16[64,144,128]{2,1,0:T(8,128)(2,1)} fusion(bf16[64,144,128]{2,1,0:T(8,128)(2,1)S(1)} %collective-permute-done.1, bf16[64,144,128]{2,1,0:T(8,128)(2,1)S(1)} %span_half.2), kind=kLoop, calls=%fused_computation | loop fusion | flops 4718592 | bytes 7077888 | tf_op jit(solution)/shard_map/convert_element_type | solution.py:654
  66.5 6.4 %all-to-all-start.1 = ((bf16[64,144,128]{2,1,0:T(8,128)(2,1)}), bf16[64,144,128]{2,1,0:T(8,128)(2,1)S(1)}, u32[]{:S(2)}, u32[]{:S(2)}) async-start(bf16[64,144,128]{2,1,0:T(8,128)(2,1)} %add_convert_fusion), calls=%async_computation.1 | async-start | bytes 4718592 | tf_op jit(solution)/shard_map/all_to_all | solution.py:655
  72.9 1.7 copy-done.3
  74.5 1.7 copy-done.5
  76.2 4.9 %down_grad.1 = bf16[512,2048]{1,0:T(8,128)(2,1)} custom-call(s32[1]{0:T(128)} %bitcast.tp_ref.half_ref, bf16[1152,512]{1,0:T(8,128)(2,1)S(1)} %get-tuple-element.73.act_ref, bf16[1152,1024]{1,0:T(8,128)(2,1)S(1)} %copy-done.3, bf16[1152,1024]{1,0:T(8,128)(2,1)S(1)} %copy-done.5), custom_call_target="tpu_custom_call" | custom-call | flops 2000000000 | bytes 10000000 | tf_op jit(solution)/shard_map/down_grad/pallas_call | solution.py:181
  81.1 6.7 %convolution_convert_fusion.1 = bf16[2048,512]{1,0:T(8,128)(2,1)} fusion(bf16[1152,2048]{1,0:T(8,128)(2,1)} %copy-done.1, bf16[1152,512]{1,0:T(8,128)(2,1)S(1)} %copy-done.38), kind=kOutput, calls=%fused_computation.2 | convolution fusion | flops 2416967680 | bytes 7995392 | tf_op jit(solution)/shard_map/dot_general | solution.py:43
  87.8 4.1 %convolution_convert_fusion = bf16[2048,512]{1,0:T(8,128)(2,1)} fusion(bf16[1152,2048]{1,0:T(8,128)(2,1)S(1)} %bitcast.26, bf16[1152,512]{1,0:T(8,128)(2,1)S(1)} %copy-done.36), kind=kOutput, calls=%fused_computation.1 | convolution fusion | flops 2416967680 | bytes 7995392 | tf_op jit(solution)/shard_map/dot_general | solution.py:43
  91.9 14.4 %all-to-all-done.1.ret_ref = bf16[64,144,128]{2,1,0:T(8,128)(2,1)S(1)} async-done(((bf16[64,144,128]{2,1,0:T(8,128)(2,1)}), bf16[64,144,128]{2,1,0:T(8,128)(2,1)S(1)}, u32[]{:S(2)}, u32[]{:S(2)}) %all-to-all-start.1) | async-done | bytes 2359328 | tf_op jit(solution)/shard_map/all_to_all | solution.py:655
  107.3 2.3 %combine.1.mine_ref = bf16[224,1024]{1,0:T(8,128)(2,1)S(1)} custom-call(s32[1]{0:T(128)} %bitcast.tp_ref.half_ref, f32[224,8]{1,0:T(8,128)S(1)} %copy-done.28, bf16[64,144,128]{2,1,0:T(8,128)(2,1)S(1)} %all-to-all-done.1.ret_ref, bf16[224,2048]{1,0:T(8,128)(2,1)S(1)} %copy-done.10), custom_call_target="tpu_custom_call" | custom-call | flops 1000000000 | bytes 3000000 | tf_op jit(solution)/shard_map/combine/pallas_call | solution.py:181
  109.7 1.8 %collective-permute-done.2.other_ref = bf16[224,1024]{1,0:T(8,128)(2,1)S(1)} collective-permute-done((bf16[224,1024]{1,0:T(8,128)(2,1)S(1)}, bf16[224,1024]{1,0:T(8,128)(2,1)S(1)}, u32[]{:S(2)}, u32[]{:S(2)}) %collective-permute-start.2) | collective-permute-done | bytes 458784 | tf_op jit(solution)/shard_map/ppermute | solution.py:625
  111.5 2.0 %mixer_cotangent.1 = (bf16[224,2048]{1,0:T(8,128)(2,1)}, f32[224,512]{1,0:T(8,128)S(1)}, bf16[224,512]{1,0:T(8,128)(2,1)}, bf16[64,16,128]{2,1,0:T(8,128)(2,1)}) custom-call(s32[1]{0:T(128)} %bitcast.tp_ref.half_ref, bf16[224,1024]{1,0:T(8,128)(2,1)S(1)} %combine.1.mine_ref, bf16[224,1024]{1,0:T(8,128)(2,1)S(1)} %collective-permute-done.2.other_ref, ...), custom_call_target="tpu_custom_call" | custom-call | flops 1000000000 | bytes 5000000 | tf_op jit(solution)/shard_map/mixer_cotangent/pallas_call | solution.py:181
  114.3 5.5 %all-to-all-start.2 = ((bf16[64,16,128]{2,1,0:T(8,128)(2,1)}), bf16[64,16,128]{2,1,0:T(8,128)(2,1)S(1)}, u32[]{:S(2)}, u32[]{:S(2)}) async-start(bf16[64,16,128]{2,1,0:T(8,128)(2,1)} %get-tuple-element.86), calls=%async_computation.2 | async-start | bytes 524288 | tf_op jit(solution)/shard_map/all_to_all | solution.py:689
  119.8 6.2 %mixer_backward.1 = (f32[224,512]{1,0:T(8,128)}, f32[224,256]{1,0:T(8,128)}, bf16[224,256]{1,0:T(8,128)(2,1)}, f32[224,8]{1,0:T(8,128)}) custom-call(bf16[224,512]{1,0:T(8,128)(2,1)} %v_ref.2, bf16[224,256]{1,0:T(8,128)(2,1)} %k_ref.3, bf16[224,256]{1,0:T(8,128)(2,1)} %q_far.1, f32[8,224]{1,0:T(8,128)} %decay_far.1, f32[8,64,128]{2,1,0:T(8,128)} %bitcast.29, ...), custom_call_target="tpu_custom_call" | custom-call | flops 2000000000 | bytes 1000000 | tf_op jit(solution)/shard_map/mixer_backward/pallas_call | solution.py:181
  127.2 1.4 shares.1.shares_ref
  128.6 2.1 %all-to-all-done.2.in_ref = bf16[64,16,128]{2,1,0:T(8,128)(2,1)S(1)} async-done(((bf16[64,16,128]{2,1,0:T(8,128)(2,1)}), bf16[64,16,128]{2,1,0:T(8,128)(2,1)S(1)}, u32[]{:S(2)}, u32[]{:S(2)}) %all-to-all-start.2) | async-done | bytes 262176 | tf_op jit(solution)/shard_map/all_to_all | solution.py:689
  130.7 1.3 state_chain.1
  132.1 39.6 %all_to_all.20.in_ref = bf16[64,136,128]{2,1,0:T(8,128)(2,1)S(1)} all-to-all(bf16[64,136,128]{2,1,0:T(8,128)(2,1)S(1)} %state_chain.1), channel_id=1, replica_groups=mesh['sp_0'=4,'sp_1'=4,'sp_2'=4,'tp'=2] {'sp_0','sp_1','sp_2'}, dimensions={0} | all-to-all | bytes 4456448 | tf_op jit(solution)/shard_map/all_to_all | solution.py:743
  172.6 2.3 %mixer_ending.1 = (bf16[224,512]{1,0:T(8,128)(2,1)}, bf16[224,256]{1,0:T(8,128)(2,1)}, f32[8,224]{1,0:T(8,128)}) custom-call(bf16[64,136,128]{2,1,0:T(8,128)(2,1)S(1)} %all_to_all.20.in_ref, bf16[224,512]{1,0:T(8,128)(2,1)S(1)} %copy-done.21, bf16[224,256]{1,0:T(8,128)(2,1)S(1)} %copy-done.26, f32[224,16]{1,0:T(8,128)S(1)} %copy-done.15, ...), custom_call_target="tpu_custom_call" | custom-call | flops 1000000000 | bytes 1000000 | tf_op jit(solution)/shard_map/mixer_ending/pallas_call | solution.py:181
  (94 shorter events, 7.9 us)
Async XLA Ops:
  4.1 44.3 %all-to-all-start = ((bf16[64,144,128]{2,1,0:T(8,128)(2,1)}), bf16[64,144,128]{2,1,0:T(8,128)(2,1)S(1)}, u32[]{:S(2)}, u32[]{:S(2)}) async-start(bf16[64,144,128]{2,1,0:T(8,128)(2,1)} %dispatch.1), calls=%async_computation | async-start | bytes 4718592 | tf_op jit(solution)/shard_map/all_to_all | solution.py:628
  19.5 7.4 %copy-start.1 = (bf16[1152,2048]{1,0:T(8,128)(2,1)}, bf16[1152,2048]{1,0:T(8,128)(2,1)S(1)}, u32[]{:S(2)}) copy-start(bf16[1152,2048]{1,0:T(8,128)(2,1)S(1)} %ordered_rows.1) | copy-start | bytes 14155780
  19.5 4.8 %copy-start.31 = (bf16[1,2048,512]{2,1,0:T(8,128)(2,1)S(1)}, bf16[1,2048,512]{2,1,0:T(8,128)(2,1)}, u32[]{:S(2)}) copy-start(bf16[1,2048,512]{2,1,0:T(8,128)(2,1)} %param.19) | copy-start | bytes 6291460
  24.2 2.6 %copy-start.33 = (bf16[1,2048,512]{2,1,0:T(8,128)(2,1)S(1)}, bf16[1,2048,512]{2,1,0:T(8,128)(2,1)}, u32[]{:S(2)}) copy-start(bf16[1,2048,512]{2,1,0:T(8,128)(2,1)} %param.18) | copy-start | bytes 6291460
  48.4 5.0 %collective-permute-start = (bf16[64,144,128]{2,1,0:T(8,128)(2,1)S(1)}, bf16[64,144,128]{2,1,0:T(8,128)(2,1)S(1)}, u32[]{:S(2)}, u32[]{:S(2)}) collective-permute-start(bf16[64,144,128]{2,1,0:T(8,128)(2,1)S(1)} %all-to-all-done.mine_ref), channel_id=1, source_target_pairs={{0,1},{1,0},{2,3},{3,2},{4,5},{5,4},{6,7},{7,6},{8,9},{9,8},{10,11... | collective-permute-start | bytes 7077896 | tf_op jit(solution)/shard_map/ppermute | solution.py:625
  50.0 3.4 %copy-start.6 = (f32[1152,512]{1,0:T(8,128)S(1)}, f32[1152,512]{1,0:T(8,128)}, u32[]{:S(2)}) copy-start(f32[1152,512]{1,0:T(8,128)} %get-tuple-element.68.a1_ref) | copy-start | bytes 7077892
  50.0 3.4 %copy-start.7 = (f32[1152,512]{1,0:T(8,128)S(1)}, f32[1152,512]{1,0:T(8,128)}, u32[]{:S(2)}) copy-start(f32[1152,512]{1,0:T(8,128)} %get-tuple-element.69.a2_ref) | copy-start | bytes 7077892
  53.4 2.4 %copy-start.32 = (bf16[1,2048,512]{2,1,0:T(8,128)(2,1)S(1)}, bf16[1,2048,512]{2,1,0:T(8,128)(2,1)}, u32[]{:S(2)}) copy-start(bf16[1,2048,512]{2,1,0:T(8,128)(2,1)} %param.19) | copy-start | bytes 6291460
  55.8 3.7 %copy-start.4 = (bf16[1152,1024]{1,0:T(8,128)(2,1)}, bf16[1152,1024]{1,0:T(8,128)(2,1)S(1)}, u32[]{:S(2)}) copy-start(bf16[1152,1024]{1,0:T(8,128)(2,1)S(1)} %get-tuple-element.75.other_ref) | copy-start | bytes 7077892
  55.8 4.3 %copy-start.35 = (bf16[1152,512]{1,0:T(8,128)(2,1)}, bf16[1152,512]{1,0:T(8,128)(2,1)S(1)}, u32[]{:S(2)}) copy-start(bf16[1152,512]{1,0:T(8,128)(2,1)S(1)} %get-tuple-element.78.ug_ref) | copy-start | bytes 3538948
  55.8 4.3 %copy-start.37 = (bf16[1152,512]{1,0:T(8,128)(2,1)}, bf16[1152,512]{1,0:T(8,128)(2,1)S(1)}, u32[]{:S(2)}) copy-start(bf16[1152,512]{1,0:T(8,128)(2,1)S(1)} %get-tuple-element.77.gg_ref) | copy-start | bytes 3538948
  59.6 4.8 %collective-permute-start.1 = (bf16[64,144,128]{2,1,0:T(8,128)(2,1)S(1)}, bf16[64,144,128]{2,1,0:T(8,128)(2,1)S(1)}, u32[]{:S(2)}, u32[]{:S(2)}) collective-permute-start(bf16[64,144,128]{2,1,0:T(8,128)(2,1)S(1)} %span_half.3), channel_id=1, source_target_pairs={{0,1},{1,0},{2,3},{3,2},{4,5},{5,4},{6,7},{7,6},{8,9},{9,8},{10,11... | collective-permute-start | bytes 7077896 | tf_op jit(solution)/shard_map/ppermute | solution.py:625
  66.5 39.8 %all-to-all-start.1 = ((bf16[64,144,128]{2,1,0:T(8,128)(2,1)}), bf16[64,144,128]{2,1,0:T(8,128)(2,1)S(1)}, u32[]{:S(2)}, u32[]{:S(2)}) async-start(bf16[64,144,128]{2,1,0:T(8,128)(2,1)} %add_convert_fusion), calls=%async_computation.1 | async-start | bytes 4718592 | tf_op jit(solution)/shard_map/all_to_all | solution.py:655
  76.2 4.9 %copy-start.38 = (bf16[1152,512]{1,0:T(8,128)(2,1)S(1)}, bf16[1152,512]{1,0:T(8,128)(2,1)}, u32[]{:S(2)}) copy-start(bf16[1152,512]{1,0:T(8,128)(2,1)} %copy-done.37) | copy-start | bytes 3538948
  76.2 11.6 %slice-start = ((s8[4718592]{0:T(1024)(128)(4,1)}), s8[4194304]{0:T(1024)(128)(4,1)S(1)}, s32[]{:S(2)}) async-start(s8[4718592]{0:T(1024)(128)(4,1)} %bitcast.25), calls=%async_computation.4 | async-start | bytes 8388608
  81.1 6.7 %slice-start.1 = ((s8[4718592]{0:T(1024)(128)(4,1)}), s8[524288]{0:T(1024)(128)(4,1)S(1)}, s32[]{:S(2)}) async-start(s8[4718592]{0:T(1024)(128)(4,1)} %bitcast.25), calls=%async_computation.5 | async-start | bytes 1048576
  81.1 6.7 %copy-start.36 = (bf16[1152,512]{1,0:T(8,128)(2,1)S(1)}, bf16[1152,512]{1,0:T(8,128)(2,1)}, u32[]{:S(2)}) copy-start(bf16[1152,512]{1,0:T(8,128)(2,1)} %copy-done.35) | copy-start | bytes 3538948
  87.8 18.5 %copy-start.10 = (bf16[224,2048]{1,0:T(8,128)(2,1)S(1)}, bf16[224,2048]{1,0:T(8,128)(2,1)}, u32[]{:S(2)}) copy-start(bf16[224,2048]{1,0:T(8,128)(2,1)} %og_ref.1) | copy-start | bytes 2752516
  91.9 19.6 %copy-start.15 = (f32[224,16]{1,0:T(8,128)S(1)}, f32[224,16]{1,0:T(8,128)}, u32[]{:S(2)}) copy-start(f32[224,16]{1,0:T(8,128)} %copy-done.14) | copy-start | bytes 43012
  91.9 19.6 %copy-start.24 = (bf16[224,256]{1,0:T(8,128)(2,1)S(1)}, bf16[224,256]{1,0:T(8,128)(2,1)}, u32[]{:S(2)}) copy-start(bf16[224,256]{1,0:T(8,128)(2,1)} %q_far.1) | copy-start | bytes 344068
  107.3 4.2 %copy-start.8 = (bf16[2048,512]{1,0:T(8,128)(2,1)S(1)}, bf16[2048,512]{1,0:T(8,128)(2,1)}, u32[]{:S(2)}) copy-start(bf16[2048,512]{1,0:T(8,128)(2,1)} %ow_ref.1) | copy-start | bytes 6291460
  107.3 4.2 %copy-start.13 = (f32[224,512]{1,0:T(8,128)S(1)}, f32[224,512]{1,0:T(8,128)}, u32[]{:S(2)}) copy-start(f32[224,512]{1,0:T(8,128)} %copy-done.12) | copy-start | bytes 1376260
  107.3 4.3 %copy-start.19 = (bf16[224,512]{1,0:T(8,128)(2,1)S(1)}, bf16[224,512]{1,0:T(8,128)(2,1)}, u32[]{:S(2)}) copy-start(bf16[224,512]{1,0:T(8,128)(2,1)} %gate_ref.3) | copy-start | bytes 688132
  109.6 1.9 %collective-permute-start.2 = (bf16[224,1024]{1,0:T(8,128)(2,1)S(1)}, bf16[224,1024]{1,0:T(8,128)(2,1)S(1)}, u32[]{:S(2)}, u32[]{:S(2)}) collective-permute-start(bf16[224,1024]{1,0:T(8,128)(2,1)S(1)} %combine.1.mine_ref), channel_id=1, source_target_pairs={{0,1},{1,0},{2,3},{3,2},{4,5},{5,4},{6,7},{7,6},{8,9},{9,8},{10,11... | collective-permute-start | bytes 1376264 | tf_op jit(solution)/shard_map/ppermute | solution.py:625
  114.3 16.4 %all-to-all-start.2 = ((bf16[64,16,128]{2,1,0:T(8,128)(2,1)}), bf16[64,16,128]{2,1,0:T(8,128)(2,1)S(1)}, u32[]{:S(2)}, u32[]{:S(2)}) async-start(bf16[64,16,128]{2,1,0:T(8,128)(2,1)} %get-tuple-element.86), calls=%async_computation.2 | async-start | bytes 524288 | tf_op jit(solution)/shard_map/all_to_all | solution.py:689
  119.8 6.2 %copy-start.43 = (bf16[224,512]{1,0:T(8,128)(2,1)S(1)}, bf16[224,512]{1,0:T(8,128)(2,1)}, u32[]{:S(2)}) copy-start(bf16[224,512]{1,0:T(8,128)(2,1)} %copy-done.42) | copy-start | bytes 688132
  132.0 40.6 %copy-start.11 = (f32[224,512]{1,0:T(8,128)S(1)}, f32[224,512]{1,0:T(8,128)}, u32[]{:S(2)}) copy-start(f32[224,512]{1,0:T(8,128)} %get-tuple-element.100.dv_ref) | copy-start | bytes 1376260
  132.0 40.6 %copy-start.17 = (f32[1,8,64,128]{3,2,1,0:T(8,128)S(1)}, f32[1,8,64,128]{3,2,1,0:T(8,128)}, u32[]{:S(2)}) copy-start(f32[1,8,64,128]{3,2,1,0:T(8,128)} %param.26) | copy-start | bytes 786436
  132.0 40.5 %copy-start.21 = (bf16[224,512]{1,0:T(8,128)(2,1)S(1)}, bf16[224,512]{1,0:T(8,128)(2,1)}, u32[]{:S(2)}) copy-start(bf16[224,512]{1,0:T(8,128)(2,1)} %v_ref.2) | copy-start | bytes 688132
  132.0 40.5 %copy-start.22 = (f32[224,256]{1,0:T(8,128)S(1)}, f32[224,256]{1,0:T(8,128)}, u32[]{:S(2)}) copy-start(f32[224,256]{1,0:T(8,128)} %get-tuple-element.101.dk_ref) | copy-start | bytes 688132
  132.0 40.5 %copy-start.26 = (bf16[224,256]{1,0:T(8,128)(2,1)S(1)}, bf16[224,256]{1,0:T(8,128)(2,1)}, u32[]{:S(2)}) copy-start(bf16[224,256]{1,0:T(8,128)(2,1)} %k_ref.3) | copy-start | bytes 344068
  132.0 40.5 %copy-start.29 = (f32[224,8]{1,0:T(8,128)S(1)}, f32[224,8]{1,0:T(8,128)}, u32[]{:S(2)}) copy-start(f32[224,8]{1,0:T(8,128)} %get-tuple-element.102.diff_ref) | copy-start | bytes 21508
  (20 other events, 27.2 us)

commit v3 on v2

--- a/solution.py
+++ b/solution.py
@@ -229,18 +229,21 @@
     e0, s0, e1, s1 = (meta[:, k : k + 1] for k in range(4))
     m0 = jnp.where(s0 < MAIN, e0 * MAIN + s0, -1)
     m1 = jnp.where(s1 < MAIN, e1 * MAIN + s1, -1)
-    t0 = jnp.where(s0 >= MAIN, e0 * 16 + (s0 - MAIN) * 8, -100)
-    t1 = jnp.where(s1 >= MAIN, e1 * 16 + (s1 - MAIN) * 8, -100)
+    t0 = jnp.where(s0 >= MAIN, e0 * TAIL + s0 - MAIN, -1)
+    t1 = jnp.where(s1 >= MAIN, e1 * TAIL + s1 - MAIN, -1)
     lanes = iota((TOK, 1024), 1)
     pick = jnp.where((lanes == m0) | (lanes == m1), 1.0, 0.0).astype(BF)
     tail = ret_ref[:, 16 * COLS : MSG, :].reshape(1024, 128)
-    d0, d1 = lanes - t0, lanes - t1
+    few = iota((TOK, 128), 1)
+    tail_pick = jnp.where((few == t0) | (few == t1), 1.0, 0.0).astype(BF)
+    at = iota((128, 1024), 1) - tail_rows((128, 1024), 0)
 
     for c in range(0, COLS, 2):
         pair = [ret_ref[:, 16 * k : 16 * k + 16, :].reshape(1024, 128) for k in (c, c + 1)]
         moe = dot(pick, jnp.concatenate(pair, axis=1))
-        masks = [jnp.where((d0 == k) | (d1 == k), 1.0, 0.0).astype(BF) for k in (c, c + 1)]
-        moe = moe + jnp.concatenate([dot(m, tail) for m in masks], axis=1)
+        masks = [jnp.where(at == k, 1.0, 0.0).astype(BF) for k in (c, c + 1)]
+        rest = jnp.concatenate([dot(m, tail).astype(BF) for m in masks], axis=1)
+        moe = moe + dot(tail_pick, rest)
         own = og_ref[:, pl.ds(pl.multiple_of(tp_ref[0] * HALF + c * 128, 256), 256)]
         out_ref[:, 128 * c : 128 * c + 256] = (own.astype(F32) + moe).astype(BF)
 
@@ -412,7 +415,8 @@
 
 
 def forward_kernel(
-    v_ref, k_ref, q_ref, decay_ref, gate_ref, e_ref, routes_ref, core_ref, mixed_ref, meta_ref, fade_ref
+    v_ref, k_ref, q_ref, decay_ref, gate_ref, e_ref, routes_ref,
+    core_ref, mixed_ref, meta_ref, fade_ref, cum_ref,
 ):
     r0, r1, f0, f1 = slots(routes_ref[...])
     zero = jnp.zeros((4, TOK), F32)
@@ -420,6 +424,8 @@
     eye = jnp.where(iota((TOK, TOK), 0) == iota((TOK, TOK), 1), 1.0, 0.0).astype(BF)
     meta_ref[...] = dot(eye, table, NT)
     cum, cum_t = decay_sums(decay_ref[...])
+    cum_ref[...] = cum
+    fade_ref[:, 2 * HEADS : 3 * HEADS] = cum_t
     fade_ref[:, 0:HEADS] = jnp.exp(cum_t)
     fade_ref[:, HEADS : 2 * HEADS] = jnp.exp(cum_t[TOK - 1 : TOK, :] - cum_t)
     for g in range(GROUPS):
@@ -494,24 +500,25 @@
 
 
 def backward_kernel(
-    v_far, k_far, q_far, decay_far, e_far, core_far, dcore_far,
+    v_far, k_far, q_far, cum_far, e_far, core_far, dcore_far, fade_far,
     dv_far, dk_far, dq_far, diff_far,
-    v_ref, k_ref, q_ref, decay_ref, e_ref, core_ref, dcore_ref,
+    v_ref, k_ref, q_ref, cum_ref, e_ref, core_ref, dcore_ref, fade_ref,
     dv_ref, dk_ref, dq_ref, diff_ref, sems,
 ):
     load(
         (
-            (decay_far, decay_ref),
+            (cum_far, cum_ref),
+            (fade_far, fade_ref),
             (q_far, q_ref),
             (k_far, k_ref),
+            (dcore_far, dcore_ref),
             (v_far, v_ref),
             (e_far, e_ref),
-            (dcore_far, dcore_ref),
             (core_far, core_ref),
         ),
         sems,
     )
-    cum, cum_t = decay_sums(decay_ref[...])
+    cum, cum_t = cum_ref[...], fade_ref[:, 2 * HEADS : 3 * HEADS]
     causal = iota((TOK, TOK), 0) >= iota((TOK, TOK), 1)
     lane = iota((TOK, HEADS), 1)
 
@@ -636,16 +643,22 @@
     act = (silu * up_pre).astype(BF)
     a1 = up_pre * sig * (1.0 + gate_pre * (1.0 - sig))
     _, later_values = lax.optimization_barrier((message, values))
-    core, mixer_out, meta, fade = call(
+    core, mixer_out, meta, fade, cum = call(
         forward_kernel,
-        [sds((TOK, HEADS * HD), F32), sds((TOK, HEADS * HD), BF), sds((TOK, 8), F32), sds((TOK, 16), F32)],
+        [
+            sds((TOK, HEADS * HD), F32),
+            sds((TOK, HEADS * HD), BF),
+            sds((TOK, 8), F32),
+            sds((TOK, 3 * HEADS), F32),
+            sds((HEADS, TOK), F32),
+        ],
         (later_values, key_side, query_side, decay_log, gate_in, entry, routes.T),
         10**9,
         10**6,
         name="mixer_forward",
     )
-    moved, rows, act, a1, silu, core, mixer_out, meta, fade = lax.optimization_barrier(
-        (moved, rows, act, a1, silu, core, mixer_out, meta, fade)
+    moved, rows, act, a1, silu, core, mixer_out, meta, fade, cum = lax.optimization_barrier(
+        (moved, rows, act, a1, silu, core, mixer_out, meta, fade, cum)
     )
 
     arrived, gate_grad, up_grad = hidden_grads(tp, moved, swap(moved), down_w, a1, silu)
@@ -695,7 +708,7 @@
             sds((TOK, GROUPS * NS), BF),
             sds((TOK, HEADS), F32),
         ],
-        (values, key_side, query_side, decay_log, entry, core, dcore),
+        (values, key_side, query_side, cum, entry, core, dcore, fade),
         2 * 10**9,
         10**6,
         scratch=[
@@ -706,13 +719,14 @@
             pltpu.VMEM((HEADS, HD, NS), F32),
             pltpu.VMEM((TOK, HEADS * HD), F32),
             pltpu.VMEM((TOK, HEADS * HD), F32),
+            pltpu.VMEM((TOK, 3 * HEADS), F32),
             pltpu.VMEM((TOK, HEADS * HD), F32),
             pltpu.VMEM((TOK, GROUPS * NS), F32),
             pltpu.VMEM((TOK, GROUPS * NS), BF),
             pltpu.VMEM((TOK, HEADS), F32),
-            pltpu.SemaphoreType.DMA((7,)),
+            pltpu.SemaphoreType.DMA((8,)),
         ],
-        hbm_ins=tuple(range(7)),
+        hbm_ins=tuple(range(8)),
         hbm_outs=tuple(range(4)),
         limit=60,
         name="mixer_backward",

time: 176 us -> 173 us (0.983)
    unnamed x92 -> x96, local copies, waits for them, and re-layouts: 14.4 us -> 13.8 us
where the time goes in v3:
time: 173 us
  Pallas kernels  38.8 us (22%)
  blocking collectives  38.1 us (22%)
  waiting for transfers between devices  36.2 us (21%)
  starting transfers between devices  24.1 us (14%)
  matrix products  18.4 us (11%)
  local copies, waits for them, and re-layouts  13.8 us (8%)
  other arithmetic  2.18 us (1%)
    pallas_call x15, Pallas kernels, call(): pl.pallas_call(kernel, out_shape=outs, in_specs=in_specs, out_specs=[far...  38.8 us
    all_to_all x1, blocking collectives, per_device(): lax.all_to_all(message, SP, split_axis=0, concat_axis=0, tiled=True)  38.1 us
    all_to_all x1, waiting for transfers between devices, per_device(): moved = lax.all_to_all(message, SP, split_axis=0, concat_axis=0, tiled=True)  15.9 us
    all_to_all x1, waiting for transfers between devices, per_device(): returned = lax.all_to_all(back, SP, split_axis=0, concat_axis=0, tiled=True)  14.4 us
    unnamed x96, local copies, waits for them, and re-layouts  13.8 us
    all_to_all x1, starting transfers between devices, per_device(): moved = lax.all_to_all(message, SP, split_axis=0, concat_axis=0, tiled=True)  11.5 us
    dot_general x2, matrix products, dot(): return lax.dot_general(a, b, dims, preferred_element_type=F32)  10.8 us
    all_to_all x1, starting transfers between devices, per_device(): returned = lax.all_to_all(back, SP, split_axis=0, concat_axis=0, tiled=True)  6.35 us
  transfers between devices with their start and end apart: 6, of which 5 were waited for; matrix products, arithmetic and copies ran while one was open for 11% of the time, Pallas kernels for 12%

profile of v3, /device:TPU:0, one launch (start us, length us, event | category | flops | bytes accessed | tf_op | source)
XLA Modules:
  0.0 172.8 jit_solution(17565072549223374481)
XLA Ops:
  0.6 3.5 %dispatch.1 = bf16[64,144,128]{2,1,0:T(8,128)(2,1)} custom-call(s32[1]{0:T(128)} %bitcast.tp_ref.half_ref, s32[2,224]{1,0:T(2,128)} %bitcast.36, f32[2,224]{1,0:T(2,128)} %bitcast.39, bf16[224,2048]{1,0:T(8,128)(2,1)} %og_ref.1), custom_call_target="tpu_custom_call" | custom-call | flops 1000000000 | bytes 3000000 | tf_op jit(solution)/shard_map/dispatch/pallas_call | solution.py:181
  4.1 11.5 %all-to-all-start = ((bf16[64,144,128]{2,1,0:T(8,128)(2,1)}), bf16[64,144,128]{2,1,0:T(8,128)(2,1)S(1)}, u32[]{:S(2)}, u32[]{:S(2)}) async-start(bf16[64,144,128]{2,1,0:T(8,128)(2,1)} %dispatch.1), calls=%async_computation | async-start | bytes 4718592 | tf_op jit(solution)/shard_map/all_to_all | solution.py:635
  15.7 2.3 %copy-done = bf16[1,64,18,2048]{3,1,2,0:T(8,128)(2,1)S(1)} copy-done((bf16[1,64,18,2048]{3,1,2,0:T(8,128)(2,1)S(1)}, bf16[1,64,18,2048]{3,1,2,0:T(8,128)(2,1)}, u32[]{:S(2)}) %copy-start) | copy-done | bytes 4718616
  18.1 1.4 ordered_rows.1
  19.6 1.9 %mixer_forward.1 = (f32[224,512]{1,0:T(8,128)S(1)}, bf16[224,512]{1,0:T(8,128)(2,1)S(1)}, f32[224,8]{1,0:T(8,128)S(1)}, f32[224,24]{1,0:T(8,128)S(1)}, f32[8,224]{1,0:T(8,128)S(1)}) custom-call(bf16[224,512]{1,0:T(8,128)(2,1)S(1)} %copy-done.21, bf16[224,256]{1,0:T(8,128)(2,1)S(1)} %copy-done.26, bf16[224,256]{1,0:T(8,128)(2,1)S(1)} %copy-done.24, ...), custom_call_target="tpu_custom_call" | custom-call | flops 1000000000 | bytes 1000000 | tf_op jit(solution)/shard_map/mixer_forward/pallas_call | solution.py:181
  24.9 2.6 %fusion.1 = f32[1152,512]{1,0:T(8,128)S(1)} fusion(bf16[1152,2048]{1,0:T(8,128)(2,1)S(1)} %ordered_rows.1, bf16[1,2048,512]{2,1,0:T(8,128)(2,1)S(1)} %copy-done.32), kind=kOutput, calls=%fused_computation.7 | convolution fusion | flops 2415919104 | bytes 9175040 | tf_op jit(solution)/shard_map/dot_general | solution.py:640
  27.5 5.1 %add_multiply_fusion = (f32[1152,512]{1,0:T(8,128)}, bf16[1152,512]{1,0:T(8,128)(2,1)S(1)}, f32[1152,512]{1,0:T(8,128)}) fusion(f32[1152,512]{1,0:T(8,128)S(1)} %fusion.1, bf16[1152,2048]{1,0:T(8,128)(2,1)S(1)} %ordered_rows.1, bf16[1,2048,512]{2,1,0:T(8,128)(2,1)S(1)} %copy-done.34), kind=kOutput, calls=%fused_computation.3 | convolution fusion | flops 2422407168 | bytes 15073280 | tf_op jit(solution)/shard_map/dot_general | solution.py:639
  32.6 15.9 %all-to-all-done.mine_ref = bf16[64,144,128]{2,1,0:T(8,128)(2,1)S(1)} async-done(((bf16[64,144,128]{2,1,0:T(8,128)(2,1)}), bf16[64,144,128]{2,1,0:T(8,128)(2,1)S(1)}, u32[]{:S(2)}, u32[]{:S(2)}) %all-to-all-start) | async-done | bytes 2359328 | tf_op jit(solution)/shard_map/all_to_all | solution.py:635
  48.5 1.6 copy-done.9
  50.1 2.0 %hidden_first.1 = (bf16[1152,1024]{1,0:T(8,128)(2,1)S(1)}, f32[1152,512]{1,0:T(8,128)S(1)}) custom-call(s32[1]{0:T(128)} %bitcast.tp_ref.half_ref, bf16[64,144,128]{2,1,0:T(8,128)(2,1)S(1)} %all-to-all-done.mine_ref, bf16[512,2048]{1,0:T(8,128)(2,1)S(1)} %bitcast.27), custom_call_target="tpu_custom_call" | custom-call | flops 2000000000 | bytes 10000000 | tf_op jit(solution)/shard_map/hidden_first/pallas_call | solution.py:181
  52.1 1.4 copy-done.2
  53.5 2.3 %hidden_second.1 = (bf16[1152,1024]{1,0:T(8,128)(2,1)S(1)}, bf16[1152,512]{1,0:T(8,128)(2,1)S(1)}, bf16[1152,512]{1,0:T(8,128)(2,1)S(1)}) custom-call(s32[1]{0:T(128)} %bitcast.tp_ref.half_ref, bf16[64,144,128]{2,1,0:T(8,128)(2,1)S(1)} %collective-permute-done.other_ref, bf16[512,2048]{1,0:T(8,128)(2,1)S(1)} %bitcast.28, ...), custom_call_target="tpu_custom_call" | custom-call | flops 2000000000 | bytes 10000000 | tf_op jit(solution)/shard_map/hidden_second/pallas_call | solution.py:181
  55.9 3.7 %span_half.3 = bf16[64,144,128]{2,1,0:T(8,128)(2,1)S(1)} custom-call(s32[1]{0:T(128)} %bitcast.tp_ref.half_ref, bf16[1152,512]{1,0:T(8,128)(2,1)S(1)} %get-tuple-element.80.gg_ref, bf16[1152,512]{1,0:T(8,128)(2,1)S(1)} %get-tuple-element.81.ug_ref, bf16[2048,512]{1,0:T(8,128)(2,1)S(1)} %bitcast.34, bf16[2048,512]{1,0:T(8,128)(2,1)S(1)} %bitcast.32), custom_call_target="tpu_custom_call" | custom-call | flops 4000000000 | bytes 10000000 | tf_op jit(solution)/shard_map/span_half/pallas_call | solution.py:181
  60.2 3.7 %span_half.2 = bf16[64,144,128]{2,1,0:T(8,128)(2,1)S(1)} custom-call(s32[1]{0:T(128)} %bitcast.tp_ref.half_ref, bf16[1152,512]{1,0:T(8,128)(2,1)S(1)} %get-tuple-element.80.gg_ref, bf16[1152,512]{1,0:T(8,128)(2,1)S(1)} %get-tuple-element.81.ug_ref, bf16[2048,512]{1,0:T(8,128)(2,1)S(1)} %bitcast.35, bf16[2048,512]{1,0:T(8,128)(2,1)S(1)} %bitcast.33), custom_call_target="tpu_custom_call" | custom-call | flops 4000000000 | bytes 10000000 | tf_op jit(solution)/shard_map/span_half/pallas_call | solution.py:181
  64.3 2.2 %add_convert_fusion = bf16[64,144,128]{2,1,0:T(8,128)(2,1)} fusion(bf16[64,144,128]{2,1,0:T(8,128)(2,1)S(1)} %collective-permute-done.1, bf16[64,144,128]{2,1,0:T(8,128)(2,1)S(1)} %span_half.2), kind=kLoop, calls=%fused_computation | loop fusion | flops 4718592 | bytes 7077888 | tf_op jit(solution)/shard_map/convert_element_type | solution.py:667
  66.5 6.4 %all-to-all-start.1 = ((bf16[64,144,128]{2,1,0:T(8,128)(2,1)}), bf16[64,144,128]{2,1,0:T(8,128)(2,1)S(1)}, u32[]{:S(2)}, u32[]{:S(2)}) async-start(bf16[64,144,128]{2,1,0:T(8,128)(2,1)} %add_convert_fusion), calls=%async_computation.1 | async-start | bytes 4718592 | tf_op jit(solution)/shard_map/all_to_all | solution.py:668
  72.9 1.7 copy-done.3
  74.5 1.7 copy-done.5
  76.2 4.9 %down_grad.1 = bf16[512,2048]{1,0:T(8,128)(2,1)} custom-call(s32[1]{0:T(128)} %bitcast.tp_ref.half_ref, bf16[1152,512]{1,0:T(8,128)(2,1)S(1)} %get-tuple-element.76.act_ref, bf16[1152,1024]{1,0:T(8,128)(2,1)S(1)} %copy-done.3, bf16[1152,1024]{1,0:T(8,128)(2,1)S(1)} %copy-done.5), custom_call_target="tpu_custom_call" | custom-call | flops 2000000000 | bytes 10000000 | tf_op jit(solution)/shard_map/down_grad/pallas_call | solution.py:181
  81.1 6.6 %convolution_convert_fusion.1 = bf16[2048,512]{1,0:T(8,128)(2,1)} fusion(bf16[1152,2048]{1,0:T(8,128)(2,1)} %copy-done.1, bf16[1152,512]{1,0:T(8,128)(2,1)S(1)} %copy-done.39), kind=kOutput, calls=%fused_computation.2 | convolution fusion | flops 2416967680 | bytes 7995392 | tf_op jit(solution)/shard_map/dot_general | solution.py:43
  87.8 4.1 %convolution_convert_fusion = bf16[2048,512]{1,0:T(8,128)(2,1)} fusion(bf16[1152,2048]{1,0:T(8,128)(2,1)S(1)} %bitcast.26, bf16[1152,512]{1,0:T(8,128)(2,1)S(1)} %copy-done.37), kind=kOutput, calls=%fused_computation.1 | convolution fusion | flops 2416967680 | bytes 7995392 | tf_op jit(solution)/shard_map/dot_general | solution.py:43
  91.9 14.4 %all-to-all-done.1.ret_ref = bf16[64,144,128]{2,1,0:T(8,128)(2,1)S(1)} async-done(((bf16[64,144,128]{2,1,0:T(8,128)(2,1)}), bf16[64,144,128]{2,1,0:T(8,128)(2,1)S(1)}, u32[]{:S(2)}, u32[]{:S(2)}) %all-to-all-start.1) | async-done | bytes 2359328 | tf_op jit(solution)/shard_map/all_to_all | solution.py:668
  107.3 1.6 combine.1.mine_ref
  108.9 1.8 %collective-permute-done.2.other_ref = bf16[224,1024]{1,0:T(8,128)(2,1)S(1)} collective-permute-done((bf16[224,1024]{1,0:T(8,128)(2,1)S(1)}, bf16[224,1024]{1,0:T(8,128)(2,1)S(1)}, u32[]{:S(2)}, u32[]{:S(2)}) %collective-permute-start.2) | collective-permute-done | bytes 458784 | tf_op jit(solution)/shard_map/ppermute | solution.py:632
  110.8 2.0 %mixer_cotangent.1 = (bf16[224,2048]{1,0:T(8,128)(2,1)}, f32[224,512]{1,0:T(8,128)S(1)}, bf16[224,512]{1,0:T(8,128)(2,1)}, bf16[64,16,128]{2,1,0:T(8,128)(2,1)}) custom-call(s32[1]{0:T(128)} %bitcast.tp_ref.half_ref, bf16[224,1024]{1,0:T(8,128)(2,1)S(1)} %combine.1.mine_ref, bf16[224,1024]{1,0:T(8,128)(2,1)S(1)} %collective-permute-done.2.other_ref, ...), custom_call_target="tpu_custom_call" | custom-call | flops 1000000000 | bytes 5000000 | tf_op jit(solution)/shard_map/mixer_cotangent/pallas_call | solution.py:181
  113.6 5.5 %all-to-all-start.2 = ((bf16[64,16,128]{2,1,0:T(8,128)(2,1)}), bf16[64,16,128]{2,1,0:T(8,128)(2,1)S(1)}, u32[]{:S(2)}, u32[]{:S(2)}) async-start(bf16[64,16,128]{2,1,0:T(8,128)(2,1)} %get-tuple-element.89), calls=%async_computation.2 | async-start | bytes 524288 | tf_op jit(solution)/shard_map/all_to_all | solution.py:702
  119.1 5.9 %mixer_backward.1 = (f32[224,512]{1,0:T(8,128)}, f32[224,256]{1,0:T(8,128)}, bf16[224,256]{1,0:T(8,128)(2,1)}, f32[224,8]{1,0:T(8,128)}) custom-call(bf16[224,512]{1,0:T(8,128)(2,1)} %v_ref.2, bf16[224,256]{1,0:T(8,128)(2,1)} %k_ref.3, bf16[224,256]{1,0:T(8,128)(2,1)} %q_far.1, f32[8,224]{1,0:T(8,128)} %copy-done.45, f32[8,64,128]{2,1,0:T(8,128)} %bitcast.29, ...), custom_call_target="tpu_custom_call" | custom-call | flops 2000000000 | bytes 1000000 | tf_op jit(solution)/shard_map/mixer_backward/pallas_call | solution.py:181
  125.0 1.4 shares.1.shares_ref
  126.4 3.6 %all-to-all-done.2.in_ref = bf16[64,16,128]{2,1,0:T(8,128)(2,1)S(1)} async-done(((bf16[64,16,128]{2,1,0:T(8,128)(2,1)}), bf16[64,16,128]{2,1,0:T(8,128)(2,1)S(1)}, u32[]{:S(2)}, u32[]{:S(2)}) %all-to-all-start.2) | async-done | bytes 262176 | tf_op jit(solution)/shard_map/all_to_all | solution.py:702
  130.0 1.3 state_chain.1
  131.3 38.1 %all_to_all.20.in_ref = bf16[64,136,128]{2,1,0:T(8,128)(2,1)S(1)} all-to-all(bf16[64,136,128]{2,1,0:T(8,128)(2,1)S(1)} %state_chain.1), channel_id=1, replica_groups=mesh['sp_0'=4,'sp_1'=4,'sp_2'=4,'tp'=2] {'sp_0','sp_1','sp_2'}, dimensions={0} | all-to-all | bytes 4456448 | tf_op jit(solution)/shard_map/all_to_all | solution.py:757
  170.4 2.3 %mixer_ending.1 = (bf16[224,512]{1,0:T(8,128)(2,1)}, bf16[224,256]{1,0:T(8,128)(2,1)}, f32[8,224]{1,0:T(8,128)}) custom-call(bf16[64,136,128]{2,1,0:T(8,128)(2,1)S(1)} %all_to_all.20.in_ref, bf16[224,512]{1,0:T(8,128)(2,1)S(1)} %copy-done.22, bf16[224,256]{1,0:T(8,128)(2,1)S(1)} %copy-done.27, f32[224,24]{1,0:T(8,128)S(1)} %copy-done.16, ...), custom_call_target="tpu_custom_call" | custom-call | flops 1000000000 | bytes 1000000 | tf_op jit(solution)/shard_map/mixer_ending/pallas_call | solution.py:181
  (98 shorter events, 7.3 us)
Async XLA Ops:
  4.1 44.3 %all-to-all-start = ((bf16[64,144,128]{2,1,0:T(8,128)(2,1)}), bf16[64,144,128]{2,1,0:T(8,128)(2,1)S(1)}, u32[]{:S(2)}, u32[]{:S(2)}) async-start(bf16[64,144,128]{2,1,0:T(8,128)(2,1)} %dispatch.1), calls=%async_computation | async-start | bytes 4718592 | tf_op jit(solution)/shard_map/all_to_all | solution.py:635
  19.5 8.0 %copy-start.1 = (bf16[1152,2048]{1,0:T(8,128)(2,1)}, bf16[1152,2048]{1,0:T(8,128)(2,1)S(1)}, u32[]{:S(2)}) copy-start(bf16[1152,2048]{1,0:T(8,128)(2,1)S(1)} %ordered_rows.1) | copy-start | bytes 14155780
  19.5 5.4 %copy-start.32 = (bf16[1,2048,512]{2,1,0:T(8,128)(2,1)S(1)}, bf16[1,2048,512]{2,1,0:T(8,128)(2,1)}, u32[]{:S(2)}) copy-start(bf16[1,2048,512]{2,1,0:T(8,128)(2,1)} %param.19) | copy-start | bytes 6291460
  48.5 5.0 %collective-permute-start = (bf16[64,144,128]{2,1,0:T(8,128)(2,1)S(1)}, bf16[64,144,128]{2,1,0:T(8,128)(2,1)S(1)}, u32[]{:S(2)}, u32[]{:S(2)}) collective-permute-start(bf16[64,144,128]{2,1,0:T(8,128)(2,1)S(1)} %all-to-all-done.mine_ref), channel_id=1, source_target_pairs={{0,1},{1,0},{2,3},{3,2},{4,5},{5,4},{6,7},{7,6},{8,9},{9,8},{10,11... | collective-permute-start | bytes 7077896 | tf_op jit(solution)/shard_map/ppermute | solution.py:632
  50.1 3.4 %copy-start.6 = (f32[1152,512]{1,0:T(8,128)S(1)}, f32[1152,512]{1,0:T(8,128)}, u32[]{:S(2)}) copy-start(f32[1152,512]{1,0:T(8,128)} %get-tuple-element.71.a1_ref) | copy-start | bytes 7077892
  50.1 3.4 %copy-start.7 = (f32[1152,512]{1,0:T(8,128)S(1)}, f32[1152,512]{1,0:T(8,128)}, u32[]{:S(2)}) copy-start(f32[1152,512]{1,0:T(8,128)} %get-tuple-element.72.a2_ref) | copy-start | bytes 7077892
  55.8 3.7 %copy-start.4 = (bf16[1152,1024]{1,0:T(8,128)(2,1)}, bf16[1152,1024]{1,0:T(8,128)(2,1)S(1)}, u32[]{:S(2)}) copy-start(bf16[1152,1024]{1,0:T(8,128)(2,1)S(1)} %get-tuple-element.78.other_ref) | copy-start | bytes 7077892
  55.8 4.3 %copy-start.36 = (bf16[1152,512]{1,0:T(8,128)(2,1)}, bf16[1152,512]{1,0:T(8,128)(2,1)S(1)}, u32[]{:S(2)}) copy-start(bf16[1152,512]{1,0:T(8,128)(2,1)S(1)} %get-tuple-element.81.ug_ref) | copy-start | bytes 3538948
  55.8 4.3 %copy-start.38 = (bf16[1152,512]{1,0:T(8,128)(2,1)}, bf16[1152,512]{1,0:T(8,128)(2,1)S(1)}, u32[]{:S(2)}) copy-start(bf16[1152,512]{1,0:T(8,128)(2,1)S(1)} %get-tuple-element.80.gg_ref) | copy-start | bytes 3538948
  59.6 4.7 %collective-permute-start.1 = (bf16[64,144,128]{2,1,0:T(8,128)(2,1)S(1)}, bf16[64,144,128]{2,1,0:T(8,128)(2,1)S(1)}, u32[]{:S(2)}, u32[]{:S(2)}) collective-permute-start(bf16[64,144,128]{2,1,0:T(8,128)(2,1)S(1)} %span_half.3), channel_id=1, source_target_pairs={{0,1},{1,0},{2,3},{3,2},{4,5},{5,4},{6,7},{7,6},{8,9},{9,8},{10,11... | collective-permute-start | bytes 7077896 | tf_op jit(solution)/shard_map/ppermute | solution.py:632
  66.5 39.8 %all-to-all-start.1 = ((bf16[64,144,128]{2,1,0:T(8,128)(2,1)}), bf16[64,144,128]{2,1,0:T(8,128)(2,1)S(1)}, u32[]{:S(2)}, u32[]{:S(2)}) async-start(bf16[64,144,128]{2,1,0:T(8,128)(2,1)} %add_convert_fusion), calls=%async_computation.1 | async-start | bytes 4718592 | tf_op jit(solution)/shard_map/all_to_all | solution.py:668
  76.2 4.9 %copy-start.39 = (bf16[1152,512]{1,0:T(8,128)(2,1)S(1)}, bf16[1152,512]{1,0:T(8,128)(2,1)}, u32[]{:S(2)}) copy-start(bf16[1152,512]{1,0:T(8,128)(2,1)} %copy-done.38) | copy-start | bytes 3538948
  76.2 11.6 %slice-start = ((s8[4718592]{0:T(1024)(128)(4,1)}), s8[4194304]{0:T(1024)(128)(4,1)S(1)}, s32[]{:S(2)}) async-start(s8[4718592]{0:T(1024)(128)(4,1)} %bitcast.25), calls=%async_computation.4 | async-start | bytes 8388608
  81.1 6.7 %slice-start.1 = ((s8[4718592]{0:T(1024)(128)(4,1)}), s8[524288]{0:T(1024)(128)(4,1)S(1)}, s32[]{:S(2)}) async-start(s8[4718592]{0:T(1024)(128)(4,1)} %bitcast.25), calls=%async_computation.5 | async-start | bytes 1048576
  81.1 6.7 %copy-start.37 = (bf16[1152,512]{1,0:T(8,128)(2,1)S(1)}, bf16[1152,512]{1,0:T(8,128)(2,1)}, u32[]{:S(2)}) copy-start(bf16[1152,512]{1,0:T(8,128)(2,1)} %copy-done.36) | copy-start | bytes 3538948
  87.8 18.6 %copy-start.10 = (bf16[224,2048]{1,0:T(8,128)(2,1)S(1)}, bf16[224,2048]{1,0:T(8,128)(2,1)}, u32[]{:S(2)}) copy-start(bf16[224,2048]{1,0:T(8,128)(2,1)} %og_ref.1) | copy-start | bytes 2752516
  91.9 18.8 %copy-start.15 = (f32[224,24]{1,0:T(8,128)S(1)}, f32[224,24]{1,0:T(8,128)}, u32[]{:S(2)}) copy-start(f32[224,24]{1,0:T(8,128)} %copy-done.14) | copy-start | bytes 64516
  91.9 18.8 %copy-start.25 = (bf16[224,256]{1,0:T(8,128)(2,1)S(1)}, bf16[224,256]{1,0:T(8,128)(2,1)}, u32[]{:S(2)}) copy-start(bf16[224,256]{1,0:T(8,128)(2,1)} %q_far.1) | copy-start | bytes 344068
  107.3 3.5 %copy-start.8 = (bf16[2048,512]{1,0:T(8,128)(2,1)S(1)}, bf16[2048,512]{1,0:T(8,128)(2,1)}, u32[]{:S(2)}) copy-start(bf16[2048,512]{1,0:T(8,128)(2,1)} %ow_ref.1) | copy-start | bytes 6291460
  107.3 3.5 %copy-start.13 = (f32[224,512]{1,0:T(8,128)S(1)}, f32[224,512]{1,0:T(8,128)}, u32[]{:S(2)}) copy-start(f32[224,512]{1,0:T(8,128)} %copy-done.12) | copy-start | bytes 1376260
  107.3 3.5 %copy-start.20 = (bf16[224,512]{1,0:T(8,128)(2,1)S(1)}, bf16[224,512]{1,0:T(8,128)(2,1)}, u32[]{:S(2)}) copy-start(bf16[224,512]{1,0:T(8,128)(2,1)} %gate_ref.3) | copy-start | bytes 688132
  108.8 1.9 %collective-permute-start.2 = (bf16[224,1024]{1,0:T(8,128)(2,1)S(1)}, bf16[224,1024]{1,0:T(8,128)(2,1)S(1)}, u32[]{:S(2)}, u32[]{:S(2)}) collective-permute-start(bf16[224,1024]{1,0:T(8,128)(2,1)S(1)} %combine.1.mine_ref), channel_id=1, source_target_pairs={{0,1},{1,0},{2,3},{3,2},{4,5},{5,4},{6,7},{7,6},{8,9},{9,8},{10,11... | collective-permute-start | bytes 1376264 | tf_op jit(solution)/shard_map/ppermute | solution.py:632
  113.6 16.4 %all-to-all-start.2 = ((bf16[64,16,128]{2,1,0:T(8,128)(2,1)}), bf16[64,16,128]{2,1,0:T(8,128)(2,1)S(1)}, u32[]{:S(2)}, u32[]{:S(2)}) async-start(bf16[64,16,128]{2,1,0:T(8,128)(2,1)} %get-tuple-element.89), calls=%async_computation.2 | async-start | bytes 524288 | tf_op jit(solution)/shard_map/all_to_all | solution.py:702
  119.1 5.9 %copy-start.40 = (bf16[224,2048]{1,0:T(8,128)(2,1)S(1)}, bf16[224,2048]{1,0:T(8,128)(2,1)}, u32[]{:S(2)}) copy-start(bf16[224,2048]{1,0:T(8,128)(2,1)} %get-tuple-element.96.hidden_ref) | copy-start | bytes 2752516
  119.1 5.9 %copy-start.44 = (bf16[224,512]{1,0:T(8,128)(2,1)S(1)}, bf16[224,512]{1,0:T(8,128)(2,1)}, u32[]{:S(2)}) copy-start(bf16[224,512]{1,0:T(8,128)(2,1)} %copy-done.43) | copy-start | bytes 688132
  131.2 39.1 %copy-start.11 = (f32[224,512]{1,0:T(8,128)S(1)}, f32[224,512]{1,0:T(8,128)}, u32[]{:S(2)}) copy-start(f32[224,512]{1,0:T(8,128)} %get-tuple-element.104.dv_ref) | copy-start | bytes 1376260
  131.3 39.1 %copy-start.16 = (f32[224,24]{1,0:T(8,128)S(1)}, f32[224,24]{1,0:T(8,128)}, u32[]{:S(2)}) copy-start(f32[224,24]{1,0:T(8,128)} %copy-done.14) | copy-start | bytes 64516
  131.3 39.1 %copy-start.18 = (f32[1,8,64,128]{3,2,1,0:T(8,128)S(1)}, f32[1,8,64,128]{3,2,1,0:T(8,128)}, u32[]{:S(2)}) copy-start(f32[1,8,64,128]{3,2,1,0:T(8,128)} %param.26) | copy-start | bytes 786436
  131.3 39.1 %copy-start.22 = (bf16[224,512]{1,0:T(8,128)(2,1)S(1)}, bf16[224,512]{1,0:T(8,128)(2,1)}, u32[]{:S(2)}) copy-start(bf16[224,512]{1,0:T(8,128)(2,1)} %v_ref.2) | copy-start | bytes 688132
  131.3 39.1 %copy-start.23 = (f32[224,256]{1,0:T(8,128)S(1)}, f32[224,256]{1,0:T(8,128)}, u32[]{:S(2)}) copy-start(f32[224,256]{1,0:T(8,128)} %get-tuple-element.105.dk_ref) | copy-start | bytes 688132
  131.3 39.1 %copy-start.27 = (bf16[224,256]{1,0:T(8,128)(2,1)S(1)}, bf16[224,256]{1,0:T(8,128)(2,1)}, u32[]{:S(2)}) copy-start(bf16[224,256]{1,0:T(8,128)(2,1)} %k_ref.3) | copy-start | bytes 344068
  131.3 39.1 %copy-start.30 = (f32[224,8]{1,0:T(8,128)S(1)}, f32[224,8]{1,0:T(8,128)}, u32[]{:S(2)}) copy-start(f32[224,8]{1,0:T(8,128)} %get-tuple-element.106.diff_ref) | copy-start | bytes 21508
  (22 other events, 31.6 us)

commit v4 on v3

--- a/solution.py
+++ b/solution.py
@@ -445,21 +445,28 @@
     return a - hi.astype(F32)
 
 
+def own_half_kernel(
+    tp_ref, mine_ref, ow_ref, core_ref, gate_ref, part_ref, rise_ref, slope_ref
+):
+    part_ref[...] = dot(mine_ref[...], ow_ref[half_of(tp_ref), :])
+    gate = gate_ref[...].astype(F32)
+    sig = jax.nn.sigmoid(gate)
+    rise_ref[...] = gate * sig
+    slope_ref[...] = core_ref[...] * (sig * (1.0 + gate * (1.0 - sig)))
+
+
 def cotangent_kernel(
-    tp_ref, mine_ref, other_ref, ow_ref, core_ref, gate_ref, decay_ref, q_ref, fade_ref,
+    tp_ref, mine_ref, other_ref, ow_ref, part_ref, rise_ref, slope_ref, decay_ref, q_ref, fade_ref,
     hidden_ref, dcore_ref, dgate_ref, msg_ref,
 ):
     first = tp_ref[0] == 0
     x, y = mine_ref[...], other_ref[...]
-    lo, hi = jnp.where(first, x, y), jnp.where(first, y, x)
-    hidden_ref[:, :HALF] = lo
-    hidden_ref[:, HALF:] = hi
-    cot = dot(lo, ow_ref[:HALF, :]) + dot(hi, ow_ref[HALF:, :])
-    gate = gate_ref[...].astype(F32)
-    sig = jax.nn.sigmoid(gate)
-    dcore = cot * (gate * sig)
+    hidden_ref[:, :HALF] = jnp.where(first, x, y)
+    hidden_ref[:, HALF:] = jnp.where(first, y, x)
+    cot = part_ref[...] + dot(y, ow_ref[half_of(tp_ref, True), :])
+    dcore = cot * rise_ref[...]
     dcore_ref[...] = dcore
-    dgate_ref[...] = (cot * core_ref[...] * (sig * (1.0 + gate * (1.0 - sig)))).astype(BF)
+    dgate_ref[...] = (cot * slope_ref[...]).astype(BF)
     growth = fade_ref[:, 0:HEADS]
     logs = jnp.sum(decay_ref[...], axis=1, keepdims=True)
     high, low = split(logs)
@@ -676,6 +683,15 @@
     )
 
     hidden_half = combine_rows(tp, meta, returned, out_grad)
+    part, rise, slope = call(
+        own_half_kernel,
+        [sds((TOK, FH), F32)] * 3,
+        (hidden_half, out_weight, core, gate_in),
+        10**9,
+        5 * 10**6,
+        scalar=tp,
+        name="mixer_own_half",
+    )
     grad_hidden, dcore, dgate, own_state = call(
         cotangent_kernel,
         [
@@ -688,8 +704,9 @@
             hidden_half,
             swap(hidden_half),
             out_weight,
-            core,
-            gate_in,
+            part,
+            rise,
+            slope,
             decay_log,
             query_side,
             fade,

time: 173 us -> 172 us (level)
    pallas_call x15 -> x16, Pallas kernels: 38.8 us -> 39.1 us  [call(): pl.pallas_call(kernel, out_shape=outs, in_specs=in_specs, out_specs=[far...]
  transfers between devices with their start and end apart: 6 -> 6, of which waited for: 5 -> 5; matrix products, arithmetic and copies ran while one was open for 11% -> 11% of each run, Pallas kernels for 12% -> 13%
where the time goes in v4:
time: 172 us
  Pallas kernels  39.1 us (23%)
  blocking collectives  38.1 us (22%)
  waiting for transfers between devices  35.5 us (21%)
  starting transfers between devices  24.1 us (14%)
  matrix products  18.5 us (11%)
  local copies, waits for them, and re-layouts  12.9 us (8%)
  other arithmetic  2.18 us (1%)
    pallas_call x16, Pallas kernels, call(): pl.pallas_call(kernel, out_shape=outs, in_specs=in_specs, out_specs=[far...  39.1 us
    all_to_all x1, blocking collectives, per_device(): lax.all_to_all(message, SP, split_axis=0, concat_axis=0, tiled=True)  38.1 us
    all_to_all x1, waiting for transfers between devices, per_device(): moved = lax.all_to_all(message, SP, split_axis=0, concat_axis=0, tiled=True)  15.9 us
    all_to_all x1, waiting for transfers between devices, per_device(): returned = lax.all_to_all(back, SP, split_axis=0, concat_axis=0, tiled=True)  14.4 us
    unnamed x96, local copies, waits for them, and re-layouts  12.9 us
    all_to_all x1, starting transfers between devices, per_device(): moved = lax.all_to_all(message, SP, split_axis=0, concat_axis=0, tiled=True)  11.5 us
    dot_general x2, matrix products, dot(): return lax.dot_general(a, b, dims, preferred_element_type=F32)  10.8 us
    all_to_all x1, starting transfers between devices, per_device(): returned = lax.all_to_all(back, SP, split_axis=0, concat_axis=0, tiled=True)  6.35 us
  transfers between devices with their start and end apart: 6, of which 5 were waited for; matrix products, arithmetic and copies ran while one was open for 11% of the time, Pallas kernels for 13%

profile of v4, /device:TPU:0, one launch (start us, length us, event | category | flops | bytes accessed | tf_op | source)
XLA Modules:
  0.0 171.7 jit_solution(16397837535380305180)
XLA Ops:
  0.6 3.5 %dispatch.1 = bf16[64,144,128]{2,1,0:T(8,128)(2,1)} custom-call(s32[1]{0:T(128)} %bitcast.tp_ref.half_ref, s32[2,224]{1,0:T(2,128)} %bitcast.36, f32[2,224]{1,0:T(2,128)} %bitcast.39, bf16[224,2048]{1,0:T(8,128)(2,1)} %og_ref.1), custom_call_target="tpu_custom_call" | custom-call | flops 1000000000 | bytes 3000000 | tf_op jit(solution)/shard_map/dispatch/pallas_call | solution.py:181
  4.1 11.5 %all-to-all-start = ((bf16[64,144,128]{2,1,0:T(8,128)(2,1)}), bf16[64,144,128]{2,1,0:T(8,128)(2,1)S(1)}, u32[]{:S(2)}, u32[]{:S(2)}) async-start(bf16[64,144,128]{2,1,0:T(8,128)(2,1)} %dispatch.1), calls=%async_computation | async-start | bytes 4718592 | tf_op jit(solution)/shard_map/all_to_all | solution.py:642
  15.7 2.3 %copy-done = bf16[1,64,18,2048]{3,1,2,0:T(8,128)(2,1)S(1)} copy-done((bf16[1,64,18,2048]{3,1,2,0:T(8,128)(2,1)S(1)}, bf16[1,64,18,2048]{3,1,2,0:T(8,128)(2,1)}, u32[]{:S(2)}) %copy-start) | copy-done | bytes 4718616
  18.1 1.4 ordered_rows.1
  19.6 1.9 %mixer_forward.1 = (f32[224,512]{1,0:T(8,128)S(1)}, bf16[224,512]{1,0:T(8,128)(2,1)S(1)}, f32[224,8]{1,0:T(8,128)S(1)}, f32[224,24]{1,0:T(8,128)S(1)}, f32[8,224]{1,0:T(8,128)S(1)}) custom-call(bf16[224,512]{1,0:T(8,128)(2,1)S(1)} %copy-done.17, bf16[224,256]{1,0:T(8,128)(2,1)S(1)} %copy-done.22, bf16[224,256]{1,0:T(8,128)(2,1)S(1)} %copy-done.20, ...), custom_call_target="tpu_custom_call" | custom-call | flops 1000000000 | bytes 1000000 | tf_op jit(solution)/shard_map/mixer_forward/pallas_call | solution.py:181
  24.9 2.6 %fusion.1 = f32[1152,512]{1,0:T(8,128)S(1)} fusion(bf16[1152,2048]{1,0:T(8,128)(2,1)S(1)} %ordered_rows.1, bf16[1,2048,512]{2,1,0:T(8,128)(2,1)S(1)} %copy-done.28), kind=kOutput, calls=%fused_computation.7 | convolution fusion | flops 2415919104 | bytes 9175040 | tf_op jit(solution)/shard_map/dot_general | solution.py:647
  27.5 5.1 %add_multiply_fusion = (f32[1152,512]{1,0:T(8,128)}, bf16[1152,512]{1,0:T(8,128)(2,1)S(1)}, f32[1152,512]{1,0:T(8,128)}) fusion(f32[1152,512]{1,0:T(8,128)S(1)} %fusion.1, bf16[1152,2048]{1,0:T(8,128)(2,1)S(1)} %ordered_rows.1, bf16[1,2048,512]{2,1,0:T(8,128)(2,1)S(1)} %copy-done.30), kind=kOutput, calls=%fused_computation.3 | convolution fusion | flops 2422407168 | bytes 15073280 | tf_op jit(solution)/shard_map/dot_general | solution.py:646
  32.6 15.9 %all-to-all-done.mine_ref = bf16[64,144,128]{2,1,0:T(8,128)(2,1)S(1)} async-done(((bf16[64,144,128]{2,1,0:T(8,128)(2,1)}), bf16[64,144,128]{2,1,0:T(8,128)(2,1)S(1)}, u32[]{:S(2)}, u32[]{:S(2)}) %all-to-all-start) | async-done | bytes 2359328 | tf_op jit(solution)/shard_map/all_to_all | solution.py:642
  48.5 1.6 copy-done.9
  50.1 2.0 %hidden_first.1 = (bf16[1152,1024]{1,0:T(8,128)(2,1)S(1)}, f32[1152,512]{1,0:T(8,128)S(1)}) custom-call(s32[1]{0:T(128)} %bitcast.tp_ref.half_ref, bf16[64,144,128]{2,1,0:T(8,128)(2,1)S(1)} %all-to-all-done.mine_ref, bf16[512,2048]{1,0:T(8,128)(2,1)S(1)} %bitcast.27), custom_call_target="tpu_custom_call" | custom-call | flops 2000000000 | bytes 10000000 | tf_op jit(solution)/shard_map/hidden_first/pallas_call | solution.py:181
  52.1 1.4 copy-done.2
  53.5 2.3 %hidden_second.1 = (bf16[1152,1024]{1,0:T(8,128)(2,1)S(1)}, bf16[1152,512]{1,0:T(8,128)(2,1)S(1)}, bf16[1152,512]{1,0:T(8,128)(2,1)S(1)}) custom-call(s32[1]{0:T(128)} %bitcast.tp_ref.half_ref, bf16[64,144,128]{2,1,0:T(8,128)(2,1)S(1)} %collective-permute-done.other_ref, bf16[512,2048]{1,0:T(8,128)(2,1)S(1)} %bitcast.28, ...), custom_call_target="tpu_custom_call" | custom-call | flops 2000000000 | bytes 10000000 | tf_op jit(solution)/shard_map/hidden_second/pallas_call | solution.py:181
  55.9 3.7 %span_half.3 = bf16[64,144,128]{2,1,0:T(8,128)(2,1)S(1)} custom-call(s32[1]{0:T(128)} %bitcast.tp_ref.half_ref, bf16[1152,512]{1,0:T(8,128)(2,1)S(1)} %get-tuple-element.83.gg_ref, bf16[1152,512]{1,0:T(8,128)(2,1)S(1)} %get-tuple-element.84.ug_ref, bf16[2048,512]{1,0:T(8,128)(2,1)S(1)} %bitcast.34, bf16[2048,512]{1,0:T(8,128)(2,1)S(1)} %bitcast.32), custom_call_target="tpu_custom_call" | custom-call | flops 4000000000 | bytes 10000000 | tf_op jit(solution)/shard_map/span_half/pallas_call | solution.py:181
  60.2 3.7 %span_half.2 = bf16[64,144,128]{2,1,0:T(8,128)(2,1)S(1)} custom-call(s32[1]{0:T(128)} %bitcast.tp_ref.half_ref, bf16[1152,512]{1,0:T(8,128)(2,1)S(1)} %get-tuple-element.83.gg_ref, bf16[1152,512]{1,0:T(8,128)(2,1)S(1)} %get-tuple-element.84.ug_ref, bf16[2048,512]{1,0:T(8,128)(2,1)S(1)} %bitcast.35, bf16[2048,512]{1,0:T(8,128)(2,1)S(1)} %bitcast.33), custom_call_target="tpu_custom_call" | custom-call | flops 4000000000 | bytes 10000000 | tf_op jit(solution)/shard_map/span_half/pallas_call | solution.py:181
  64.3 2.2 %add_convert_fusion = bf16[64,144,128]{2,1,0:T(8,128)(2,1)} fusion(bf16[64,144,128]{2,1,0:T(8,128)(2,1)S(1)} %collective-permute-done.1, bf16[64,144,128]{2,1,0:T(8,128)(2,1)S(1)} %span_half.2), kind=kLoop, calls=%fused_computation | loop fusion | flops 4718592 | bytes 7077888 | tf_op jit(solution)/shard_map/convert_element_type | solution.py:674
  66.5 6.4 %all-to-all-start.1 = ((bf16[64,144,128]{2,1,0:T(8,128)(2,1)}), bf16[64,144,128]{2,1,0:T(8,128)(2,1)S(1)}, u32[]{:S(2)}, u32[]{:S(2)}) async-start(bf16[64,144,128]{2,1,0:T(8,128)(2,1)} %add_convert_fusion), calls=%async_computation.1 | async-start | bytes 4718592 | tf_op jit(solution)/shard_map/all_to_all | solution.py:675
  72.9 1.7 copy-done.3
  74.6 1.7 copy-done.5
  76.2 4.9 %down_grad.1 = bf16[512,2048]{1,0:T(8,128)(2,1)} custom-call(s32[1]{0:T(128)} %bitcast.tp_ref.half_ref, bf16[1152,512]{1,0:T(8,128)(2,1)S(1)} %get-tuple-element.79.act_ref, bf16[1152,1024]{1,0:T(8,128)(2,1)S(1)} %copy-done.3, bf16[1152,1024]{1,0:T(8,128)(2,1)S(1)} %copy-done.5), custom_call_target="tpu_custom_call" | custom-call | flops 2000000000 | bytes 10000000 | tf_op jit(solution)/shard_map/down_grad/pallas_call | solution.py:181
  81.2 6.7 %convolution_convert_fusion.1 = bf16[2048,512]{1,0:T(8,128)(2,1)} fusion(bf16[1152,2048]{1,0:T(8,128)(2,1)} %copy-done.1, bf16[1152,512]{1,0:T(8,128)(2,1)S(1)} %copy-done.35), kind=kOutput, calls=%fused_computation.2 | convolution fusion | flops 2416967680 | bytes 7995392 | tf_op jit(solution)/shard_map/dot_general | solution.py:43
  87.9 4.1 %convolution_convert_fusion = bf16[2048,512]{1,0:T(8,128)(2,1)} fusion(bf16[1152,2048]{1,0:T(8,128)(2,1)S(1)} %bitcast.26, bf16[1152,512]{1,0:T(8,128)(2,1)S(1)} %copy-done.33), kind=kOutput, calls=%fused_computation.1 | convolution fusion | flops 2416967680 | bytes 7995392 | tf_op jit(solution)/shard_map/dot_general | solution.py:43
  92.0 14.4 %all-to-all-done.1.ret_ref = bf16[64,144,128]{2,1,0:T(8,128)(2,1)S(1)} async-done(((bf16[64,144,128]{2,1,0:T(8,128)(2,1)}), bf16[64,144,128]{2,1,0:T(8,128)(2,1)S(1)}, u32[]{:S(2)}, u32[]{:S(2)}) %all-to-all-start.1) | async-done | bytes 2359328 | tf_op jit(solution)/shard_map/all_to_all | solution.py:675
  106.4 1.6 combine.1.mine_ref
  108.7 1.2 collective-permute-done.2.other_ref
  109.9 1.7 %mixer_cotangent.1 = (bf16[224,2048]{1,0:T(8,128)(2,1)}, f32[224,512]{1,0:T(8,128)S(1)}, bf16[224,512]{1,0:T(8,128)(2,1)}, bf16[64,16,128]{2,1,0:T(8,128)(2,1)}) custom-call(s32[1]{0:T(128)} %bitcast.tp_ref.half_ref, bf16[224,1024]{1,0:T(8,128)(2,1)S(1)} %combine.1.mine_ref, bf16[224,1024]{1,0:T(8,128)(2,1)S(1)} %collective-permute-done.2.other_ref, ...), custom_call_target="tpu_custom_call" | custom-call | flops 1000000000 | bytes 5000000 | tf_op jit(solution)/shard_map/mixer_cotangent/pallas_call | solution.py:181
  112.4 5.5 %all-to-all-start.2 = ((bf16[64,16,128]{2,1,0:T(8,128)(2,1)}), bf16[64,16,128]{2,1,0:T(8,128)(2,1)S(1)}, u32[]{:S(2)}, u32[]{:S(2)}) async-start(bf16[64,16,128]{2,1,0:T(8,128)(2,1)} %get-tuple-element.95), calls=%async_computation.2 | async-start | bytes 524288 | tf_op jit(solution)/shard_map/all_to_all | solution.py:719
  118.0 5.9 %mixer_backward.1 = (f32[224,512]{1,0:T(8,128)}, f32[224,256]{1,0:T(8,128)}, bf16[224,256]{1,0:T(8,128)(2,1)}, f32[224,8]{1,0:T(8,128)}) custom-call(bf16[224,512]{1,0:T(8,128)(2,1)} %v_ref.2, bf16[224,256]{1,0:T(8,128)(2,1)} %k_ref.3, bf16[224,256]{1,0:T(8,128)(2,1)} %q_far.1, f32[8,224]{1,0:T(8,128)} %copy-done.45, f32[8,64,128]{2,1,0:T(8,128)} %bitcast.29, ...), custom_call_target="tpu_custom_call" | custom-call | flops 2000000000 | bytes 1000000 | tf_op jit(solution)/shard_map/mixer_backward/pallas_call | solution.py:181
  123.9 1.4 shares.1.shares_ref
  125.3 3.6 %all-to-all-done.2.in_ref = bf16[64,16,128]{2,1,0:T(8,128)(2,1)S(1)} async-done(((bf16[64,16,128]{2,1,0:T(8,128)(2,1)}), bf16[64,16,128]{2,1,0:T(8,128)(2,1)S(1)}, u32[]{:S(2)}, u32[]{:S(2)}) %all-to-all-start.2) | async-done | bytes 262176 | tf_op jit(solution)/shard_map/all_to_all | solution.py:719
  128.9 1.3 state_chain.1
  130.2 38.1 %all_to_all.20.in_ref = bf16[64,136,128]{2,1,0:T(8,128)(2,1)S(1)} all-to-all(bf16[64,136,128]{2,1,0:T(8,128)(2,1)S(1)} %state_chain.1), channel_id=1, replica_groups=mesh['sp_0'=4,'sp_1'=4,'sp_2'=4,'tp'=2] {'sp_0','sp_1','sp_2'}, dimensions={0} | all-to-all | bytes 4456448 | tf_op jit(solution)/shard_map/all_to_all | solution.py:774
  169.3 2.3 %mixer_ending.1 = (bf16[224,512]{1,0:T(8,128)(2,1)}, bf16[224,256]{1,0:T(8,128)(2,1)}, f32[8,224]{1,0:T(8,128)}) custom-call(bf16[64,136,128]{2,1,0:T(8,128)(2,1)S(1)} %all_to_all.20.in_ref, bf16[224,512]{1,0:T(8,128)(2,1)S(1)} %copy-done.18, bf16[224,256]{1,0:T(8,128)(2,1)S(1)} %copy-done.23, f32[224,24]{1,0:T(8,128)S(1)} %copy-done.14, ...), custom_call_target="tpu_custom_call" | custom-call | flops 1000000000 | bytes 1000000 | tf_op jit(solution)/shard_map/mixer_ending/pallas_call | solution.py:181
  (99 shorter events, 7.0 us)
Async XLA Ops:
  4.1 44.3 %all-to-all-start = ((bf16[64,144,128]{2,1,0:T(8,128)(2,1)}), bf16[64,144,128]{2,1,0:T(8,128)(2,1)S(1)}, u32[]{:S(2)}, u32[]{:S(2)}) async-start(bf16[64,144,128]{2,1,0:T(8,128)(2,1)} %dispatch.1), calls=%async_computation | async-start | bytes 4718592 | tf_op jit(solution)/shard_map/all_to_all | solution.py:642
  15.7 2.3 %copy-start = (bf16[1,64,18,2048]{3,1,2,0:T(8,128)(2,1)S(1)}, bf16[1,64,18,2048]{3,1,2,0:T(8,128)(2,1)}, u32[]{:S(2)}) copy-start(bf16[1,64,18,2048]{3,1,2,0:T(8,128)(2,1)} %param.17) | copy-start | bytes 14155780
  19.5 8.0 %copy-start.1 = (bf16[1152,2048]{1,0:T(8,128)(2,1)}, bf16[1152,2048]{1,0:T(8,128)(2,1)S(1)}, u32[]{:S(2)}) copy-start(bf16[1152,2048]{1,0:T(8,128)(2,1)S(1)} %ordered_rows.1) | copy-start | bytes 14155780
  19.5 5.4 %copy-start.28 = (bf16[1,2048,512]{2,1,0:T(8,128)(2,1)S(1)}, bf16[1,2048,512]{2,1,0:T(8,128)(2,1)}, u32[]{:S(2)}) copy-start(bf16[1,2048,512]{2,1,0:T(8,128)(2,1)} %param.19) | copy-start | bytes 6291460
  24.9 2.6 %copy-start.30 = (bf16[1,2048,512]{2,1,0:T(8,128)(2,1)S(1)}, bf16[1,2048,512]{2,1,0:T(8,128)(2,1)}, u32[]{:S(2)}) copy-start(bf16[1,2048,512]{2,1,0:T(8,128)(2,1)} %param.18) | copy-start | bytes 6291460
  48.5 5.0 %collective-permute-start = (bf16[64,144,128]{2,1,0:T(8,128)(2,1)S(1)}, bf16[64,144,128]{2,1,0:T(8,128)(2,1)S(1)}, u32[]{:S(2)}, u32[]{:S(2)}) collective-permute-start(bf16[64,144,128]{2,1,0:T(8,128)(2,1)S(1)} %all-to-all-done.mine_ref), channel_id=1, source_target_pairs={{0,1},{1,0},{2,3},{3,2},{4,5},{5,4},{6,7},{7,6},{8,9},{9,8},{10,11... | collective-permute-start | bytes 7077896 | tf_op jit(solution)/shard_map/ppermute | solution.py:639
  50.1 3.4 %copy-start.6 = (f32[1152,512]{1,0:T(8,128)S(1)}, f32[1152,512]{1,0:T(8,128)}, u32[]{:S(2)}) copy-start(f32[1152,512]{1,0:T(8,128)} %get-tuple-element.74.a1_ref) | copy-start | bytes 7077892
  50.1 3.4 %copy-start.7 = (f32[1152,512]{1,0:T(8,128)S(1)}, f32[1152,512]{1,0:T(8,128)}, u32[]{:S(2)}) copy-start(f32[1152,512]{1,0:T(8,128)} %get-tuple-element.75.a2_ref) | copy-start | bytes 7077892
  53.5 2.4 %copy-start.29 = (bf16[1,2048,512]{2,1,0:T(8,128)(2,1)S(1)}, bf16[1,2048,512]{2,1,0:T(8,128)(2,1)}, u32[]{:S(2)}) copy-start(bf16[1,2048,512]{2,1,0:T(8,128)(2,1)} %param.19) | copy-start | bytes 6291460
  53.5 2.4 %copy-start.31 = (bf16[1,2048,512]{2,1,0:T(8,128)(2,1)S(1)}, bf16[1,2048,512]{2,1,0:T(8,128)(2,1)}, u32[]{:S(2)}) copy-start(bf16[1,2048,512]{2,1,0:T(8,128)(2,1)} %param.18) | copy-start | bytes 6291460
  55.8 3.7 %copy-start.4 = (bf16[1152,1024]{1,0:T(8,128)(2,1)}, bf16[1152,1024]{1,0:T(8,128)(2,1)S(1)}, u32[]{:S(2)}) copy-start(bf16[1152,1024]{1,0:T(8,128)(2,1)S(1)} %get-tuple-element.81.other_ref) | copy-start | bytes 7077892
  55.9 4.3 %copy-start.32 = (bf16[1152,512]{1,0:T(8,128)(2,1)}, bf16[1152,512]{1,0:T(8,128)(2,1)S(1)}, u32[]{:S(2)}) copy-start(bf16[1152,512]{1,0:T(8,128)(2,1)S(1)} %get-tuple-element.84.ug_ref) | copy-start | bytes 3538948
  55.9 4.3 %copy-start.34 = (bf16[1152,512]{1,0:T(8,128)(2,1)}, bf16[1152,512]{1,0:T(8,128)(2,1)S(1)}, u32[]{:S(2)}) copy-start(bf16[1152,512]{1,0:T(8,128)(2,1)S(1)} %get-tuple-element.83.gg_ref) | copy-start | bytes 3538948
  59.6 4.8 %collective-permute-start.1 = (bf16[64,144,128]{2,1,0:T(8,128)(2,1)S(1)}, bf16[64,144,128]{2,1,0:T(8,128)(2,1)S(1)}, u32[]{:S(2)}, u32[]{:S(2)}) collective-permute-start(bf16[64,144,128]{2,1,0:T(8,128)(2,1)S(1)} %span_half.3), channel_id=1, source_target_pairs={{0,1},{1,0},{2,3},{3,2},{4,5},{5,4},{6,7},{7,6},{8,9},{9,8},{10,11... | collective-permute-start | bytes 7077896 | tf_op jit(solution)/shard_map/ppermute | solution.py:639
  66.5 39.8 %all-to-all-start.1 = ((bf16[64,144,128]{2,1,0:T(8,128)(2,1)}), bf16[64,144,128]{2,1,0:T(8,128)(2,1)S(1)}, u32[]{:S(2)}, u32[]{:S(2)}) async-start(bf16[64,144,128]{2,1,0:T(8,128)(2,1)} %add_convert_fusion), calls=%async_computation.1 | async-start | bytes 4718592 | tf_op jit(solution)/shard_map/all_to_all | solution.py:675
  76.2 4.9 %copy-start.35 = (bf16[1152,512]{1,0:T(8,128)(2,1)S(1)}, bf16[1152,512]{1,0:T(8,128)(2,1)}, u32[]{:S(2)}) copy-start(bf16[1152,512]{1,0:T(8,128)(2,1)} %copy-done.34) | copy-start | bytes 3538948
  76.2 11.6 %slice-start = ((s8[4718592]{0:T(1024)(128)(4,1)}), s8[4194304]{0:T(1024)(128)(4,1)S(1)}, s32[]{:S(2)}) async-start(s8[4718592]{0:T(1024)(128)(4,1)} %bitcast.25), calls=%async_computation.4 | async-start | bytes 8388608
  81.2 6.7 %slice-start.1 = ((s8[4718592]{0:T(1024)(128)(4,1)}), s8[524288]{0:T(1024)(128)(4,1)S(1)}, s32[]{:S(2)}) async-start(s8[4718592]{0:T(1024)(128)(4,1)} %bitcast.25), calls=%async_computation.5 | async-start | bytes 1048576
  81.2 6.7 %copy-start.33 = (bf16[1152,512]{1,0:T(8,128)(2,1)S(1)}, bf16[1152,512]{1,0:T(8,128)(2,1)}, u32[]{:S(2)}) copy-start(bf16[1152,512]{1,0:T(8,128)(2,1)} %copy-done.32) | copy-start | bytes 3538948
  87.8 18.5 %copy-start.10 = (bf16[224,2048]{1,0:T(8,128)(2,1)S(1)}, bf16[224,2048]{1,0:T(8,128)(2,1)}, u32[]{:S(2)}) copy-start(bf16[224,2048]{1,0:T(8,128)(2,1)} %og_ref.1) | copy-start | bytes 2752516
  87.8 18.5 %copy-start.25 = (f32[224,8]{1,0:T(8,128)S(1)}, f32[224,8]{1,0:T(8,128)}, u32[]{:S(2)}) copy-start(f32[224,8]{1,0:T(8,128)} %copy-done.24) | copy-start | bytes 21508
  108.0 1.9 %collective-permute-start.2 = (bf16[224,1024]{1,0:T(8,128)(2,1)S(1)}, bf16[224,1024]{1,0:T(8,128)(2,1)S(1)}, u32[]{:S(2)}, u32[]{:S(2)}) collective-permute-start(bf16[224,1024]{1,0:T(8,128)(2,1)S(1)} %combine.1.mine_ref), channel_id=1, source_target_pairs={{0,1},{1,0},{2,3},{3,2},{4,5},{5,4},{6,7},{7,6},{8,9},{9,8},{10,11... | collective-permute-start | bytes 1376264 | tf_op jit(solution)/shard_map/ppermute | solution.py:639
  112.4 16.4 %all-to-all-start.2 = ((bf16[64,16,128]{2,1,0:T(8,128)(2,1)}), bf16[64,16,128]{2,1,0:T(8,128)(2,1)S(1)}, u32[]{:S(2)}, u32[]{:S(2)}) async-start(bf16[64,16,128]{2,1,0:T(8,128)(2,1)} %get-tuple-element.95), calls=%async_computation.2 | async-start | bytes 524288 | tf_op jit(solution)/shard_map/all_to_all | solution.py:719
  118.0 5.9 %copy-start.36 = (bf16[224,2048]{1,0:T(8,128)(2,1)S(1)}, bf16[224,2048]{1,0:T(8,128)(2,1)}, u32[]{:S(2)}) copy-start(bf16[224,2048]{1,0:T(8,128)(2,1)} %get-tuple-element.102.hidden_ref) | copy-start | bytes 2752516
  118.0 5.9 %copy-start.44 = (bf16[224,512]{1,0:T(8,128)(2,1)S(1)}, bf16[224,512]{1,0:T(8,128)(2,1)}, u32[]{:S(2)}) copy-start(bf16[224,512]{1,0:T(8,128)(2,1)} %copy-done.43) | copy-start | bytes 688132
  130.1 39.1 %copy-start.11 = (f32[224,512]{1,0:T(8,128)S(1)}, f32[224,512]{1,0:T(8,128)}, u32[]{:S(2)}) copy-start(f32[224,512]{1,0:T(8,128)} %get-tuple-element.110.dv_ref) | copy-start | bytes 1376260
  130.2 39.1 %copy-start.14 = (f32[224,24]{1,0:T(8,128)S(1)}, f32[224,24]{1,0:T(8,128)}, u32[]{:S(2)}) copy-start(f32[224,24]{1,0:T(8,128)} %copy-done.12) | copy-start | bytes 64516
  130.2 39.1 %copy-start.16 = (f32[1,8,64,128]{3,2,1,0:T(8,128)S(1)}, f32[1,8,64,128]{3,2,1,0:T(8,128)}, u32[]{:S(2)}) copy-start(f32[1,8,64,128]{3,2,1,0:T(8,128)} %param.26) | copy-start | bytes 786436
  130.2 39.1 %copy-start.18 = (bf16[224,512]{1,0:T(8,128)(2,1)S(1)}, bf16[224,512]{1,0:T(8,128)(2,1)}, u32[]{:S(2)}) copy-start(bf16[224,512]{1,0:T(8,128)(2,1)} %v_ref.2) | copy-start | bytes 688132
  130.2 39.1 %copy-start.19 = (f32[224,256]{1,0:T(8,128)S(1)}, f32[224,256]{1,0:T(8,128)}, u32[]{:S(2)}) copy-start(f32[224,256]{1,0:T(8,128)} %get-tuple-element.111.dk_ref) | copy-start | bytes 688132
  130.2 39.1 %copy-start.23 = (bf16[224,256]{1,0:T(8,128)(2,1)S(1)}, bf16[224,256]{1,0:T(8,128)(2,1)}, u32[]{:S(2)}) copy-start(bf16[224,256]{1,0:T(8,128)(2,1)} %k_ref.3) | copy-start | bytes 344068
  130.2 39.1 %copy-start.26 = (f32[224,8]{1,0:T(8,128)S(1)}, f32[224,8]{1,0:T(8,128)}, u32[]{:S(2)}) copy-start(f32[224,8]{1,0:T(8,128)} %get-tuple-element.112.diff_ref) | copy-start | bytes 21508
  (22 other events, 30.0 us)
